TPU v7x, 32 devices: a whole 2x2x4 slice. The times are simulated.
32 devices in a mesh: grp: 2 (over x), fs: 4 (over y, core), tp: 4 (over z).
Axes of the slice: x: 2, y: 2, z: 4, core: 2. Of those that a mesh axis runs over, the one named last changes fastest.
Arguments:
- prompt_tokens: bfloat16 [4096, 2048], P(('grp', 'fs', 'tp')), parts along dimension 0, may hold values from -6 to 6
- up_weight: float32 [2048, 8192], P('fs', 'tp'), may hold values from -0.125 to 0.125
- down_weight: float32 [2048, 8192], P('fs', 'tp'), may hold values from -0.0625 to 0.0625
- pre_gain: float32 [2048], P('fs'), may hold values from 0.1 to 1.9
- post_gain: float32 [2048], replicated, may hold values from 0.1 to 1.9
Outputs:
- mixed: bfloat16 [4096, 2048], P(('grp', 'fs', 'tp')), parts along dimension 0
- sampler_up: bfloat16 [4096, 8192], P('grp', 'tp'), parts along dimension 0
- sampler_down: bfloat16 [4096, 8192], P('grp', 'tp'), parts along dimension 0
There are 2 independent parts, one for each index of `grp`. A program takes and returns all parts, laid end to end along the dimension named above; an argument that names none is the same for every part. Nothing has to cross between parts.
All inputs are finite; a program needn't handle non-finite values.
Results may differ from a plain program's by a relative error of at most 0.015.
Values may be sent and summed in bfloat16 or wider, within the bound.
No kernel may reach another device: no remote copies, remote signals or barrier semaphores. Data moves between devices by JAX's collectives and lax.ppermute only.
A program may use at most 128 MiB of HBM per device.

v0:
```python
import jax
import jax.numpy as jnp
from jax import lax
from jax.sharding import PartitionSpec as P


def per_device(prompt_tokens, up_weight, down_weight, pre_gain, post_gain):
    up_local = (up_weight * pre_gain[:, None]).astype(jnp.bfloat16)
    down_local = down_weight.astype(jnp.bfloat16)
    values = prompt_tokens.astype(jnp.float32)
    normed = (values * lax.rsqrt(jnp.mean(values * values, axis=1, keepdims=True) + 1e-06)).astype(
        jnp.bfloat16
    )
    sampler_up, sampler_down = (
        lax.all_gather(up_local, "fs", axis=0, tiled=True),
        lax.all_gather(down_local, "fs", axis=0, tiled=True),
    )
    lifted = jnp.dot(
        lax.all_gather(normed, "tp", axis=0, tiled=True),
        sampler_up,
        preferred_element_type=jnp.float32,
    )
    hidden = jnp.square(jax.nn.relu(lifted)).astype(jnp.bfloat16)
    summed = lax.psum_scatter(
        lax.dot_general(
            hidden, sampler_down, (((1,), (1,)), ((), ())), preferred_element_type=jnp.float32
        ).astype(jnp.bfloat16),
        "tp",
        scatter_dimension=0,
        tiled=True,
    ).astype(jnp.float32)
    scaled = summed * lax.rsqrt(jnp.mean(summed * summed, axis=1, keepdims=True) + 1e-06)
    mixed = (scaled * post_gain[None, :]).astype(jnp.bfloat16)
    return (mixed, sampler_up, sampler_down)


def solution(mesh):
    placed = (P(("grp", "fs", "tp"), None), P("fs", "tp"), P("fs", "tp"), P("fs"), P())
    return jax.shard_map(
        per_device,
        mesh=mesh,
        in_specs=placed,
        out_specs=(P(("grp", "fs", "tp"), None), P("grp", "tp"), P("grp", "tp")),
        check_vma=False,
    )
```

profile of v0, /device:TPU:0, one launch (start us, length us, event | category | flops | bytes accessed | tf_op | source)
XLA Modules:
  0.0 265.7 jit_solution(5066965389178030191)
XLA Ops:
  7.2 0.0 all-gather.4.cloned.1.call-start
  7.2 1.2 fusion
  8.4 2.0 fusion.1
  10.4 0.0 all-gather.4.cloned.1.call-update
  10.5 0.0 all-gather.6.cloned.1.call-start
  10.5 3.8 %multiply_convert_fusion.1 = bf16[512,2048]{1,0:T(8,128)(2,1)} fusion(f32[512,2048]{1,0:T(8,128)} %param.6, f32[512]{0:T(512)} %param.8), kind=kLoop, calls=%fused_computation.1 | loop fusion | flops 2097152 | bytes 6293504 | tf_op jit(solution)/shard_map/convert_element_type | solution.py:8
  14.3 0.0 all-gather.6.cloned.1.call-update
  14.3 0.0 all-gather.8.cloned.1.call-start
  14.4 3.8 %convert_element_type.28 = bf16[512,2048]{1,0:T(8,128)(2,1)} convert(f32[512,2048]{1,0:T(8,128)} %param.7) | non-fusion elementwise | flops 1048576 | bytes 6291456 | tf_op jit(solution)/shard_map/convert_element_type | solution.py:9
  18.2 0.0 all-gather.8.cloned.1.call-update
  18.2 0.0 copy-start
  18.3 0.0 reduce-scatter.2.cloned.1.call-start
  18.3 40.7 %all-gather.4.cloned.1.call-done = bf16[512,2048]{1,0:T(8,128)(2,1)} async-done(((bf16[128,2048]{1,0:T(8,128)(2,1)}), bf16[512,2048]{1,0:T(8,128)(2,1)}) %all-gather.4.cloned.1.call-update) | async-done | bytes 2097168 | tf_op jit(solution)/shard_map/all_gather | solution.py:19
  59.0 59.2 %all-gather.6.cloned.1.call-done = bf16[2048,2048]{1,0:T(8,128)(2,1)} async-done(((bf16[512,2048]{1,0:T(8,128)(2,1)}), bf16[2048,2048]{1,0:T(8,128)(2,1)}) %all-gather.6.cloned.1.call-update) | async-done | bytes 8388624 | tf_op jit(solution)/shard_map/all_gather | solution.py:15
  118.2 60.4 %all-gather.8.cloned.1.call-done = bf16[2048,2048]{1,0:T(8,128)(2,1)} async-done(((bf16[512,2048]{1,0:T(8,128)(2,1)}), bf16[2048,2048]{1,0:T(8,128)(2,1)}) %all-gather.8.cloned.1.call-update) | async-done | bytes 8388624 | tf_op jit(solution)/shard_map/all_gather | solution.py:16
  178.7 16.5 %convolution_convert_fusion = bf16[512,2048]{1,0:T(8,128)(2,1)} fusion(bf16[2048,2048]{1,0:T(8,128)(2,1)} %all-gather.8.cloned.1.call-done, bf16[512,2048]{1,0:T(8,128)(2,1)} %all-gather.4.cloned.1.call-done, bf16[2048,2048]{1,0:T(8,128)(2,1)} %all-gather.6.cloned.1.call-done), kind=kOutput, calls=%fused_computation.2 | convolution fusion | flops 8594128896 | bytes 20971520 | tf_op jit(solution)/shard_map/dot_general | solution.py:25
  195.2 0.0 reduce-scatter.2.cloned.1.call-update
  195.2 43.8 %reduce-scatter.2.cloned.1.call-done = bf16[128,2048]{1,0:T(8,128)(2,1)} async-done(((bf16[512,2048]{1,0:T(8,128)(2,1)}), bf16[128,2048]{1,0:T(8,128)(2,1)}) %reduce-scatter.2.cloned.1.call-update) | async-done | bytes 524304 | tf_op jit(solution)/shard_map/reduce_scatter | solution.py:24
  239.0 1.2 fusion.2
  240.2 0.0 copy-done
  240.2 2.0 fusion.4
  242.3 8.4 %copy.10 = bf16[2048,2048]{1,0:T(8,128)(2,1)} copy(bf16[2048,2048]{1,0:T(8,128)(2,1)} %all-gather.6.cloned.1.call-done) | data formatting | bytes 16777216
  250.7 8.4 %copy.11 = bf16[2048,2048]{1,0:T(8,128)(2,1)} copy(bf16[2048,2048]{1,0:T(8,128)(2,1)} %all-gather.8.cloned.1.call-done) | data formatting | bytes 16777216
  (2 shorter events, 0.0 us)
Async XLA Ops:
  7.2 51.8 %all-gather.4.cloned.1.call-start = ((), (), s32[]{:S(2)}) async-start(), calls=%async_computation.1 | async-start | bytes 2621440 | tf_op jit(solution)/shard_map/all_gather | solution.py:19
  10.5 107.8 %all-gather.6.cloned.1.call-start = ((), (), s32[]{:S(2)}) async-start(), calls=%async_computation.2 | async-start | bytes 10485760 | tf_op jit(solution)/shard_map/all_gather | solution.py:15
  14.3 164.3 %all-gather.8.cloned.1.call-start = ((), (), s32[]{:S(2)}) async-start(), calls=%async_computation.3 | async-start | bytes 10485760 | tf_op jit(solution)/shard_map/all_gather | solution.py:16
  18.2 222.0 %copy-start = (f32[2048]{0:T(1024)S(1)}, f32[2048]{0:T(1024)}, u32[]{:S(2)}) copy-start(f32[2048]{0:T(1024)} %param.9) | copy-start | bytes 24580
  18.3 220.7 %reduce-scatter.2.cloned.1.call-start = ((), (), s32[]{:S(2)}) async-start(), calls=%async_computation.4 | async-start | bytes 2621440 | tf_op jit(solution)/shard_map/reduce_scatter | solution.py:24
Sparse Core Ops, SparseCore 0:
  10.6 48.3 all-gather.3
  61.1 57.0 all-gather.5
  120.4 58.2 all-gather.7
  195.3 43.6 reduce-scatter.1
where the time goes:
time: 266 us
  waiting for transfers between devices  204 us (77%)
  local copies, waits for them, and re-layouts  16.9 us (6%)
  matrix products  16.5 us (6%)
  other arithmetic  14.1 us (5%)
  between operations  13.8 us (5%)
    all_gather x1, waiting for transfers between devices, per_device(): lax.all_gather(down_local, 'fs', axis=0, tiled=True)  60.4 us
    all_gather x1, waiting for transfers between devices, per_device(): lax.all_gather(up_local, 'fs', axis=0, tiled=True)  59.2 us
    reduce_scatter x1, waiting for transfers between devices, per_device(): lax.psum_scatter(lax.dot_general(hidden, sampler_down, (((1,), (1,)), (()...  43.8 us
    all_gather x1, waiting for transfers between devices, per_device(): lax.all_gather(normed, 'tp', axis=0, tiled=True)  40.7 us
    unnamed x4, local copies, waits for them, and re-layouts  16.9 us
    dot_general x1, matrix products, per_device(): lax.dot_general(hidden, sampler_down, (((1,), (1,)), ((), ())), preferred...  16.5 us
  transfers between devices with their start and end apart: 4, of which 4 were waited for; matrix products, arithmetic and copies ran while one was open for 3% of the time, Pallas kernels for 0%

commit v1 on v0

v1 whole, which is shorter than its diff:
```python
import jax
import jax.numpy as jnp
from jax import lax
from jax.experimental import pallas as pl
from jax.experimental.pallas import tpu as pltpu
from jax.sharding import PartitionSpec as P


BF = jnp.bfloat16
F32 = jnp.float32
ANY = pl.BlockSpec(memory_space=pl.ANY)
SMEM = pl.BlockSpec(memory_space=pltpu.SMEM)
LIMIT = pltpu.CompilerParams(vmem_limit_bytes=48 * 2**20)


def plain(prompt_tokens, up_weight, down_weight, pre_gain, post_gain):
    up_local = (up_weight * pre_gain[:, None]).astype(BF)
    down_local = down_weight.astype(BF)
    values = prompt_tokens.astype(F32)
    normed = (
        values * lax.rsqrt(jnp.mean(values * values, axis=1, keepdims=True) + 1e-06)
    ).astype(BF)
    sampler_up = lax.all_gather(up_local, "fs", axis=0, tiled=True)
    sampler_down = lax.all_gather(down_local, "fs", axis=0, tiled=True)
    lifted = jnp.dot(
        lax.all_gather(normed, "tp", axis=0, tiled=True),
        sampler_up,
        preferred_element_type=F32,
    )
    hidden = jnp.square(jax.nn.relu(lifted)).astype(BF)
    part = lax.dot_general(
        hidden, sampler_down, (((1,), (1,)), ((), ())), preferred_element_type=F32
    )
    summed = lax.psum_scatter(
        part.astype(BF), "tp", scatter_dimension=0, tiled=True
    ).astype(F32)
    scaled = summed * lax.rsqrt(jnp.mean(summed * summed, axis=1, keepdims=True) + 1e-06)
    return (scaled * post_gain[None, :]).astype(BF), sampler_up, sampler_down


def norm_tokens(tokens, starts, sizes):
    n, width = tokens.shape

    def body(at, x, o, buf):
        v = x[...].astype(F32)
        buf[...] = (v * lax.rsqrt(jnp.mean(v * v, axis=1, keepdims=True) + 1e-06)).astype(BF)
        col = 0
        for p, size in enumerate(sizes):
            o[:, col : col + size] = buf[:, pl.ds(pl.multiple_of(at[p], 128), size)]
            col += size

    return pl.pallas_call(
        body,
        out_shape=jax.ShapeDtypeStruct((n, width), BF),
        in_specs=[SMEM, pl.BlockSpec(memory_space=pltpu.VMEM)],
        out_specs=pl.BlockSpec(memory_space=pltpu.VMEM),
        scratch_shapes=[pltpu.VMEM((n, width), BF)],
        name="norm_tokens",
    )(starts, tokens)


def up_tile(blocks, pieces, starts, j, n_tiles, hidden, whole, rows, sub=256):
    tok, width = blocks[0].shape
    n_tok = tok * len(blocks)
    hid = pieces[0].shape[1]
    tile = hid // n_tiles
    steps = tile // sub
    n, nb = len(pieces), len(blocks)
    sizes = [p.shape[0] for p in pieces]

    def body(*refs):
        at, toks, ins = refs[0], refs[1 : 1 + nb], refs[1 + nb : 1 + nb + n]
        o, whole_out, x, sem = refs[-4:]
        i = pl.program_id(0)

        @pl.when(i == 0)
        def _():
            for b in range(nb):
                x[b * tok : (b + 1) * tok, :] = toks[b][...]

        copies = []
        for p in range(n):
            c = pltpu.make_async_copy(
                ins[p],
                whole_out.at[
                    pl.ds(pl.multiple_of(at[p], 16), sizes[p]),
                    pl.ds(pl.multiple_of(j * tile + i * sub, sub), sub),
                ],
                sem.at[p],
            )
            c.start()
            copies.append(c)
        total, c0 = None, 0
        for p in range(n):
            term = jnp.dot(x[:, c0 : c0 + sizes[p]], ins[p][...], preferred_element_type=F32)
            total = term if total is None else total + term
            c0 += sizes[p]
        o[...] = jnp.square(jnp.maximum(total, 0.0)).astype(BF)
        for c in copies:
            c.wait()

    in_specs = [SMEM] + [pl.BlockSpec((tok, width), lambda i: (0, 0))] * nb
    for p in pieces:
        first = j * steps if p.shape[1] == hid else 0
        in_specs.append(pl.BlockSpec((p.shape[0], sub), lambda i, f=first: (0, f + i)))
    args = [starts, *blocks, *pieces]
    aliases = {}
    if hidden is not None:
        in_specs += [ANY, ANY]
        args += [hidden, whole]
        aliases = {len(args) - 2: 0, len(args) - 1: 1}
    return pl.pallas_call(
        body,
        grid=(steps,),
        out_shape=(
            jax.ShapeDtypeStruct((n_tok, hid), BF),
            jax.ShapeDtypeStruct((rows, hid), BF),
        ),
        in_specs=in_specs,
        out_specs=(pl.BlockSpec((n_tok, sub), lambda i: (0, j * steps + i)), ANY),
        scratch_shapes=[pltpu.VMEM((n_tok, width), BF), pltpu.SemaphoreType.DMA((n,))],
        input_output_aliases=aliases,
        compiler_params=LIMIT,
        cost_estimate=pl.CostEstimate(
            flops=2 * n_tok * width * tile, bytes_accessed=4 * width * tile, transcendentals=0
        ),
        name="up_tile",
    )(*args)


def up_rest(block, whole, starts, sizes, sub=256):
    tok, width = block.shape
    hid = whole.shape[1]

    def body(at, x, w, o):
        total, c0 = None, 0
        for p, size in enumerate(sizes):
            rows = pl.ds(pl.multiple_of(at[p], 128), size)
            term = jnp.dot(x[:, c0 : c0 + size], w[rows, :], preferred_element_type=F32)
            total = term if total is None else total + term
            c0 += size
        o[...] = jnp.square(jnp.maximum(total, 0.0)).astype(BF)

    return pl.pallas_call(
        body,
        grid=(hid // sub,),
        out_shape=jax.ShapeDtypeStruct((tok, hid), BF),
        in_specs=[
            SMEM,
            pl.BlockSpec((tok, width), lambda i: (0, 0)),
            pl.BlockSpec((width, sub), lambda i: (0, i)),
        ],
        out_specs=pl.BlockSpec((tok, sub), lambda i: (0, i)),
        compiler_params=LIMIT,
        cost_estimate=pl.CostEstimate(
            flops=2 * tok * width * hid, bytes_accessed=2 * width * hid, transcendentals=0
        ),
        name="up_rest",
    )(starts, block, whole)


def down_step(hiddens, outs, pieces, starts, whole, rows, steps, keep_whole=True):
    hid = hiddens[0].shape[1]
    nh, n, no = len(hiddens), len(pieces), len(outs)
    sizes = [p.shape[0] // steps for p in pieces]
    cols = sum(sizes)
    n_tok = sum(h.shape[0] for h in hiddens)

    def body(*refs):
        at, hs, ins = refs[0], refs[1 : 1 + nh], refs[1 + nh : 1 + nh + n]
        tail = refs[-(no + 2) :] if keep_whole else refs[-no:]
        i = pl.program_id(0)
        copies = []
        if keep_whole:
            whole_out, sem = tail[no], tail[no + 1]
            for p in range(n):
                c = pltpu.make_async_copy(
                    ins[p],
                    whole_out.at[pl.ds(pl.multiple_of(at[p] + i * sizes[p], 16), sizes[p]), :],
                    sem.at[p],
                )
                c.start()
                copies.append(c)
        c0 = 0
        for p in range(n):
            prods = [
                lax.dot_general(
                    h[...], ins[p][...], (((1,), (1,)), ((), ())), preferred_element_type=F32
                ).astype(BF)
                for h in hs
            ]
            for o, runs in zip(tail, outs):
                r0 = 0
                for which, first, count in runs:
                    o[r0 : r0 + count, c0 : c0 + sizes[p]] = prods[which][first : first + count]
                    r0 += count
            c0 += sizes[p]
        for c in copies:
            c.wait()

    in_specs = [SMEM] + [pl.BlockSpec(h.shape, lambda i: (0, 0)) for h in hiddens]
    in_specs += [pl.BlockSpec((s, hid), lambda i: (i, 0)) for s in sizes]
    args = [starts, *hiddens, *pieces]
    out_shape, out_specs = [], []
    for runs in outs:
        count = sum(r[2] for r in runs)
        out_shape.append(jax.ShapeDtypeStruct((count, cols * steps), BF))
        out_specs.append(pl.BlockSpec((count, cols), lambda i: (0, i)))
    aliases, scratch = {}, []
    if keep_whole:
        out_shape.append(jax.ShapeDtypeStruct((rows, hid), BF))
        out_specs.append(ANY)
        scratch = [pltpu.SemaphoreType.DMA((n,))]
        if whole is not None:
            in_specs.append(ANY)
            args.append(whole)
            aliases = {len(args) - 1: no}
    return pl.pallas_call(
        body,
        grid=(steps,),
        out_shape=tuple(out_shape),
        in_specs=in_specs,
        out_specs=tuple(out_specs),
        scratch_shapes=scratch,
        input_output_aliases=aliases,
        compiler_params=LIMIT,
        cost_estimate=pl.CostEstimate(
            flops=2 * n_tok * cols * steps * hid,
            bytes_accessed=4 * cols * steps * hid + 2 * n_tok * hid,
            transcendentals=0,
        ),
        name="down_step",
    )(*args)


def finish(terms, starts, layout, post_gain, tok, width):
    counts = [len(t) for t in terms]

    def body(*refs):
        at, gain, ins, o = refs[0], refs[1], list(refs[2:-1]), refs[-1]
        sums = []
        for count in counts:
            group, ins = ins[:count], ins[count:]
            sums.append(sum(g[...].astype(F32) for g in group))
        power = sum(jnp.sum(s * s, axis=1, keepdims=True) for s in sums)
        scale = lax.rsqrt(power / width + 1e-06)
        for p, (i, c0, size) in enumerate(layout):
            to = pl.ds(pl.multiple_of(at[p], 128), size)
            o[:, to] = (sums[i][:, c0 : c0 + size] * scale * gain[:, to]).astype(BF)

    flat = [a for t in terms for a in t]
    vm = pl.BlockSpec(memory_space=pltpu.VMEM)
    return pl.pallas_call(
        body,
        grid=(1,),
        out_shape=jax.ShapeDtypeStruct((tok, width), BF),
        in_specs=[SMEM, pl.BlockSpec((1, width), lambda i: (0, 0))]
        + [pl.BlockSpec((tok, a.shape[1]), lambda i: (0, 0)) for a in flat],
        out_specs=pl.BlockSpec((tok, width), lambda i: (0, 0)),
        name="finish",
    )(starts, post_gain.reshape(1, width), *flat)


U_CUTS = 4
D_CUTS = 2


def routed(n_grp, n_fs, n_tp):
    n_y = n_fs // 2

    def grp_shift(v, d):
        return lax.ppermute(v, "grp", [((i + d) % n_grp, i) for i in range(n_grp)])

    def y_shift(v, d):
        return lax.ppermute(v, "fs", [((i + 2 * d) % n_fs, i) for i in range(n_fs)])

    def core_swap(v):
        return lax.ppermute(v, "fs", [(i, i ^ 1) for i in range(n_fs)])

    def tp_swap(v, m):
        return lax.ppermute(v, "tp", [(i, i ^ m) for i in range(n_tp)])

    def per_device(prompt_tokens, up_weight, down_weight, pre_gain, post_gain):
        fs = lax.axis_index("fs")
        grp = lax.axis_index("grp")
        rows, hid = up_weight.shape
        tok, width = prompt_tokens.shape
        half = rows // n_grp
        tile = hid // U_CUTS
        sub = half // D_CUTS

        def other(dy, dc):
            y = (fs // 2 + dy) % n_y
            return (2 * y + (fs % 2 if dc == 0 else 1 - fs % 2)) * rows

        def table(entries):
            return jnp.stack(entries).astype(jnp.int32)

        own_rows = [other(0, 0), other(0, 1)]
        sides = [((grp + j) % n_grp) * half for j in range(n_grp)]
        up_rows = own_rows + [other(1, dc) + s for dc in range(2) for s in sides]
        up_sizes = [rows, rows] + [half] * (2 * n_grp)
        up_at = table(up_rows)

        def exchange(mine):
            got = y_shift(mine, 1)
            near = [core_swap(got)]
            far = [got]
            for j in range(1, n_grp):
                part = grp_shift(got, j)
                far.append(part)
                near.append(core_swap(part))
            return far + near

        gain = pre_gain[:, None]
        half_up = lax.dynamic_slice_in_dim(up_weight, grp * half, half, 0)
        half_gain = lax.dynamic_slice_in_dim(gain, grp * half, half, 0)
        up_far = [
            exchange((half_up[:, i * tile : (i + 1) * tile] * half_gain).astype(BF))
            for i in range(U_CUTS)
        ]
        down_far = [
            exchange(lax.dynamic_slice_in_dim(down_weight, grp * half + i * sub, sub, 0).astype(BF))
            for i in range(D_CUTS)
        ]
        up_own = (up_weight * gain).astype(BF)
        up_near = [up_own, core_swap(up_own)]
        down_own = down_weight.astype(BF)
        down_near = [down_own, core_swap(down_own)]

        r0 = norm_tokens(prompt_tokens, up_at, up_sizes)
        r2 = tp_swap(r0, 2)
        r1 = tp_swap(r0, 1)
        r3 = tp_swap(r2, 1)

        hidden, whole_up = None, None
        for i in range(U_CUTS):
            hidden, whole_up = up_tile(
                [r1, r0, r2], up_near + up_far[i], up_at, i, U_CUTS, hidden, whole_up, n_fs * rows
            )
        hidden3 = up_rest(r3, whole_up, up_at, up_sizes)

        terms, layout, places = [], [], []

        def place(index, steps, starts, sizes):
            c0 = 0
            for j in range(steps):
                for start, size in zip(starts, sizes):
                    layout.append((index, c0, size // steps))
                    places.append(start + j * (size // steps))
                    c0 += size // steps

        near_steps = rows // 128
        near_at = table(own_rows)
        row1, row0, row2, row3 = (0, 0, tok), (0, tok, tok), (0, 2 * tok, tok), (1, 0, tok)
        send1, keep0, keep2, whole_down = down_step(
            [hidden], [[row1], [row0], [row2]], down_near, near_at, None, n_fs * rows, near_steps
        )
        got1 = tp_swap(send1, 1)
        (send3,) = down_step(
            [hidden3], [[(0, 0, tok)]], down_near, near_at, None, n_fs * rows, near_steps, False
        )
        got3 = tp_swap(send3, 1)
        pair = (keep2.astype(F32) + got3.astype(F32)).astype(BF)
        terms.append([keep0, got1, tp_swap(pair, 2)])
        place(0, near_steps, own_rows, [rows, rows])

        for i in range(D_CUTS):
            at = [other(1, dc) + s + i * sub for dc in range(2) for s in sides]
            send, keep0, keep2, whole_down = down_step(
                [hidden, hidden3],
                [[row1, row3], [row0], [row2]],
                down_far[i],
                table(at),
                whole_down,
                n_fs * rows,
                1,
            )
            got = tp_swap(send, 1)
            pair = (keep2.astype(F32) + got[tok:].astype(F32)).astype(BF)
            terms.append([keep0, got, tp_swap(pair, 2)])
            place(i + 1, 1, at, [sub] * len(at))
        mixed = finish(terms, table(places), layout, post_gain, tok, width)
        return mixed, whole_up, whole_down

    return per_device


def solution(mesh):
    n_grp, n_fs, n_tp = (mesh.shape[a] for a in ("grp", "fs", "tp"))
    placed = (P(("grp", "fs", "tp"), None), P("fs", "tp"), P("fs", "tp"), P("fs"), P())
    fits = n_grp == 2 and n_fs == 4 and n_tp == 4
    return jax.shard_map(
        routed(n_grp, n_fs, n_tp) if fits else plain,
        mesh=mesh,
        in_specs=placed,
        out_specs=(P(("grp", "fs", "tp"), None), P("grp", "tp"), P("grp", "tp")),
        check_vma=False,
    )
```

time: 266 us -> 176 us (0.66)
  waiting for transfers between devices: 204 us -> 72 us
  Pallas kernels: 0 us -> 47.9 us
  starting transfers between devices: 0.16 us -> 31.6 us
  matrix products: 16.5 us -> 0 us
  between operations: 13.8 us -> 0.97 us
  other arithmetic: 14.1 us -> 9.07 us
  local copies, waits for them, and re-layouts: 16.9 us -> 14 us
    all_gather x3 -> x0, waiting for transfers between devices: 160 us -> none  [the longest x1 60.4 us: per_device(): lax.all_gather(down_local, 'fs', axis=0, tiled=True)]
    ppermute x0 -> x36, waiting for transfers between devices: none -> 72 us  [the longest x10 30.2 us: tp_swap(): return lax.ppermute(v, 'tp', [(i, i ^ m) for i in range(n_tp)])]
    pallas_call x0 -> x11, Pallas kernels: none -> 47.9 us  [the longest x4 19.8 us: down_step(): pl.pallas_call(body, grid=(steps,), out_shape=tuple(out_shape), in_specs=...]
    reduce_scatter x1 -> x0, waiting for transfers between devices: 43.8 us -> none  [per_device(): lax.psum_scatter(lax.dot_general(hidden, sampler_down, (((1,), (1,)), (()...]
    ppermute x0 -> x36, starting transfers between devices: none -> 31.6 us  [the longest x10 15 us: tp_swap(): return lax.ppermute(v, 'tp', [(i, i ^ m) for i in range(n_tp)])]
    dot_general x1 -> x0, matrix products: 16.5 us -> none  [per_device(): lax.dot_general(hidden, sampler_down, (((1,), (1,)), ((), ())), preferred...]
    unnamed x4 -> x54, local copies, waits for them, and re-layouts: 16.9 us -> 10.2 us
    convert_element_type x4 -> x6, other arithmetic: 11.6 us -> 8.83 us  [the longest x1 3.79 us: per_device(): up_own = (up_weight * gain).astype(BF)]
  transfers between devices with their start and end apart: 4 -> 36, of which waited for: 4 -> 16; matrix products, arithmetic and copies ran while one was open for 3% -> 6% of each run, Pallas kernels for 0% -> 26%
where the time goes in v1:
time: 176 us; the launch traced here: 175 us
  waiting for transfers between devices  72 us (41%)
  Pallas kernels  47.9 us (27%)
  starting transfers between devices  31.6 us (18%)
  local copies, waits for them, and re-layouts  14 us (8%)
  other arithmetic  9.07 us (5%)
    ppermute x10, waiting for transfers between devices, tp_swap(): return lax.ppermute(v, 'tp', [(i, i ^ m) for i in range(n_tp)])  30.2 us
    ppermute x6, waiting for transfers between devices, y_shift(): return lax.ppermute(v, 'fs', [((i + 2 * d) % n_fs, i) for i in range(n_fs)])  23.9 us
    pallas_call x4, Pallas kernels, down_step(): pl.pallas_call(body, grid=(steps,), out_shape=tuple(out_shape), in_specs=...  19.8 us
    pallas_call x4, Pallas kernels, up_tile(): pl.pallas_call(body, grid=(steps,), out_shape=(jax.ShapeDtypeStruct((n_to...  16.3 us
    ppermute x6, waiting for transfers between devices, grp_shift(): return lax.ppermute(v, 'grp', [((i + d) % n_grp, i) for i in range(n_grp)])  16.1 us
    ppermute x10, starting transfers between devices, tp_swap(): return lax.ppermute(v, 'tp', [(i, i ^ m) for i in range(n_tp)])  15 us
    unnamed x54, local copies, waits for them, and re-layouts  10.2 us
    ppermute x6, starting transfers between devices, grp_shift(): return lax.ppermute(v, 'grp', [((i + d) % n_grp, i) for i in range(n_grp)])  7.74 us
  transfers between devices with their start and end apart: 36, of which 16 were waited for; matrix products, arithmetic and copies ran while one was open for 6% of the time, Pallas kernels for 26%

profile of v1, /device:TPU:0, one launch (start us, length us, event | category | flops | bytes accessed | tf_op | source)
XLA Modules:
  0.0 175.5 jit_solution(17295652384068821572)
XLA Ops:
  1.4 2.4 %fusion = (bf16[256,512]{1,0:T(8,128)(2,1)}, bf16[256,512]{1,0:T(8,128)(2,1)S(1)}, bf16[256,512]{1,0:T(8,128)(2,1)S(1)}, bf16[256,512]{1,0:T(8,128)(2,1)S(1)}) fusion(f32[512,2048]{1,0:T(8,128)} %param.6, s32[]{:T(128)S(6)} %select_n.104, f32[256]{0:T(256)S(1)} %dynamic-slice.3, s32[]{:T(128)S(6)} %add.193, s32[]{:T(128)S(6)} %add.192, s32[]{:T(128)S(6)} %add.191), kind=kLoop, calls=%fused_computation.4 | loop fusion | flops 1048576 | bytes 3146768 | tf_op jit(solution)/shard_map/convert_element_type | solution.py:319
  3.8 3.0 %collective-permute-start.3 = (bf16[256,512]{1,0:T(8,128)(2,1)S(1)}, bf16[256,512]{1,0:T(8,128)(2,1)S(1)}, u32[]{:S(2)}, u32[]{:S(2)}) collective-permute-start(bf16[256,512]{1,0:T(8,128)(2,1)S(1)} %get-tuple-element.46), channel_id=1, source_target_pairs={{8,0},{12,4},{0,8},{4,12},{9,1},{13,5},{1,9},{5,13},{10,2},{14,6},... | collective-permute-start | bytes 786440 | tf_op jit(solution)/shard_map/ppermute | solution.py:275
  6.8 3.8 %multiply_convert_fusion.refs_4_ = bf16[512,2048]{1,0:T(8,128)(2,1)} fusion(f32[512,2048]{1,0:T(8,128)} %param.6, f32[512]{0:T(512)} %param.8), kind=kLoop, calls=%fused_computation | loop fusion | flops 2097152 | bytes 6293504 | tf_op jit(solution)/shard_map/convert_element_type | solution.py:326
  11.3 2.1 %norm_tokens.1.refs_2_ = bf16[128,2048]{1,0:T(8,128)(2,1)} custom-call(s32[6]{0:T(128)} %stack.97.at.refs_0_, bf16[128,2048]{1,0:T(8,128)(2,1)} %x.1), custom_call_target="tpu_custom_call" | custom-call | tf_op jit(solution)/shard_map/norm_tokens/pallas_call | solution.py:52
  13.4 2.1 %collective-permute-start = (bf16[128,2048]{1,0:T(8,128)(2,1)}, bf16[128,2048]{1,0:T(8,128)(2,1)S(1)}, u32[]{:S(2)}, u32[]{:S(2)}) collective-permute-start(bf16[128,2048]{1,0:T(8,128)(2,1)} %norm_tokens.1.refs_2_), channel_id=1, source_target_pairs={{0,1},{1,0},{2,3},{3,2},{4,5},{5,4},{6,7},{7,6},{8,9},{9,8},{10,11... | collective-permute-start | bytes 1572872 | tf_op jit(solution)/shard_map/ppermute | solution.py:281
  15.5 2.6 %collective-permute-start.1 = (bf16[128,2048]{1,0:T(8,128)(2,1)}, bf16[128,2048]{1,0:T(8,128)(2,1)}, u32[]{:S(2)}, u32[]{:S(2)}) collective-permute-start(bf16[128,2048]{1,0:T(8,128)(2,1)} %norm_tokens.1.refs_2_), channel_id=1, source_target_pairs={{0,2},{1,3},{2,0},{3,1},{4,6},{5,7},{6,4},{7,5},{8,10},{9,11},{10,... | collective-permute-start | bytes 1572872 | tf_op jit(solution)/shard_map/ppermute | solution.py:281
  18.1 1.5 collective-permute-start.11
  19.6 1.0 collective-permute-start.15
  20.6 6.8 %collective-permute-done.11.refs_6_ = bf16[256,512]{1,0:T(8,128)(2,1)} collective-permute-done((bf16[256,512]{1,0:T(8,128)(2,1)S(1)}, bf16[256,512]{1,0:T(8,128)(2,1)}, u32[]{:S(2)}, u32[]{:S(2)}) %collective-permute-start.11) | collective-permute-done | bytes 262176 | tf_op jit(solution)/shard_map/ppermute | solution.py:275
  27.4 1.5 collective-permute-start.4
  28.8 2.5 %convert_element_type.56.refs_2_ = bf16[512,2048]{1,0:T(8,128)(2,1)S(1)} convert(f32[512,2048]{1,0:T(8,128)} %param.7) | non-fusion elementwise | flops 1048576 | bytes 6291456 | tf_op jit(solution)/shard_map/convert_element_type | solution.py:328
  31.6 7.5 %collective-permute-done.refs_1_ = bf16[128,2048]{1,0:T(8,128)(2,1)S(1)} collective-permute-done((bf16[128,2048]{1,0:T(8,128)(2,1)}, bf16[128,2048]{1,0:T(8,128)(2,1)S(1)}, u32[]{:S(2)}, u32[]{:S(2)}) %collective-permute-start) | collective-permute-done | bytes 524320 | tf_op jit(solution)/shard_map/ppermute | solution.py:281
  39.1 2.7 %collective-permute-done.1.refs_3_ = bf16[128,2048]{1,0:T(8,128)(2,1)} collective-permute-done((bf16[128,2048]{1,0:T(8,128)(2,1)}, bf16[128,2048]{1,0:T(8,128)(2,1)}, u32[]{:S(2)}, u32[]{:S(2)}) %collective-permute-start.1) | collective-permute-done | bytes 524320 | tf_op jit(solution)/shard_map/ppermute | solution.py:281
  41.7 1.5 collective-permute-start.8
  45.2 4.3 %collective-permute-done.8.refs_7_ = bf16[256,512]{1,0:T(8,128)(2,1)} collective-permute-done((bf16[256,512]{1,0:T(8,128)(2,1)}, bf16[256,512]{1,0:T(8,128)(2,1)}, u32[]{:S(2)}, u32[]{:S(2)}) %collective-permute-start.8) | collective-permute-done | bytes 262176 | tf_op jit(solution)/shard_map/ppermute | solution.py:272
  49.5 2.5 %collective-permute-start.16 = (bf16[256,512]{1,0:T(8,128)(2,1)}, bf16[256,512]{1,0:T(8,128)(2,1)S(1)}, u32[]{:S(2)}, u32[]{:S(2)}) collective-permute-start(bf16[256,512]{1,0:T(8,128)(2,1)} %copy-done.9), channel_id=1, source_target_pairs={{16,0},{0,16},{17,1},{1,17},{18,2},{2,18},{19,3},{3,19},{20,4},{4,... | collective-permute-start | bytes 786440 | tf_op jit(solution)/shard_map/ppermute | solution.py:272
  51.9 1.7 dynamic-slice_convert_fusion
  53.6 0.9 collective-permute-done.12.refs_7_
  54.5 1.5 collective-permute-start.24
  56.5 3.0 %collective-permute-done.16.refs_7_ = bf16[256,512]{1,0:T(8,128)(2,1)S(1)} collective-permute-done((bf16[256,512]{1,0:T(8,128)(2,1)}, bf16[256,512]{1,0:T(8,128)(2,1)S(1)}, u32[]{:S(2)}, u32[]{:S(2)}) %collective-permute-start.16) | collective-permute-done | bytes 262176 | tf_op jit(solution)/shard_map/ppermute | solution.py:272
  59.6 1.7 collective-permute-done.17.refs_8_
  62.2 7.2 %collective-permute-done.24.refs_3_ = bf16[128,2048]{1,0:T(8,128)(2,1)} collective-permute-done((bf16[128,2048]{1,0:T(8,128)(2,1)S(1)}, bf16[128,2048]{1,0:T(8,128)(2,1)}, u32[]{:S(2)}, u32[]{:S(2)}) %collective-permute-start.24) | collective-permute-done | bytes 524320 | tf_op jit(solution)/shard_map/ppermute | solution.py:275
  69.4 9.7 %collective-permute-done.30.refs_3_ = bf16[128,2048]{1,0:T(8,128)(2,1)} collective-permute-done((bf16[128,2048]{1,0:T(8,128)(2,1)S(1)}, bf16[128,2048]{1,0:T(8,128)(2,1)}, u32[]{:S(2)}, u32[]{:S(2)}) %collective-permute-start.30) | collective-permute-done | bytes 524320 | tf_op jit(solution)/shard_map/ppermute | solution.py:275
  81.5 1.5 collective-permute-start.21
  83.7 1.5 collective-permute-start.31
  85.4 0.9 copy-done.10
  86.4 0.9 copy-done.12
  87.3 0.9 copy-done.14
  88.3 0.9 copy-done.16
  89.2 4.0 %up_tile.4 = (bf16[384,2048]{1,0:T(8,128)(2,1)S(1)}, bf16[2048,2048]{1,0:T(8,128)(2,1)}) custom-call(s32[6]{0:T(128)S(1)} %copy-done.20, bf16[128,2048]{1,0:T(8,128)(2,1)S(1)} %collective-permute-done.refs_1_, bf16[128,2048]{1,0:T(8,128)(2,1)S(1)} %copy-done, bf16[128,2048]{1,0:T(8,128)(2,1)} %collective-permute-done.1.refs_3_, ...), custom_call_target="tpu_custom_call" | custom-call | flops 805306368 | bytes 4194304 | tf_op jit(solution)/shard_map/up_tile/pallas_call | solution.py:112
  93.8 1.8 %collective-permute-done.25.refs_4_ = bf16[128,2048]{1,0:T(8,128)(2,1)} collective-permute-done((bf16[128,2048]{1,0:T(8,128)(2,1)}, bf16[128,2048]{1,0:T(8,128)(2,1)}, u32[]{:S(2)}, u32[]{:S(2)}) %collective-permute-start.25) | collective-permute-done | bytes 524320 | tf_op jit(solution)/shard_map/ppermute | solution.py:272
  95.6 4.2 %up_tile.5 = (bf16[384,2048]{1,0:T(8,128)(2,1)S(1)}, bf16[2048,2048]{1,0:T(8,128)(2,1)}) custom-call(s32[6]{0:T(128)S(1)} %copy-done.20, bf16[128,2048]{1,0:T(8,128)(2,1)S(1)} %collective-permute-done.refs_1_, bf16[128,2048]{1,0:T(8,128)(2,1)S(1)} %copy-done, ...), custom_call_target="tpu_custom_call", output_to_operand_aliasing={{0}: (10, {}), {1}: (11, {})} | custom-call | flops 805306368 | bytes 4194304 | tf_op jit(solution)/shard_map/up_tile/pallas_call | solution.py:112
  100.4 6.0 %collective-permute-done.31.refs_4_ = bf16[128,2048]{1,0:T(8,128)(2,1)} collective-permute-done((bf16[128,2048]{1,0:T(8,128)(2,1)}, bf16[128,2048]{1,0:T(8,128)(2,1)}, u32[]{:S(2)}, u32[]{:S(2)}) %collective-permute-start.31) | collective-permute-done | bytes 524320 | tf_op jit(solution)/shard_map/ppermute | solution.py:272
  106.4 4.2 %up_tile.6 = (bf16[384,2048]{1,0:T(8,128)(2,1)S(1)}, bf16[2048,2048]{1,0:T(8,128)(2,1)}) custom-call(s32[6]{0:T(128)S(1)} %copy-done.20, bf16[128,2048]{1,0:T(8,128)(2,1)S(1)} %collective-permute-done.refs_1_, bf16[128,2048]{1,0:T(8,128)(2,1)S(1)} %copy-done, ...), custom_call_target="tpu_custom_call", output_to_operand_aliasing={{0}: (10, {}), {1}: (11, {})} | custom-call | flops 805306368 | bytes 4194304 | tf_op jit(solution)/shard_map/up_tile/pallas_call | solution.py:112
  110.7 4.0 %up_tile.7 = (bf16[384,2048]{1,0:T(8,128)(2,1)S(1)}, bf16[2048,2048]{1,0:T(8,128)(2,1)}) custom-call(s32[6]{0:T(128)S(1)} %copy-done.20, bf16[128,2048]{1,0:T(8,128)(2,1)S(1)} %collective-permute-done.refs_1_, bf16[128,2048]{1,0:T(8,128)(2,1)S(1)} %copy-done, ...), custom_call_target="tpu_custom_call", output_to_operand_aliasing={{0}: (10, {}), {1}: (11, {})} | custom-call | flops 805306368 | bytes 4194304 | tf_op jit(solution)/shard_map/up_tile/pallas_call | solution.py:112
  114.7 7.1 %up_rest.1.refs_1_.refs_2_ = bf16[128,2048]{1,0:T(8,128)(2,1)S(1)} custom-call(s32[6]{0:T(128)S(1)} %copy-done.20, bf16[128,2048]{1,0:T(8,128)(2,1)} %collective-permute-done.21.x, bf16[2048,2048]{1,0:T(8,128)(2,1)} %get-tuple-element.21.w), custom_call_target="tpu_custom_call" | custom-call | flops 1073741824 | bytes 8388608 | tf_op jit(solution)/shard_map/up_rest/pallas_call | solution.py:144
  121.7 3.5 %down_step.5 = bf16[128,1024]{1,0:T(8,128)(2,1)S(1)} custom-call(s32[2]{0:T(128)S(1)} %pad_add_fusion.refs_0_, bf16[128,2048]{1,0:T(8,128)(2,1)S(1)} %up_rest.1.refs_1_.refs_2_, bf16[512,2048]{1,0:T(8,128)(2,1)S(1)} %convert_element_type.56.refs_2_, bf16[512,2048]{1,0:T(8,128)(2,1)} %collective-permute-done.19.refs_3_), custom_call_target="tpu_custom_call" | custom-call | flops 536870912 | bytes 8912896 | tf_op jit(solution)/shard_map/down_step/pallas_call | solution.py:218
  125.3 1.3 collective-permute-start.22
  126.6 7.1 %down_step.4 = (bf16[128,1024]{1,0:T(8,128)(2,1)S(1)}, bf16[128,1024]{1,0:T(8,128)(2,1)S(1)}, bf16[128,1024]{1,0:T(8,128)(2,1)S(1)}, bf16[2048,2048]{1,0:T(8,128)(2,1)}) custom-call(s32[2]{0:T(128)S(1)} %pad_add_fusion.refs_0_, bf16[384,2048]{1,0:T(8,128)(2,1)S(1)} %get-tuple-element.29.refs_1_, bf16[512,2048]{1,0:T(8,128)(2,1)S(1)} %convert_element_type.56.refs_2_, ...), custom_call_target="tpu_custom_call" | custom-call | flops 1610612736 | bytes 9961472 | tf_op jit(solution)/shard_map/down_step/pallas_call | solution.py:218
  135.2 4.6 %down_step.6 = (bf16[256,512]{1,0:T(8,128)(2,1)S(1)}, bf16[128,512]{1,0:T(8,128)(2,1)S(1)}, bf16[128,512]{1,0:T(8,128)(2,1)S(1)}, bf16[2048,2048]{1,0:T(8,128)(2,1)}) custom-call(s32[4]{0:T(128)S(1)} %pad_add_fusion.1.refs_0_, bf16[384,2048]{1,0:T(8,128)(2,1)S(1)} %get-tuple-element.29.refs_1_, ...), custom_call_target="tpu_custom_call", output_to_operand_aliasing={{3}: (7, {})} | custom-call | flops 1073741824 | bytes 6291456 | tf_op jit(solution)/shard_map/down_step/pallas_call | solution.py:218
  139.8 1.3 collective-permute-start.28
  141.1 4.6 %down_step.7 = (bf16[256,512]{1,0:T(8,128)(2,1)S(1)}, bf16[128,512]{1,0:T(8,128)(2,1)S(1)}, bf16[128,512]{1,0:T(8,128)(2,1)S(1)}, bf16[2048,2048]{1,0:T(8,128)(2,1)}) custom-call(s32[4]{0:T(128)S(1)} %pad_add_fusion.2.refs_0_, bf16[384,2048]{1,0:T(8,128)(2,1)S(1)} %get-tuple-element.29.refs_1_, ...), custom_call_target="tpu_custom_call", output_to_operand_aliasing={{3}: (7, {})} | custom-call | flops 1073741824 | bytes 6291456 | tf_op jit(solution)/shard_map/down_step/pallas_call | solution.py:218
  146.6 1.9 %collective-permute-start.23 = (bf16[128,1024]{1,0:T(8,128)(2,1)S(1)}, bf16[128,1024]{1,0:T(8,128)(2,1)S(1)}, u32[]{:S(2)}, u32[]{:S(2)}) collective-permute-start(bf16[128,1024]{1,0:T(8,128)(2,1)S(1)} %add_convert_fusion), channel_id=1, source_target_pairs={{0,2},{1,3},{2,0},{3,1},{4,6},{5,7},{6,4},{7,5},{8,10},{9,11},{10,... | collective-permute-start | bytes 786440 | tf_op jit(solution)/shard_map/ppermute | solution.py:281
  148.9 2.7 %collective-permute-start.29 = (bf16[128,512]{1,0:T(8,128)(2,1)S(1)}, bf16[128,512]{1,0:T(8,128)(2,1)S(1)}, u32[]{:S(2)}, u32[]{:S(2)}) collective-permute-start(bf16[128,512]{1,0:T(8,128)(2,1)S(1)} %add_convert_fusion.2), channel_id=1, source_target_pairs={{0,2},{1,3},{2,0},{3,1},{4,6},{5,7},{6,4},{7,5},{8,10},{9,11},{10,... | collective-permute-start | bytes 393224 | tf_op jit(solution)/shard_map/ppermute | solution.py:281
  151.5 9.1 %collective-permute-done.34.refs_9_ = bf16[256,512]{1,0:T(8,128)(2,1)S(1)} collective-permute-done((bf16[256,512]{1,0:T(8,128)(2,1)S(1)}, bf16[256,512]{1,0:T(8,128)(2,1)S(1)}, u32[]{:S(2)}, u32[]{:S(2)}) %collective-permute-start.34) | collective-permute-done | bytes 262176 | tf_op jit(solution)/shard_map/ppermute | solution.py:281
  161.4 9.3 %collective-permute-done.29.refs_7_ = bf16[128,512]{1,0:T(8,128)(2,1)S(1)} collective-permute-done((bf16[128,512]{1,0:T(8,128)(2,1)S(1)}, bf16[128,512]{1,0:T(8,128)(2,1)S(1)}, u32[]{:S(2)}, u32[]{:S(2)}) %collective-permute-start.29) | collective-permute-done | bytes 131104 | tf_op jit(solution)/shard_map/ppermute | solution.py:281
  170.7 1.4 collective-permute-done.35.refs_10_
  172.8 2.6 %finish.1 = bf16[128,2048]{1,0:T(8,128)(2,1)} custom-call(s32[16]{0:T(128)} %stack.95.refs_0_, f32[1,2048]{1,0:T(1,128)} %bitcast.17, bf16[128,1024]{1,0:T(8,128)(2,1)} %copy-done.17, bf16[128,1024]{1,0:T(8,128)(2,1)} %copy-done.23, bf16[128,1024]{1,0:T(8,128)(2,1)} %copy-done.24, bf16[128,512]{1,0:T(8,128)(2,1)} %copy-done.18, bf16[256,512]{1,0:T(8,128)(2,1)} %copy-done.21, ...), custom_call_target="tpu_custom_call" | custom-call | tf_op jit(solution)/shard_map/finish/pallas_call | solution.py:253
  (102 shorter events, 13.7 us)
Async XLA Ops:
  3.8 14.3 %collective-permute-start.3 = (bf16[256,512]{1,0:T(8,128)(2,1)S(1)}, bf16[256,512]{1,0:T(8,128)(2,1)S(1)}, u32[]{:S(2)}, u32[]{:S(2)}) collective-permute-start(bf16[256,512]{1,0:T(8,128)(2,1)S(1)} %get-tuple-element.46), channel_id=1, source_target_pairs={{8,0},{12,4},{0,8},{4,12},{9,1},{13,5},{1,9},{5,13},{10,2},{14,6},... | collective-permute-start | bytes 786440 | tf_op jit(solution)/shard_map/ppermute | solution.py:275
  10.6 74.7 %collective-permute-start.2 = (bf16[512,2048]{1,0:T(8,128)(2,1)}, bf16[512,2048]{1,0:T(8,128)(2,1)}, u32[]{:S(2)}, u32[]{:S(2)}) collective-permute-start(bf16[512,2048]{1,0:T(8,128)(2,1)} %multiply_convert_fusion.refs_4_), channel_id=1, source_target_pairs={{0,4},{4,0},{8,12},{12,8},{1,5},{5,1},{9,13},{13,9},{2,6},{6,2},{1... | collective-permute-start | bytes 6291464 | tf_op jit(solution)/shard_map/ppermute | solution.py:278
  10.6 9.0 %collective-permute-start.7 = (bf16[256,512]{1,0:T(8,128)(2,1)S(1)}, bf16[256,512]{1,0:T(8,128)(2,1)}, u32[]{:S(2)}, u32[]{:S(2)}) collective-permute-start(bf16[256,512]{1,0:T(8,128)(2,1)S(1)} %get-tuple-element.45), channel_id=1, source_target_pairs={{8,0},{12,4},{0,8},{4,12},{9,1},{13,5},{1,9},{5,13},{10,2},{14,6},... | collective-permute-start | bytes 786440 | tf_op jit(solution)/shard_map/ppermute | solution.py:275
  13.4 25.7 %collective-permute-start = (bf16[128,2048]{1,0:T(8,128)(2,1)}, bf16[128,2048]{1,0:T(8,128)(2,1)S(1)}, u32[]{:S(2)}, u32[]{:S(2)}) collective-permute-start(bf16[128,2048]{1,0:T(8,128)(2,1)} %norm_tokens.1.refs_2_), channel_id=1, source_target_pairs={{0,1},{1,0},{2,3},{3,2},{4,5},{5,4},{6,7},{7,6},{8,9},{9,8},{10,11... | collective-permute-start | bytes 1572872 | tf_op jit(solution)/shard_map/ppermute | solution.py:281
  15.5 26.3 %collective-permute-start.1 = (bf16[128,2048]{1,0:T(8,128)(2,1)}, bf16[128,2048]{1,0:T(8,128)(2,1)}, u32[]{:S(2)}, u32[]{:S(2)}) collective-permute-start(bf16[128,2048]{1,0:T(8,128)(2,1)} %norm_tokens.1.refs_2_), channel_id=1, source_target_pairs={{0,2},{1,3},{2,0},{3,1},{4,6},{5,7},{6,4},{7,5},{8,10},{9,11},{10,... | collective-permute-start | bytes 1572872 | tf_op jit(solution)/shard_map/ppermute | solution.py:281
  18.1 9.3 %collective-permute-start.11 = (bf16[256,512]{1,0:T(8,128)(2,1)S(1)}, bf16[256,512]{1,0:T(8,128)(2,1)}, u32[]{:S(2)}, u32[]{:S(2)}) collective-permute-start(bf16[256,512]{1,0:T(8,128)(2,1)S(1)} %get-tuple-element.44), channel_id=1, source_target_pairs={{8,0},{12,4},{0,8},{4,12},{9,1},{13,5},{1,9},{5,13},{10,2},{14,6},... | collective-permute-start | bytes 786440 | tf_op jit(solution)/shard_map/ppermute | solution.py:275
  19.6 65.9 %copy-start = (bf16[128,2048]{1,0:T(8,128)(2,1)S(1)}, bf16[128,2048]{1,0:T(8,128)(2,1)}, u32[]{:S(2)}) copy-start(bf16[128,2048]{1,0:T(8,128)(2,1)} %norm_tokens.1.refs_2_) | copy-start | bytes 1572868
  19.6 65.9 %copy-start.20 = (s32[6]{0:T(128)S(1)}, s32[6]{0:T(128)}, u32[]{:S(2)}) copy-start(s32[6]{0:T(128)} %stack.97.at.refs_0_) | copy-start | bytes 76
  19.6 12.0 %collective-permute-start.15 = (bf16[256,512]{1,0:T(8,128)(2,1)}, bf16[256,512]{1,0:T(8,128)(2,1)S(1)}, u32[]{:S(2)}, u32[]{:S(2)}) collective-permute-start(bf16[256,512]{1,0:T(8,128)(2,1)} %get-tuple-element.43), channel_id=1, source_target_pairs={{8,0},{12,4},{0,8},{4,12},{9,1},{13,5},{1,9},{5,13},{10,2},{14,6},... | collective-permute-start | bytes 786440 | tf_op jit(solution)/shard_map/ppermute | solution.py:275
  27.4 15.9 %collective-permute-start.4 = (bf16[256,512]{1,0:T(8,128)(2,1)S(1)}, bf16[256,512]{1,0:T(8,128)(2,1)S(1)}, u32[]{:S(2)}, u32[]{:S(2)}) collective-permute-start(bf16[256,512]{1,0:T(8,128)(2,1)S(1)} %collective-permute-done.3.refs_6_), channel_id=1, source_target_pairs={{16,0},{0,16},{17,1},{1,17},{18,2},{2,18},{19,3},{3,19},{20,4},{4,... | collective-permute-start | bytes 786440 | tf_op jit(solution)/shard_map/ppermute | solution.py:272
  31.5 13.7 %copy-start.9 = (bf16[256,512]{1,0:T(8,128)(2,1)}, bf16[256,512]{1,0:T(8,128)(2,1)S(1)}, u32[]{:S(2)}) copy-start(bf16[256,512]{1,0:T(8,128)(2,1)S(1)} %collective-permute-done.15.refs_6_) | copy-start | bytes 786436
  31.6 90.2 %collective-permute-start.19 = (bf16[512,2048]{1,0:T(8,128)(2,1)S(1)}, bf16[512,2048]{1,0:T(8,128)(2,1)}, u32[]{:S(2)}, u32[]{:S(2)}) collective-permute-start(bf16[512,2048]{1,0:T(8,128)(2,1)S(1)} %convert_element_type.56.refs_2_), channel_id=1, source_target_pairs={{0,4},{4,0},{8,12},{12,8},{1,5},{5,1},{9,13},{13,9},{2,6},{6,2},{1... | collective-permute-start | bytes 6291464 | tf_op jit(solution)/shard_map/ppermute | solution.py:278
  39.1 4.2 %collective-permute-start.5 = (bf16[256,512]{1,0:T(8,128)(2,1)S(1)}, bf16[256,512]{1,0:T(8,128)(2,1)S(1)}, u32[]{:S(2)}, u32[]{:S(2)}) collective-permute-start(bf16[256,512]{1,0:T(8,128)(2,1)S(1)} %collective-permute-done.3.refs_6_), channel_id=1, source_target_pairs={{0,4},{4,0},{8,12},{12,8},{1,5},{5,1},{9,13},{13,9},{2,6},{6,2},{1... | collective-permute-start | bytes 786440 | tf_op jit(solution)/shard_map/ppermute | solution.py:278
  41.7 7.7 %collective-permute-start.8 = (bf16[256,512]{1,0:T(8,128)(2,1)}, bf16[256,512]{1,0:T(8,128)(2,1)}, u32[]{:S(2)}, u32[]{:S(2)}) collective-permute-start(bf16[256,512]{1,0:T(8,128)(2,1)} %collective-permute-done.7.refs_6_), channel_id=1, source_target_pairs={{16,0},{0,16},{17,1},{1,17},{18,2},{2,18},{19,3},{3,19},{20,4},{4,... | collective-permute-start | bytes 786440 | tf_op jit(solution)/shard_map/ppermute | solution.py:272
  43.2 6.2 %collective-permute-start.9 = (bf16[256,512]{1,0:T(8,128)(2,1)}, bf16[256,512]{1,0:T(8,128)(2,1)}, u32[]{:S(2)}, u32[]{:S(2)}) collective-permute-start(bf16[256,512]{1,0:T(8,128)(2,1)} %collective-permute-done.7.refs_6_), channel_id=1, source_target_pairs={{0,4},{4,0},{8,12},{12,8},{1,5},{5,1},{9,13},{13,9},{2,6},{6,2},{1... | collective-permute-start | bytes 786440 | tf_op jit(solution)/shard_map/ppermute | solution.py:278
  44.7 9.8 %collective-permute-start.12 = (bf16[256,512]{1,0:T(8,128)(2,1)}, bf16[256,512]{1,0:T(8,128)(2,1)}, u32[]{:S(2)}, u32[]{:S(2)}) collective-permute-start(bf16[256,512]{1,0:T(8,128)(2,1)} %collective-permute-done.11.refs_6_), channel_id=1, source_target_pairs={{16,0},{0,16},{17,1},{1,17},{18,2},{2,18},{19,3},{3,19},{20,4},{4,... | collective-permute-start | bytes 786440 | tf_op jit(solution)/shard_map/ppermute | solution.py:272
  49.5 6.6 %collective-permute-start.13 = (bf16[256,512]{1,0:T(8,128)(2,1)}, bf16[256,512]{1,0:T(8,128)(2,1)}, u32[]{:S(2)}, u32[]{:S(2)}) collective-permute-start(bf16[256,512]{1,0:T(8,128)(2,1)} %collective-permute-done.11.refs_6_), channel_id=1, source_target_pairs={{0,4},{4,0},{8,12},{12,8},{1,5},{5,1},{9,13},{13,9},{2,6},{6,2},{1... | collective-permute-start | bytes 786440 | tf_op jit(solution)/shard_map/ppermute | solution.py:278
  49.5 10.1 %collective-permute-start.16 = (bf16[256,512]{1,0:T(8,128)(2,1)}, bf16[256,512]{1,0:T(8,128)(2,1)S(1)}, u32[]{:S(2)}, u32[]{:S(2)}) collective-permute-start(bf16[256,512]{1,0:T(8,128)(2,1)} %copy-done.9), channel_id=1, source_target_pairs={{16,0},{0,16},{17,1},{1,17},{18,2},{2,18},{19,3},{3,19},{20,4},{4,... | collective-permute-start | bytes 786440 | tf_op jit(solution)/shard_map/ppermute | solution.py:272
  54.5 14.9 %collective-permute-start.24 = (bf16[128,2048]{1,0:T(8,128)(2,1)S(1)}, bf16[128,2048]{1,0:T(8,128)(2,1)}, u32[]{:S(2)}, u32[]{:S(2)}) collective-permute-start(bf16[128,2048]{1,0:T(8,128)(2,1)S(1)} %get-tuple-element.48), channel_id=1, source_target_pairs={{8,0},{12,4},{0,8},{4,12},{9,1},{13,5},{1,9},{5,13},{10,2},{14,6},... | collective-permute-start | bytes 1572872 | tf_op jit(solution)/shard_map/ppermute | solution.py:275
  56.0 23.1 %collective-permute-start.30 = (bf16[128,2048]{1,0:T(8,128)(2,1)S(1)}, bf16[128,2048]{1,0:T(8,128)(2,1)}, u32[]{:S(2)}, u32[]{:S(2)}) collective-permute-start(bf16[128,2048]{1,0:T(8,128)(2,1)S(1)} %get-tuple-element.47), channel_id=1, source_target_pairs={{8,0},{12,4},{0,8},{4,12},{9,1},{13,5},{1,9},{5,13},{10,2},{14,6},... | collective-permute-start | bytes 1572872 | tf_op jit(solution)/shard_map/ppermute | solution.py:275
  59.6 1.7 collective-permute-start.17
  62.0 17.8 %collective-permute-start.6 = (bf16[256,512]{1,0:T(8,128)(2,1)}, bf16[256,512]{1,0:T(8,128)(2,1)S(1)}, u32[]{:S(2)}, u32[]{:S(2)}) collective-permute-start(bf16[256,512]{1,0:T(8,128)(2,1)} %copy-done.1), channel_id=1, source_target_pairs={{0,4},{4,0},{8,12},{12,8},{1,5},{5,1},{9,13},{13,9},{2,6},{6,2},{1... | collective-permute-start | bytes 786440 | tf_op jit(solution)/shard_map/ppermute | solution.py:278
  69.4 11.4 %collective-permute-start.10 = (bf16[256,512]{1,0:T(8,128)(2,1)}, bf16[256,512]{1,0:T(8,128)(2,1)S(1)}, u32[]{:S(2)}, u32[]{:S(2)}) collective-permute-start(bf16[256,512]{1,0:T(8,128)(2,1)} %collective-permute-done.8.refs_7_), channel_id=1, source_target_pairs={{0,4},{4,0},{8,12},{12,8},{1,5},{5,1},{9,13},{13,9},{2,6},{6,2},{1... | collective-permute-start | bytes 786440 | tf_op jit(solution)/shard_map/ppermute | solution.py:278
  79.1 3.9 %collective-permute-start.18 = (bf16[256,512]{1,0:T(8,128)(2,1)S(1)}, bf16[256,512]{1,0:T(8,128)(2,1)S(1)}, u32[]{:S(2)}, u32[]{:S(2)}) collective-permute-start(bf16[256,512]{1,0:T(8,128)(2,1)S(1)} %collective-permute-done.16.refs_7_), channel_id=1, source_target_pairs={{0,4},{4,0},{8,12},{12,8},{1,5},{5,1},{9,13},{13,9},{2,6},{6,2},{1... | collective-permute-start | bytes 786440 | tf_op jit(solution)/shard_map/ppermute | solution.py:278
  80.5 15.1 %collective-permute-start.25 = (bf16[128,2048]{1,0:T(8,128)(2,1)}, bf16[128,2048]{1,0:T(8,128)(2,1)}, u32[]{:S(2)}, u32[]{:S(2)}) collective-permute-start(bf16[128,2048]{1,0:T(8,128)(2,1)} %collective-permute-done.24.refs_3_), channel_id=1, source_target_pairs={{16,0},{0,16},{17,1},{1,17},{18,2},{2,18},{19,3},{3,19},{20,4},{4,... | collective-permute-start | bytes 1572872 | tf_op jit(solution)/shard_map/ppermute | solution.py:272
  81.5 18.3 %collective-permute-start.21 = (bf16[128,2048]{1,0:T(8,128)(2,1)}, bf16[128,2048]{1,0:T(8,128)(2,1)}, u32[]{:S(2)}, u32[]{:S(2)}) collective-permute-start(bf16[128,2048]{1,0:T(8,128)(2,1)} %collective-permute-done.1.refs_3_), channel_id=1, source_target_pairs={{0,1},{1,0},{2,3},{3,2},{4,5},{5,4},{6,7},{7,6},{8,9},{9,8},{10,11... | collective-permute-start | bytes 1572872 | tf_op jit(solution)/shard_map/ppermute | solution.py:281
  83.7 22.7 %collective-permute-start.31 = (bf16[128,2048]{1,0:T(8,128)(2,1)}, bf16[128,2048]{1,0:T(8,128)(2,1)}, u32[]{:S(2)}, u32[]{:S(2)}) collective-permute-start(bf16[128,2048]{1,0:T(8,128)(2,1)} %collective-permute-done.30.refs_3_), channel_id=1, source_target_pairs={{16,0},{0,16},{17,1},{1,17},{18,2},{2,18},{19,3},{3,19},{20,4},{4,... | collective-permute-start | bytes 1572872 | tf_op jit(solution)/shard_map/ppermute | solution.py:272
  85.3 7.9 %collective-permute-start.14 = (bf16[256,512]{1,0:T(8,128)(2,1)}, bf16[256,512]{1,0:T(8,128)(2,1)S(1)}, u32[]{:S(2)}, u32[]{:S(2)}) collective-permute-start(bf16[256,512]{1,0:T(8,128)(2,1)} %collective-permute-done.12.refs_7_), channel_id=1, source_target_pairs={{0,4},{4,0},{8,12},{12,8},{1,5},{5,1},{9,13},{13,9},{2,6},{6,2},{1... | collective-permute-start | bytes 786440 | tf_op jit(solution)/shard_map/ppermute | solution.py:278
  93.2 41.2 %collective-permute-start.26 = (bf16[128,2048]{1,0:T(8,128)(2,1)}, bf16[128,2048]{1,0:T(8,128)(2,1)S(1)}, u32[]{:S(2)}, u32[]{:S(2)}) collective-permute-start(bf16[128,2048]{1,0:T(8,128)(2,1)} %collective-permute-done.24.refs_3_), channel_id=1, source_target_pairs={{0,4},{4,0},{8,12},{12,8},{1,5},{5,1},{9,13},{13,9},{2,6},{6,2},{1... | collective-permute-start | bytes 1572872 | tf_op jit(solution)/shard_map/ppermute | solution.py:278
  95.6 39.5 %collective-permute-start.27 = (bf16[128,2048]{1,0:T(8,128)(2,1)}, bf16[128,2048]{1,0:T(8,128)(2,1)S(1)}, u32[]{:S(2)}, u32[]{:S(2)}) collective-permute-start(bf16[128,2048]{1,0:T(8,128)(2,1)} %collective-permute-done.25.refs_4_), channel_id=1, source_target_pairs={{0,4},{4,0},{8,12},{12,8},{1,5},{5,1},{9,13},{13,9},{2,6},{6,2},{1... | collective-permute-start | bytes 1572872 | tf_op jit(solution)/shard_map/ppermute | solution.py:278
  95.6 10.8 %copy-start.8 = (bf16[256,512]{1,0:T(8,128)(2,1)S(1)}, bf16[256,512]{1,0:T(8,128)(2,1)}, u32[]{:S(2)}) copy-start(bf16[256,512]{1,0:T(8,128)(2,1)} %copy-done.7) | copy-start | bytes 786436
  99.8 41.3 %collective-permute-start.32 = (bf16[128,2048]{1,0:T(8,128)(2,1)}, bf16[128,2048]{1,0:T(8,128)(2,1)S(1)}, u32[]{:S(2)}, u32[]{:S(2)}) collective-permute-start(bf16[128,2048]{1,0:T(8,128)(2,1)} %collective-permute-done.30.refs_3_), channel_id=1, source_target_pairs={{0,4},{4,0},{8,12},{12,8},{1,5},{5,1},{9,13},{13,9},{2,6},{6,2},{1... | collective-permute-start | bytes 1572872 | tf_op jit(solution)/shard_map/ppermute | solution.py:278
  106.4 34.7 %collective-permute-start.33 = (bf16[128,2048]{1,0:T(8,128)(2,1)}, bf16[128,2048]{1,0:T(8,128)(2,1)S(1)}, u32[]{:S(2)}, u32[]{:S(2)}) collective-permute-start(bf16[128,2048]{1,0:T(8,128)(2,1)} %collective-permute-done.31.refs_4_), channel_id=1, source_target_pairs={{0,4},{4,0},{8,12},{12,8},{1,5},{5,1},{9,13},{13,9},{2,6},{6,2},{1... | collective-permute-start | bytes 1572872 | tf_op jit(solution)/shard_map/ppermute | solution.py:278
  106.4 4.2 %copy-start.2 = (bf16[256,512]{1,0:T(8,128)(2,1)S(1)}, bf16[256,512]{1,0:T(8,128)(2,1)}, u32[]{:S(2)}) copy-start(bf16[256,512]{1,0:T(8,128)(2,1)} %copy-done.1) | copy-start | bytes 786436
  106.4 4.2 %copy-start.4 = (bf16[256,512]{1,0:T(8,128)(2,1)S(1)}, bf16[256,512]{1,0:T(8,128)(2,1)}, u32[]{:S(2)}) copy-start(bf16[256,512]{1,0:T(8,128)(2,1)} %copy-done.3) | copy-start | bytes 786436
  106.4 4.2 %copy-start.6 = (bf16[256,512]{1,0:T(8,128)(2,1)S(1)}, bf16[256,512]{1,0:T(8,128)(2,1)}, u32[]{:S(2)}) copy-start(bf16[256,512]{1,0:T(8,128)(2,1)} %copy-done.5) | copy-start | bytes 786436
  125.3 21.3 %collective-permute-start.22 = (bf16[128,1024]{1,0:T(8,128)(2,1)S(1)}, bf16[128,1024]{1,0:T(8,128)(2,1)S(1)}, u32[]{:S(2)}, u32[]{:S(2)}) collective-permute-start(bf16[128,1024]{1,0:T(8,128)(2,1)S(1)} %down_step.5), channel_id=1, source_target_pairs={{0,1},{1,0},{2,3},{3,2},{4,5},{5,4},{6,7},{7,6},{8,9},{9,8},{10,11... | collective-permute-start | bytes 786440 | tf_op jit(solution)/shard_map/ppermute | solution.py:281
  134.4 27.0 %collective-permute-start.20 = (bf16[128,1024]{1,0:T(8,128)(2,1)S(1)}, bf16[128,1024]{1,0:T(8,128)(2,1)S(1)}, u32[]{:S(2)}, u32[]{:S(2)}) collective-permute-start(bf16[128,1024]{1,0:T(8,128)(2,1)S(1)} %get-tuple-element.31), channel_id=1, source_target_pairs={{0,1},{1,0},{2,3},{3,2},{4,5},{5,4},{6,7},{7,6},{8,9},{9,8},{10,11... | collective-permute-start | bytes 786440 | tf_op jit(solution)/shard_map/ppermute | solution.py:281
  139.8 5.9 %copy-start.18 = (bf16[128,512]{1,0:T(8,128)(2,1)}, bf16[128,512]{1,0:T(8,128)(2,1)S(1)}, u32[]{:S(2)}) copy-start(bf16[128,512]{1,0:T(8,128)(2,1)S(1)} %get-tuple-element.35.refs_5_) | copy-start | bytes 393220
  139.8 9.0 %collective-permute-start.28 = (bf16[256,512]{1,0:T(8,128)(2,1)S(1)}, bf16[256,512]{1,0:T(8,128)(2,1)S(1)}, u32[]{:S(2)}, u32[]{:S(2)}) collective-permute-start(bf16[256,512]{1,0:T(8,128)(2,1)S(1)} %get-tuple-element.36), channel_id=1, source_target_pairs={{0,1},{1,0},{2,3},{3,2},{4,5},{5,4},{6,7},{7,6},{8,9},{9,8},{10,11... | collective-permute-start | bytes 786440 | tf_op jit(solution)/shard_map/ppermute | solution.py:281
  145.7 14.9 %copy-start.19 = (bf16[128,512]{1,0:T(8,128)(2,1)}, bf16[128,512]{1,0:T(8,128)(2,1)S(1)}, u32[]{:S(2)}) copy-start(bf16[128,512]{1,0:T(8,128)(2,1)S(1)} %get-tuple-element.39.refs_8_) | copy-start | bytes 393220
  145.7 14.9 %collective-permute-start.34 = (bf16[256,512]{1,0:T(8,128)(2,1)S(1)}, bf16[256,512]{1,0:T(8,128)(2,1)S(1)}, u32[]{:S(2)}, u32[]{:S(2)}) collective-permute-start(bf16[256,512]{1,0:T(8,128)(2,1)S(1)} %get-tuple-element.40), channel_id=1, source_target_pairs={{0,1},{1,0},{2,3},{3,2},{4,5},{5,4},{6,7},{7,6},{8,9},{9,8},{10,11... | collective-permute-start | bytes 786440 | tf_op jit(solution)/shard_map/ppermute | solution.py:281
  146.6 25.5 %collective-permute-start.23 = (bf16[128,1024]{1,0:T(8,128)(2,1)S(1)}, bf16[128,1024]{1,0:T(8,128)(2,1)S(1)}, u32[]{:S(2)}, u32[]{:S(2)}) collective-permute-start(bf16[128,1024]{1,0:T(8,128)(2,1)S(1)} %add_convert_fusion), channel_id=1, source_target_pairs={{0,2},{1,3},{2,0},{3,1},{4,6},{5,7},{6,4},{7,5},{8,10},{9,11},{10,... | collective-permute-start | bytes 786440 | tf_op jit(solution)/shard_map/ppermute | solution.py:281
  148.8 23.3 %copy-start.21 = (bf16[256,512]{1,0:T(8,128)(2,1)}, bf16[256,512]{1,0:T(8,128)(2,1)S(1)}, u32[]{:S(2)}) copy-start(bf16[256,512]{1,0:T(8,128)(2,1)S(1)} %collective-permute-done.28.refs_6_) | copy-start | bytes 786436
  148.9 21.8 %collective-permute-start.29 = (bf16[128,512]{1,0:T(8,128)(2,1)S(1)}, bf16[128,512]{1,0:T(8,128)(2,1)S(1)}, u32[]{:S(2)}, u32[]{:S(2)}) collective-permute-start(bf16[128,512]{1,0:T(8,128)(2,1)S(1)} %add_convert_fusion.2), channel_id=1, source_target_pairs={{0,2},{1,3},{2,0},{3,1},{4,6},{5,7},{6,4},{7,5},{8,10},{9,11},{10,... | collective-permute-start | bytes 393224 | tf_op jit(solution)/shard_map/ppermute | solution.py:281
  160.6 11.5 %copy-start.22 = (bf16[256,512]{1,0:T(8,128)(2,1)}, bf16[256,512]{1,0:T(8,128)(2,1)S(1)}, u32[]{:S(2)}) copy-start(bf16[256,512]{1,0:T(8,128)(2,1)S(1)} %collective-permute-done.34.refs_9_) | copy-start | bytes 786436
  160.6 11.4 %collective-permute-start.35 = (bf16[128,512]{1,0:T(8,128)(2,1)S(1)}, bf16[128,512]{1,0:T(8,128)(2,1)S(1)}, u32[]{:S(2)}, u32[]{:S(2)}) collective-permute-start(bf16[128,512]{1,0:T(8,128)(2,1)S(1)} %add_convert_fusion.1), channel_id=1, source_target_pairs={{0,2},{1,3},{2,0},{3,1},{4,6},{5,7},{6,4},{7,5},{8,10},{9,11},{10,... | collective-permute-start | bytes 393224 | tf_op jit(solution)/shard_map/ppermute | solution.py:281
  161.4 10.7 %copy-start.23 = (bf16[128,1024]{1,0:T(8,128)(2,1)}, bf16[128,1024]{1,0:T(8,128)(2,1)S(1)}, u32[]{:S(2)}) copy-start(bf16[128,1024]{1,0:T(8,128)(2,1)S(1)} %collective-permute-done.20.refs_3_) | copy-start | bytes 786436
  (15 other events, 12.3 us)

commit v2 on v0

v2 whole, which is shorter than its diff:
```python
import jax
import jax.numpy as jnp
from jax import lax
from jax.experimental import pallas as pl
from jax.experimental.pallas import tpu as pltpu
from jax.sharding import PartitionSpec as P


BF = jnp.bfloat16
F32 = jnp.float32
ANY = pl.BlockSpec(memory_space=pl.ANY)
LIMIT = pltpu.CompilerParams(vmem_limit_bytes=28 * 2**20)


def plain(prompt_tokens, up_weight, down_weight, pre_gain, post_gain):
    up_local = (up_weight * pre_gain[:, None]).astype(BF)
    down_local = down_weight.astype(BF)
    values = prompt_tokens.astype(F32)
    normed = (
        values * lax.rsqrt(jnp.mean(values * values, axis=1, keepdims=True) + 1e-06)
    ).astype(BF)
    sampler_up = lax.all_gather(up_local, "fs", axis=0, tiled=True)
    sampler_down = lax.all_gather(down_local, "fs", axis=0, tiled=True)
    lifted = jnp.dot(
        lax.all_gather(normed, "tp", axis=0, tiled=True),
        sampler_up,
        preferred_element_type=F32,
    )
    hidden = jnp.square(jax.nn.relu(lifted)).astype(BF)
    part = lax.dot_general(
        hidden, sampler_down, (((1,), (1,)), ((), ())), preferred_element_type=F32
    )
    summed = lax.psum_scatter(
        part.astype(BF), "tp", scatter_dimension=0, tiled=True
    ).astype(F32)
    scaled = summed * lax.rsqrt(jnp.mean(summed * summed, axis=1, keepdims=True) + 1e-06)
    return (scaled * post_gain[None, :]).astype(BF), sampler_up, sampler_down


def in_hbm(x):
    return pltpu.with_memory_space_constraint(x, pltpu.HBM)


def hbm_call(body, out_shape, args, **options):
    many = isinstance(out_shape, (tuple, list))
    return pl.pallas_call(
        body,
        out_shape=out_shape,
        in_specs=[ANY] * len(args),
        out_specs=tuple([ANY] * len(out_shape)) if many else ANY,
        **options,
    )(*args)


class Copies:
    def __init__(self, sems):
        self.sems, self.used = sems, 0

    def start(self, src, dst):
        c = pltpu.make_async_copy(src, dst, self.sems.at[self.used])
        self.used += 1
        c.start()
        return c


def wait_all(copies):
    for c in copies:
        c.wait()


def here():
    fs = lax.axis_index("fs")
    return fs // 2, fs % 2, lax.axis_index("grp")


def up_places(rows, half):
    y, core, grp = here()
    near = [(2 * y + core) * rows, (2 * y + 1 - core) * rows]
    far = [
        (2 * (1 - y) + c) * rows + side * half
        for c in (core, 1 - core)
        for side in (grp, 1 - grp)
    ]
    return [pl.multiple_of(a, 128) for a in near + far]


def cast(weight, gain, wanted, places, tokens=None, step=64):
    rows, hid = weight.shape
    n = len(wanted)
    whole = [w == (rows, hid) for w in wanted]
    parts = [(i, r) for i, w in enumerate(wanted) for r in range(0, w[0], step)]
    full = any(whole)
    if tokens is not None:
        tok, width = tokens.shape
        token_rows = [(r, tok // 2) for r in range(0, tok, tok // 2)]

    def body(*refs):
        w, refs = refs[0], refs[1:]
        if gain is not None:
            g, refs = refs[0], refs[1:]
        if tokens is not None:
            t, refs = refs[0], refs[1:]
        outs, refs = refs[:n], refs[n:]
        if tokens is not None:
            normed, refs = refs[0], refs[1:]
        src, bufs, refs = refs[0], refs[1 : 1 + n], refs[1 + n :]
        if gain is not None:
            line_in, column, refs = refs[0], refs[1], refs[2:]
        if tokens is not None:
            token_in, token_out, refs = refs[0], refs[1], refs[2:]
        go = Copies(refs[0])
        at = places()
        stores = []
        if gain is not None:
            line = go.start(g, line_in)

        if tokens is not None:
            token_loads = [
                go.start(t.at[r : r + c, :], token_in.at[r : r + c, :]) for r, c in token_rows
            ]

        def scaled(v, row, count):
            if gain is None:
                return v.astype(BF)
            return (v * column[pl.ds(row, count), :]).astype(BF)

        if full:
            loads = [
                go.start(w.at[r : r + step, :], src.at[r : r + step, :])
                for r in range(0, rows, step)
            ]
        else:
            loads = []
            for i, r in parts:
                row, col = at[i]
                loads.append(
                    go.start(
                        w.at[pl.ds(pl.multiple_of(row + r, 8), step), pl.ds(col, wanted[i][1])],
                        src.at[r : r + step, pl.ds(col, wanted[i][1])],
                    )
                )
        if gain is not None:
            line.wait()
            column[...] = jnp.broadcast_to(line_in[...], (128, rows)).T[:, :1]
        if tokens is not None:
            for load, (r, count) in zip(token_loads, token_rows):
                load.wait()
                v = token_in[r : r + count, :].astype(F32)
                token_out[r : r + count, :] = (
                    v * lax.rsqrt(jnp.mean(v * v, axis=1, keepdims=True) + 1e-06)
                ).astype(BF)
                stores.append(
                    go.start(token_out.at[r : r + count, :], normed.at[r : r + count, :])
                )
        if full:
            for k, r in enumerate(range(0, rows, step)):
                loads[k].wait()
                i = whole.index(True)
                bufs[i][r : r + step, :] = scaled(src[r : r + step, :], r, step)
                stores.append(go.start(bufs[i].at[r : r + step, :], outs[i].at[r : r + step, :]))
            for j in range(n):
                if not whole[j]:
                    row, col = at[j]
                    stores.append(
                        go.start(
                            bufs[i].at[
                                pl.ds(pl.multiple_of(row, 16), wanted[j][0]),
                                pl.ds(col, wanted[j][1]),
                            ],
                            outs[j],
                        )
                    )
        else:
            for k, (i, r) in enumerate(parts):
                row, col = at[i]
                loads[k].wait()
                bufs[i][r : r + step, :] = scaled(
                    src[r : r + step, col : col + wanted[i][1]], row + r, step
                )
                stores.append(go.start(bufs[i].at[r : r + step, :], outs[i].at[r : r + step, :]))
        wait_all(stores)

    out_shape = [jax.ShapeDtypeStruct(w, BF) for w in wanted]
    scratch = [pltpu.VMEM((rows, hid) if n else (8, 128), F32)]
    scratch += [pltpu.VMEM(w, BF) for w in wanted]
    args = [in_hbm(weight)]
    if gain is not None:
        args.append(in_hbm(gain))
        scratch += [pltpu.VMEM((1, rows), F32), pltpu.VMEM((rows, 1), F32)]
    if tokens is not None:
        args.append(in_hbm(tokens))
        out_shape.append(jax.ShapeDtypeStruct((tok, width), BF))
        scratch += [pltpu.VMEM((tok, width), BF), pltpu.VMEM((tok, width), BF)]
    n_sem = 2 * rows // step + n + 2 * len(parts) + 8
    return hbm_call(
        body,
        tuple(out_shape),
        args,
        scratch_shapes=scratch + [pltpu.SemaphoreType.DMA((n_sem,))],
        compiler_params=LIMIT,
        cost_estimate=pl.CostEstimate(
            flops=10**8, bytes_accessed=6 * rows * hid, transcendentals=0
        ),
        name="cast",
    )


def feed(blocks, near, chunks, prev, down_near, cuts, n_chunk=512):
    tok, width = blocks[0].shape
    rows, hid = near[0].shape
    half = rows // 2
    tile = chunks[0][1][0].shape[1]
    nb, nc, npv = len(blocks), len(chunks), len(prev)
    n_tok = nb * tok
    nf = len(chunks[0][1])
    n_in = nb + 2 + nc * nf + npv + (2 if down_near else 0)
    n_out = nc + (len(cuts) if down_near else 0)
    n_sem = n_in + nc * 2 + n_out * (2 * rows // n_chunk + 1)

    def body(*refs):
        ins, outs, scratch = refs[:n_in], refs[n_in : n_in + n_out], refs[n_in + n_out :]
        x, w, h, sems = scratch[0], scratch[1], scratch[2], scratch[-1]
        go = Copies(sems)
        tok_in, ins = ins[:nb], ins[nb:]
        near_in, ins = ins[:2], ins[2:]
        loads = [go.start(tok_in[b], x.at[b * tok : (b + 1) * tok, :]) for b in range(nb)]
        at = up_places(rows, half)
        per_tile = []
        for k, (t, _) in enumerate(chunks):
            far, ins = ins[:nf], ins[nf:]
            cols = pl.ds(t * tile, tile)
            srcs = [a.at[:, cols] for a in near_in] + list(far)
            sizes = [rows, rows] + [half] * nf
            per_tile.append(
                [
                    go.start(src, w.at[k, pl.ds(a, size), :])
                    for src, a, size in zip(srcs, at, sizes)
                ]
            )
        late = [go.start(ins[i], h.at[:, i * tile : (i + 1) * tile]) for i in range(npv)]
        ins = ins[npv:]
        if down_near:
            d, o = scratch[3], scratch[4]
            core = here()[1]
            late.append(go.start(ins[0], d.at[pl.ds(pl.multiple_of(core * rows, 128), rows), :]))
            late.append(
                go.start(ins[1], d.at[pl.ds(pl.multiple_of((1 - core) * rows, 128), rows), :])
            )
        wait_all(loads)
        stores = []
        for k, (t, _) in enumerate(chunks):
            wait_all(per_tile[k])
            for c in range(0, tile, n_chunk):
                n = min(n_chunk, tile)
                lifted = jnp.dot(x[...], w[k, :, c : c + n], preferred_element_type=F32)
                h[:, t * tile + c : t * tile + c + n] = jnp.square(
                    jnp.maximum(lifted, 0.0)
                ).astype(BF)
            stores.append(go.start(h.at[:, t * tile : (t + 1) * tile], outs[k]))
        wait_all(late)
        if down_near:
            for c in range(0, 2 * rows, n_chunk):
                o[:, c : c + n_chunk] = lax.dot_general(
                    h[...],
                    d[c : c + n_chunk, :],
                    (((1,), (1,)), ((), ())),
                    preferred_element_type=F32,
                ).astype(BF)
                for out, (first, count) in zip(outs[nc:], cuts):
                    stores.append(
                        go.start(
                            o.at[first : first + count, c : c + n_chunk],
                            out.at[:, c : c + n_chunk],
                        )
                    )
        wait_all(stores)

    out_shape = [jax.ShapeDtypeStruct((n_tok, tile), BF)] * nc
    scratch = [
        pltpu.VMEM((n_tok, width), BF),
        pltpu.VMEM((nc, width, tile), BF),
        pltpu.VMEM((n_tok, hid), BF),
    ]
    flops = 2 * n_tok * width * tile * nc
    if down_near:
        out_shape += [jax.ShapeDtypeStruct((count, 2 * rows), BF) for _, count in cuts]
        scratch += [pltpu.VMEM((2 * rows, hid), BF), pltpu.VMEM((n_tok, 2 * rows), BF)]
        flops += 2 * n_tok * hid * 2 * rows
    args = list(blocks) + list(near)
    for _, far in chunks:
        args += far
    args += list(prev) + list(down_near or [])
    return hbm_call(
        body,
        tuple(out_shape),
        args,
        scratch_shapes=scratch + [pltpu.SemaphoreType.DMA((n_sem,))],
        compiler_params=LIMIT,
        cost_estimate=pl.CostEstimate(
            flops=flops, bytes_accessed=2 * width * tile * nc, transcendentals=0
        ),
        name="feed",
    )


def down_far_step(hiddens, groups, cuts, sub):
    hid = groups[0][0].shape[1]
    n_groups, nf = len(groups), len(groups[0])
    counts = [h[0].shape[0] for h in hiddens]
    n_tok = sum(counts)
    n_h = sum(len(h) for h in hiddens)
    cols = n_groups * nf * sub
    n_in = n_h + n_groups * nf

    def body(*refs):
        ins, outs = refs[:n_in], refs[n_in : n_in + len(cuts)]
        h, d, o, sems = refs[n_in + len(cuts) :]
        go = Copies(sems)
        loads, k, r0 = [], 0, 0
        for tiles, count in zip(hiddens, counts):
            c0 = 0
            for t in tiles:
                loads.append(go.start(ins[k], h.at[r0 : r0 + count, c0 : c0 + t.shape[1]]))
                c0 += t.shape[1]
                k += 1
            r0 += count
        _, core, grp = here()
        for g in range(n_groups):
            place = [
                c * (cols // 2) + g * 2 * sub + side * sub
                for c in (core, 1 - core)
                for side in (grp, 1 - grp)
            ]
            for a in place:
                loads.append(go.start(ins[k], d.at[pl.ds(pl.multiple_of(a, 64), sub), :]))
                k += 1
        wait_all(loads)
        o[...] = lax.dot_general(
            h[...], d[...], (((1,), (1,)), ((), ())), preferred_element_type=F32
        ).astype(BF)
        stores = []
        for out, runs in zip(outs, cuts):
            r0 = 0
            for first, count in runs:
                stores.append(
                    go.start(o.at[first : first + count, :], out.at[r0 : r0 + count, :])
                )
                r0 += count
        wait_all(stores)

    return hbm_call(
        body,
        tuple(jax.ShapeDtypeStruct((sum(c for _, c in runs), cols), BF) for runs in cuts),
        [t for h in hiddens for t in h] + [p for g in groups for p in g],
        scratch_shapes=[
            pltpu.VMEM((n_tok, hid), BF),
            pltpu.VMEM((cols, hid), BF),
            pltpu.VMEM((n_tok, cols), BF),
            pltpu.SemaphoreType.DMA((n_in + sum(len(r) for r in cuts),)),
        ],
        compiler_params=LIMIT,
        cost_estimate=pl.CostEstimate(
            flops=2 * n_tok * cols * hid, bytes_accessed=2 * cols * hid, transcendentals=0
        ),
        name="down_far",
    )


def assemble(near, far, shape, places):
    pieces = list(near) + [p for g in far for p in g]

    def body(*refs):
        ins, out, buf, sems = refs[: len(pieces)], refs[len(pieces)], refs[-2], refs[-1]
        go = Copies(sems)
        spots = [
            (pl.ds(row, p.shape[0]), pl.ds(col, p.shape[1]))
            for p, (row, col) in zip(pieces, places())
        ]
        loads = [go.start(ref, buf.at[spot]) for ref, spot in zip(ins, spots)]
        stores = []
        for load, spot in zip(loads, spots):
            load.wait()
            stores.append(go.start(buf.at[spot], out.at[spot]))
        wait_all(stores)

    return hbm_call(
        body,
        jax.ShapeDtypeStruct(shape, BF),
        pieces,
        scratch_shapes=[pltpu.VMEM(shape, BF), pltpu.SemaphoreType.DMA((2 * len(pieces),))],
        compiler_params=LIMIT,
        cost_estimate=pl.CostEstimate(
            flops=10**9, bytes_accessed=4 * shape[0] * shape[1], transcendentals=0
        ),
        name="assemble",
    )


def add_rows(keep, got):
    return (keep.astype(F32) + got.astype(F32)).astype(BF)


def finish(near, far, post_gain, tok, rows):
    width = 4 * rows
    terms = [near] + far
    flat = [a for t in terms for a in t]

    def body(*refs):
        gain, ins, o = refs[0], list(refs[1:-1]), refs[-1]
        sums = []
        for t in terms:
            group, ins = ins[: len(t)], ins[len(t) :]
            sums.append(sum(g[:tok].astype(F32) for g in group))
        power = sum(jnp.sum(s * s, axis=1, keepdims=True) for s in sums)
        scale = lax.rsqrt(power / width + 1e-06)
        y = here()[0]

        def put(value, start):
            to = pl.ds(pl.multiple_of(start, 128), value.shape[1])
            o[:, to] = (value * scale * gain[:, to]).astype(BF)

        put(sums[0], y * 2 * rows)
        c0 = 0
        for s in sums[1:]:
            n = s.shape[1] // 2
            for c in range(2):
                put(s[:, c * n : (c + 1) * n], (1 - y) * 2 * rows + c * rows + c0)
            c0 += n

    vm = pl.BlockSpec(memory_space=pltpu.VMEM)
    return pl.pallas_call(
        body,
        out_shape=jax.ShapeDtypeStruct((tok, width), BF),
        in_specs=[vm] * (1 + len(flat)),
        out_specs=vm,
        name="finish",
    )(post_gain.reshape(1, width), *flat)


U_CUTS = 4
D_CUTS = 4
LEAD = 3
ROUNDS = ((0, 1), (2, 3))


def routed():
    def grp_swap(v):
        return lax.ppermute(v, "grp", [(0, 1), (1, 0)])

    def y_swap(v):
        return lax.ppermute(v, "fs", [(i, i ^ 2) for i in range(4)])

    def core_swap(v):
        return lax.ppermute(v, "fs", [(i, i ^ 1) for i in range(4)])

    def tp_swap(v, m):
        return lax.ppermute(v, "tp", [(i, i ^ m) for i in range(4)])

    def per_device(prompt_tokens, up_weight, down_weight, pre_gain, post_gain):
        rows, hid = up_weight.shape
        tok, _ = prompt_tokens.shape
        half = rows // 2
        tile = hid // U_CUTS
        sub = half // D_CUTS

        def exchange(mine):
            got = y_swap(mine)
            near = core_swap(got)
            part = grp_swap(got)
            return [got, part, near, core_swap(part)]

        gain = pre_gain.reshape(1, rows)
        spots = [lambda i=i: (here()[2] * half, i * tile) for i in range(U_CUTS)]
        block = (half, tile)
        lead = cast(up_weight, gain, [block] * LEAD, lambda: [f() for f in spots[:LEAD]])
        *_, r0 = cast(up_weight, None, [], lambda: [], prompt_tokens)
        up_own, *rest = cast(
            up_weight,
            gain,
            [(rows, hid)] + [block] * (U_CUTS - LEAD),
            lambda: [(0, 0)] + [f() for f in spots[LEAD:]],
        )
        down_own, *mine = cast(
            down_weight,
            None,
            [(rows, hid)] + [(sub, hid)] * D_CUTS,
            lambda: [(0, 0)] + [((2 * i + here()[2]) * sub, 0) for i in range(D_CUTS)],
        )
        up_far = [exchange(v) for v in [*lead, *rest]]
        down_far = [exchange(v) for v in mine]
        up_near = [up_own, core_swap(up_own)]
        down_near = [down_own, core_swap(down_own)]

        r2 = tp_swap(r0, 2)
        r1 = tp_swap(r0, 1)
        r3 = tp_swap(r2, 1)

        tiles = list(enumerate(up_far))
        cut = [(0, tok), (tok, tok), (2 * tok, tok)]
        hidden = list(feed([r1, r0, r2], up_near, tiles[:-1], [], None, []))
        last, send1, keep0, keep2 = feed([r1, r0, r2], up_near, tiles[-1:], hidden, down_near, cut)
        hidden = hidden + [last]
        got1 = tp_swap(send1, 1)
        *hidden3, send3 = feed([r3], up_near, tiles, [], down_near, cut[:1])
        got3 = tp_swap(send3, 1)
        pair = add_rows(keep2, got3)
        near_terms = [keep0, got1, tp_swap(pair, 2)]

        far_terms = []
        cuts = [[cut[0], (3 * tok, tok)], [cut[1]], [cut[2]]]
        for ids in ROUNDS:
            send, keep0, keep2 = down_far_step(
                [hidden, hidden3], [down_far[g] for g in ids], cuts, sub
            )
            got = tp_swap(send, 1)
            pair = add_rows(keep2, got[tok:])
            far_terms.append([keep0, got, tp_swap(pair, 2)])

        def up_spots():
            at = up_places(rows, half)
            spots = [(a, 0) for a in at[:2]]
            return spots + [(a, i * tile) for i in range(U_CUTS) for a in at[2:]]

        def down_spots():
            y, core, grp = here()
            spots = [((2 * y + c) * rows, 0) for c in (core, 1 - core)]
            for i in range(D_CUTS):
                spots += [
                    ((2 * (1 - y) + c) * rows + (2 * i + side) * sub, 0)
                    for c in (core, 1 - core)
                    for side in (grp, 1 - grp)
                ]
            return [(pl.multiple_of(a, 64), c) for a, c in spots]

        shape = (4 * rows, hid)
        whole_up = assemble(up_near, up_far, shape, up_spots)
        whole_down = assemble(down_near, down_far, shape, down_spots)
        mixed = finish(near_terms, far_terms, post_gain, tok, rows)
        return mixed, whole_up, whole_down

    return per_device


def solution(mesh):
    placed = (P(("grp", "fs", "tp"), None), P("fs", "tp"), P("fs", "tp"), P("fs"), P())
    fits = all(mesh.shape[a] == n for a, n in (("grp", 2), ("fs", 4), ("tp", 4)))
    return jax.shard_map(
        routed() if fits else plain,
        mesh=mesh,
        in_specs=placed,
        out_specs=(P(("grp", "fs", "tp"), None), P("grp", "tp"), P("grp", "tp")),
        check_vma=False,
    )
```

time: 266 us -> 172 us (0.65)
  waiting for transfers between devices: 204 us -> 89 us
  starting transfers between devices: 0.16 us -> 40.7 us
  Pallas kernels: 0 us -> 40.2 us
  matrix products: 16.5 us -> 0 us
  local copies, waits for them, and re-layouts: 16.9 us -> 0.77 us
  other arithmetic: 14.1 us -> 0.13 us
  between operations: 13.8 us -> 0.89 us
    all_gather x3 -> x0, waiting for transfers between devices: 160 us -> none  [the longest x1 60.4 us: per_device(): lax.all_gather(down_local, 'fs', axis=0, tiled=True)]
    ppermute x0 -> x44, waiting for transfers between devices: none -> 89 us  [the longest x10 38.4 us: tp_swap(): return lax.ppermute(v, 'tp', [(i, i ^ m) for i in range(4)])]
    reduce_scatter x1 -> x0, waiting for transfers between devices: 43.8 us -> none  [per_device(): lax.psum_scatter(lax.dot_general(hidden, sampler_down, (((1,), (1,)), (()...]
    ppermute x0 -> x44, starting transfers between devices: none -> 40.7 us  [the longest x10 15.7 us: tp_swap(): return lax.ppermute(v, 'tp', [(i, i ^ m) for i in range(4)])]
    pallas_call x0 -> x12, Pallas kernels: none -> 40.2 us  [the longest x11 37.6 us: hbm_call(): pl.pallas_call(body, out_shape=out_shape, in_specs=[ANY] * len(args), out...]
    dot_general x1 -> x0, matrix products: 16.5 us -> none  [per_device(): lax.dot_general(hidden, sampler_down, (((1,), (1,)), ((), ())), preferred...]
    unnamed x4 -> x18, local copies, waits for them, and re-layouts: 16.9 us -> 0.77 us
    convert_element_type x4 -> x3, other arithmetic: 11.6 us -> 0.13 us  [add_rows(): return (keep.astype(F32) + got.astype(F32)).astype(BF)]
  transfers between devices with their start and end apart: 4 -> 44, of which waited for: 4 -> 20; matrix products, arithmetic and copies ran while one was open for 3% -> 0% of each run, Pallas kernels for 0% -> 20%
where the time goes in v2:
time: 172 us
  waiting for transfers between devices  89 us (52%)
  starting transfers between devices  40.7 us (24%)
  Pallas kernels  40.2 us (23%)
    ppermute x10, waiting for transfers between devices, tp_swap(): return lax.ppermute(v, 'tp', [(i, i ^ m) for i in range(4)])  38.4 us
    pallas_call x11, Pallas kernels, hbm_call(): pl.pallas_call(body, out_shape=out_shape, in_specs=[ANY] * len(args), out...  37.6 us
    ppermute x8, waiting for transfers between devices, y_swap(): return lax.ppermute(v, 'fs', [(i, i ^ 2) for i in range(4)])  26.8 us
    ppermute x8, waiting for transfers between devices, grp_swap(): return lax.ppermute(v, 'grp', [(0, 1), (1, 0)])  22.6 us
    ppermute x10, starting transfers between devices, tp_swap(): return lax.ppermute(v, 'tp', [(i, i ^ m) for i in range(4)])  15.7 us
    ppermute x8, starting transfers between devices, y_swap(): return lax.ppermute(v, 'fs', [(i, i ^ 2) for i in range(4)])  11.2 us
    ppermute x8, starting transfers between devices, grp_swap(): return lax.ppermute(v, 'grp', [(0, 1), (1, 0)])  11 us
  transfers between devices with their start and end apart: 44, of which 20 were waited for; matrix products, arithmetic and copies ran while one was open for 0% of the time, Pallas kernels for 20%

profile of v2, /device:TPU:0, one launch (start us, length us, event | category | flops | bytes accessed | tf_op | source)
XLA Modules:
  0.0 171.7 jit_solution(18209939150881201594)
XLA Ops:
  0.6 2.8 %cast.5 = (bf16[512,2048]{1,0:T(8,128)(2,1)S(1)}, bf16[256,512]{1,0:T(8,128)(2,1)S(1)}) custom-call(f32[512,2048]{1,0:T(8,128)} %refs_0_.6, f32[1,512]{1,0:T(1,128)} %bitcast.3), custom_call_target="tpu_custom_call" | custom-call | flops 100000000 | bytes 6291456 | tf_op jit(solution)/shard_map/cast/pallas_call | solution.py:46
  3.4 3.1 %collective-permute-start.3 = (bf16[256,512]{1,0:T(8,128)(2,1)S(1)}, bf16[256,512]{1,0:T(8,128)(2,1)S(1)}, u32[]{:S(2)}, u32[]{:S(2)}) collective-permute-start(bf16[256,512]{1,0:T(8,128)(2,1)S(1)} %get-tuple-element.32), channel_id=1, source_target_pairs={{0,8},{4,12},{8,0},{12,4},{1,9},{5,13},{9,1},{13,5},{2,10},{6,14},... | collective-permute-start | bytes 786440 | tf_op jit(solution)/shard_map/ppermute | solution.py:451
  6.5 3.3 %cast.6 = (bf16[256,512]{1,0:T(8,128)(2,1)S(1)}, bf16[256,512]{1,0:T(8,128)(2,1)S(1)}, bf16[256,512]{1,0:T(8,128)(2,1)S(1)}) custom-call(f32[512,2048]{1,0:T(8,128)} %refs_0_.6, f32[1,512]{1,0:T(1,128)} %bitcast.4), custom_call_target="tpu_custom_call" | custom-call | flops 100000000 | bytes 6291456 | tf_op jit(solution)/shard_map/cast/pallas_call | solution.py:46
  9.9 2.0 %collective-permute-start.11 = (bf16[256,512]{1,0:T(8,128)(2,1)S(1)}, bf16[256,512]{1,0:T(8,128)(2,1)S(1)}, u32[]{:S(2)}, u32[]{:S(2)}) collective-permute-start(bf16[256,512]{1,0:T(8,128)(2,1)S(1)} %get-tuple-element.34), channel_id=1, source_target_pairs={{0,8},{4,12},{8,0},{12,4},{1,9},{5,13},{9,1},{13,5},{2,10},{6,14},... | collective-permute-start | bytes 786440 | tf_op jit(solution)/shard_map/ppermute | solution.py:451
  11.9 2.8 %cast.7 = (bf16[512,2048]{1,0:T(8,128)(2,1)S(1)}, bf16[64,2048]{1,0:T(8,128)(2,1)S(1)}, bf16[64,2048]{1,0:T(8,128)(2,1)S(1)}, bf16[64,2048]{1,0:T(8,128)(2,1)S(1)}, bf16[64,2048]{1,0:T(8,128)(2,1)S(1)}) custom-call(f32[512,2048]{1,0:T(8,128)} %refs_0_.7), custom_call_target="tpu_custom_call" | custom-call | flops 100000000 | bytes 6291456 | tf_op jit(solution)/shard_map/cast/pallas_call | solution.py:46
  14.7 2.0 %collective-permute-start.24 = (bf16[64,2048]{1,0:T(8,128)(2,1)S(1)}, bf16[64,2048]{1,0:T(8,128)(2,1)S(1)}, u32[]{:S(2)}, u32[]{:S(2)}) collective-permute-start(bf16[64,2048]{1,0:T(8,128)(2,1)S(1)} %get-tuple-element.49), channel_id=1, source_target_pairs={{0,8},{4,12},{8,0},{12,4},{1,9},{5,13},{9,1},{13,5},{2,10},{6,14},... | collective-permute-start | bytes 786440 | tf_op jit(solution)/shard_map/ppermute | solution.py:451
  16.8 2.4 %collective-permute-done.7.refs_5_.refs_3_.refs_2_ = bf16[256,512]{1,0:T(8,128)(2,1)S(1)} collective-permute-done((bf16[256,512]{1,0:T(8,128)(2,1)S(1)}, bf16[256,512]{1,0:T(8,128)(2,1)S(1)}, u32[]{:S(2)}, u32[]{:S(2)}) %collective-permute-start.7) | collective-permute-done | bytes 262176 | tf_op jit(solution)/shard_map/ppermute | solution.py:451
  19.2 2.1 %collective-permute-start.34 = (bf16[64,2048]{1,0:T(8,128)(2,1)S(1)}, bf16[64,2048]{1,0:T(8,128)(2,1)S(1)}, u32[]{:S(2)}, u32[]{:S(2)}) collective-permute-start(bf16[64,2048]{1,0:T(8,128)(2,1)S(1)} %get-tuple-element.54), channel_id=1, source_target_pairs={{0,8},{4,12},{8,0},{12,4},{1,9},{5,13},{9,1},{13,5},{2,10},{6,14},... | collective-permute-start | bytes 786440 | tf_op jit(solution)/shard_map/ppermute | solution.py:451
  21.3 1.5 cast.4.refs_1_
  22.8 2.0 %collective-permute-done.11.refs_9_.refs_7_.refs_6_ = bf16[256,512]{1,0:T(8,128)(2,1)S(1)} collective-permute-done((bf16[256,512]{1,0:T(8,128)(2,1)S(1)}, bf16[256,512]{1,0:T(8,128)(2,1)S(1)}, u32[]{:S(2)}, u32[]{:S(2)}) %collective-permute-start.11) | collective-permute-done | bytes 262176 | tf_op jit(solution)/shard_map/ppermute | solution.py:451
  24.8 2.0 %collective-permute-start = (bf16[128,2048]{1,0:T(8,128)(2,1)S(1)}, bf16[128,2048]{1,0:T(8,128)(2,1)S(1)}, u32[]{:S(2)}, u32[]{:S(2)}) collective-permute-start(bf16[128,2048]{1,0:T(8,128)(2,1)S(1)} %cast.4.refs_1_), channel_id=1, source_target_pairs={{0,1},{1,0},{2,3},{3,2},{4,5},{5,4},{6,7},{7,6},{8,9},{9,8},{10,11... | collective-permute-start | bytes 1572872 | tf_op jit(solution)/shard_map/ppermute | solution.py:457
  26.8 3.6 %collective-permute-done.15.refs_13_.refs_11_.refs_10_ = bf16[256,512]{1,0:T(8,128)(2,1)S(1)} collective-permute-done((bf16[256,512]{1,0:T(8,128)(2,1)S(1)}, bf16[256,512]{1,0:T(8,128)(2,1)S(1)}, u32[]{:S(2)}, u32[]{:S(2)}) %collective-permute-start.15) | collective-permute-done | bytes 262176 | tf_op jit(solution)/shard_map/ppermute | solution.py:451
  30.4 5.6 %collective-permute-done.24.refs_8_.refs_2_ = bf16[64,2048]{1,0:T(8,128)(2,1)S(1)} collective-permute-done((bf16[64,2048]{1,0:T(8,128)(2,1)S(1)}, bf16[64,2048]{1,0:T(8,128)(2,1)S(1)}, u32[]{:S(2)}, u32[]{:S(2)}) %collective-permute-start.24) | collective-permute-done | bytes 262176 | tf_op jit(solution)/shard_map/ppermute | solution.py:451
  36.0 5.6 %collective-permute-done.28.refs_12_.refs_6_ = bf16[64,2048]{1,0:T(8,128)(2,1)S(1)} collective-permute-done((bf16[64,2048]{1,0:T(8,128)(2,1)S(1)}, bf16[64,2048]{1,0:T(8,128)(2,1)S(1)}, u32[]{:S(2)}, u32[]{:S(2)}) %collective-permute-start.28) | collective-permute-done | bytes 262176 | tf_op jit(solution)/shard_map/ppermute | solution.py:451
  41.6 3.0 %collective-permute-start.1 = (bf16[128,2048]{1,0:T(8,128)(2,1)S(1)}, bf16[128,2048]{1,0:T(8,128)(2,1)S(1)}, u32[]{:S(2)}, u32[]{:S(2)}) collective-permute-start(bf16[128,2048]{1,0:T(8,128)(2,1)S(1)} %cast.4.refs_1_), channel_id=1, source_target_pairs={{0,2},{1,3},{2,0},{3,1},{4,6},{5,7},{6,4},{7,5},{8,10},{9,11},{10,... | collective-permute-start | bytes 1572872 | tf_op jit(solution)/shard_map/ppermute | solution.py:457
  44.7 1.8 %collective-permute-done.34.refs_8_.refs_10_ = bf16[64,2048]{1,0:T(8,128)(2,1)S(1)} collective-permute-done((bf16[64,2048]{1,0:T(8,128)(2,1)S(1)}, bf16[64,2048]{1,0:T(8,128)(2,1)S(1)}, u32[]{:S(2)}, u32[]{:S(2)}) %collective-permute-start.34) | collective-permute-done | bytes 262176 | tf_op jit(solution)/shard_map/ppermute | solution.py:451
  46.5 1.7 %collective-permute-start.38 = (bf16[64,2048]{1,0:T(8,128)(2,1)S(1)}, bf16[64,2048]{1,0:T(8,128)(2,1)S(1)}, u32[]{:S(2)}, u32[]{:S(2)}) collective-permute-start(bf16[64,2048]{1,0:T(8,128)(2,1)S(1)} %get-tuple-element.55), channel_id=1, source_target_pairs={{0,8},{4,12},{8,0},{12,4},{1,9},{5,13},{9,1},{13,5},{2,10},{6,14},... | collective-permute-start | bytes 786440 | tf_op jit(solution)/shard_map/ppermute | solution.py:451
  48.2 5.8 %collective-permute-done.38.refs_12_.refs_14_ = bf16[64,2048]{1,0:T(8,128)(2,1)S(1)} collective-permute-done((bf16[64,2048]{1,0:T(8,128)(2,1)S(1)}, bf16[64,2048]{1,0:T(8,128)(2,1)S(1)}, u32[]{:S(2)}, u32[]{:S(2)}) %collective-permute-start.38) | collective-permute-done | bytes 262176 | tf_op jit(solution)/shard_map/ppermute | solution.py:451
  54.0 1.5 collective-permute-start.4
  55.5 10.6 %collective-permute-done.1.refs_2_ = bf16[128,2048]{1,0:T(8,128)(2,1)S(1)} collective-permute-done((bf16[128,2048]{1,0:T(8,128)(2,1)S(1)}, bf16[128,2048]{1,0:T(8,128)(2,1)S(1)}, u32[]{:S(2)}, u32[]{:S(2)}) %collective-permute-start.1) | collective-permute-done | bytes 524320 | tf_op jit(solution)/shard_map/ppermute | solution.py:457
  66.1 1.5 collective-permute-start.8
  68.3 7.1 %collective-permute-done.8.refs_6_.refs_4_.refs_3_ = bf16[256,512]{1,0:T(8,128)(2,1)S(1)} collective-permute-done((bf16[256,512]{1,0:T(8,128)(2,1)S(1)}, bf16[256,512]{1,0:T(8,128)(2,1)S(1)}, u32[]{:S(2)}, u32[]{:S(2)}) %collective-permute-start.8) | collective-permute-done | bytes 262176 | tf_op jit(solution)/shard_map/ppermute | solution.py:448
  75.3 1.5 collective-permute-start.16
  76.8 2.7 %collective-permute-done.12.refs_10_.refs_8_.refs_7_ = bf16[256,512]{1,0:T(8,128)(2,1)S(1)} collective-permute-done((bf16[256,512]{1,0:T(8,128)(2,1)S(1)}, bf16[256,512]{1,0:T(8,128)(2,1)S(1)}, u32[]{:S(2)}, u32[]{:S(2)}) %collective-permute-start.12) | collective-permute-done | bytes 262176 | tf_op jit(solution)/shard_map/ppermute | solution.py:448
  79.5 1.5 collective-permute-start.25
  81.0 4.1 %collective-permute-done.16.refs_14_.refs_12_.refs_11_ = bf16[256,512]{1,0:T(8,128)(2,1)S(1)} collective-permute-done((bf16[256,512]{1,0:T(8,128)(2,1)S(1)}, bf16[256,512]{1,0:T(8,128)(2,1)S(1)}, u32[]{:S(2)}, u32[]{:S(2)}) %collective-permute-start.16) | collective-permute-done | bytes 262176 | tf_op jit(solution)/shard_map/ppermute | solution.py:448
  85.1 1.5 collective-permute-start.29
  86.6 4.1 %collective-permute-done.25.refs_9_.refs_3_ = bf16[64,2048]{1,0:T(8,128)(2,1)S(1)} collective-permute-done((bf16[64,2048]{1,0:T(8,128)(2,1)S(1)}, bf16[64,2048]{1,0:T(8,128)(2,1)S(1)}, u32[]{:S(2)}, u32[]{:S(2)}) %collective-permute-start.25) | collective-permute-done | bytes 262176 | tf_op jit(solution)/shard_map/ppermute | solution.py:448
  91.3 4.6 %collective-permute-done.29.refs_13_.refs_7_ = bf16[64,2048]{1,0:T(8,128)(2,1)S(1)} collective-permute-done((bf16[64,2048]{1,0:T(8,128)(2,1)S(1)}, bf16[64,2048]{1,0:T(8,128)(2,1)S(1)}, u32[]{:S(2)}, u32[]{:S(2)}) %collective-permute-start.29) | collective-permute-done | bytes 262176 | tf_op jit(solution)/shard_map/ppermute | solution.py:448
  95.8 1.7 collective-permute-start.21
  99.4 1.5 collective-permute-start.35
  100.9 8.3 %collective-permute-done.21.refs_0_ = bf16[128,2048]{1,0:T(8,128)(2,1)S(1)} collective-permute-done((bf16[128,2048]{1,0:T(8,128)(2,1)S(1)}, bf16[128,2048]{1,0:T(8,128)(2,1)S(1)}, u32[]{:S(2)}, u32[]{:S(2)}) %collective-permute-start.21) | collective-permute-done | bytes 524320 | tf_op jit(solution)/shard_map/ppermute | solution.py:457
  109.2 1.5 collective-permute-start.39
  111.2 5.3 %feed.5 = (bf16[128,512]{1,0:T(8,128)(2,1)S(1)}, bf16[128,512]{1,0:T(8,128)(2,1)S(1)}, bf16[128,512]{1,0:T(8,128)(2,1)S(1)}, bf16[128,512]{1,0:T(8,128)(2,1)S(1)}, bf16[128,1024]{1,0:T(8,128)(2,1)S(1)}) custom-call(bf16[128,2048]{1,0:T(8,128)(2,1)S(1)} %collective-permute-done.21.refs_0_, bf16[512,2048]{1,0:T(8,128)(2,1)S(1)} %get-tuple-element.31.refs_3_.refs_1_.refs_0_, ...), custom_call_target="tpu_custom_call" | custom-call | flops 1610612736 | bytes 8388608 | tf_op jit(solution)/shard_map/feed/pallas_call | solution.py:46
  116.5 4.2 %feed.3 = (bf16[384,512]{1,0:T(8,128)(2,1)S(1)}, bf16[384,512]{1,0:T(8,128)(2,1)S(1)}, bf16[384,512]{1,0:T(8,128)(2,1)S(1)}) custom-call(bf16[128,2048]{1,0:T(8,128)(2,1)S(1)} %collective-permute-done.refs_0_, bf16[128,2048]{1,0:T(8,128)(2,1)S(1)} %cast.4.refs_1_, bf16[128,2048]{1,0:T(8,128)(2,1)S(1)} %collective-permute-done.1.refs_2_, ...), custom_call_target="tpu_custom_call" | custom-call | flops 2415919104 | bytes 6291456 | tf_op jit(solution)/shard_map/feed/pallas_call | solution.py:46
  121.9 1.3 collective-permute-start.22
  123.1 4.3 %feed.4 = (bf16[384,512]{1,0:T(8,128)(2,1)S(1)}, bf16[128,1024]{1,0:T(8,128)(2,1)S(1)}, bf16[128,1024]{1,0:T(8,128)(2,1)S(1)}, bf16[128,1024]{1,0:T(8,128)(2,1)S(1)}) custom-call(bf16[128,2048]{1,0:T(8,128)(2,1)S(1)} %collective-permute-done.refs_0_, bf16[128,2048]{1,0:T(8,128)(2,1)S(1)} %cast.4.refs_1_, ...), custom_call_target="tpu_custom_call" | custom-call | flops 2415919104 | bytes 2097152 | tf_op jit(solution)/shard_map/feed/pallas_call | solution.py:46
  127.5 2.5 %down_far.2 = (bf16[256,512]{1,0:T(8,128)(2,1)S(1)}, bf16[128,512]{1,0:T(8,128)(2,1)S(1)}, bf16[128,512]{1,0:T(8,128)(2,1)S(1)}) custom-call(bf16[384,512]{1,0:T(8,128)(2,1)S(1)} %get-tuple-element.36.refs_9_.refs_0_, bf16[384,512]{1,0:T(8,128)(2,1)S(1)} %get-tuple-element.37.refs_10_.refs_1_, bf16[384,512]{1,0:T(8,128)(2,1)S(1)} %get-tuple-element.38.refs_11_.refs_2_, ...), custom_call_target="tpu_custom_call" | custom-call | flops 1073741824 | bytes 2097152 | tf_op jit(solution)/shard_map/down_far/pallas_call | solution.py:46
  130.8 1.3 collective-permute-start.32
  132.1 2.5 %down_far.3 = (bf16[256,512]{1,0:T(8,128)(2,1)S(1)}, bf16[128,512]{1,0:T(8,128)(2,1)S(1)}, bf16[128,512]{1,0:T(8,128)(2,1)S(1)}) custom-call(bf16[384,512]{1,0:T(8,128)(2,1)S(1)} %get-tuple-element.36.refs_9_.refs_0_, bf16[384,512]{1,0:T(8,128)(2,1)S(1)} %get-tuple-element.37.refs_10_.refs_1_, bf16[384,512]{1,0:T(8,128)(2,1)S(1)} %get-tuple-element.38.refs_11_.refs_2_, ...), custom_call_target="tpu_custom_call" | custom-call | flops 1073741824 | bytes 2097152 | tf_op jit(solution)/shard_map/down_far/pallas_call | solution.py:46
  135.6 3.0 %collective-permute-start.23 = (bf16[128,1024]{1,0:T(8,128)(2,1)S(1)}, bf16[128,1024]{1,0:T(8,128)(2,1)S(1)}, u32[]{:S(2)}, u32[]{:S(2)}) collective-permute-start(bf16[128,1024]{1,0:T(8,128)(2,1)S(1)} %add_convert_fusion), channel_id=1, source_target_pairs={{0,2},{1,3},{2,0},{3,1},{4,6},{5,7},{6,4},{7,5},{8,10},{9,11},{10,... | collective-permute-start | bytes 786440 | tf_op jit(solution)/shard_map/ppermute | solution.py:457
  138.5 12.0 %collective-permute-done.32.refs_5_ = bf16[256,512]{1,0:T(8,128)(2,1)S(1)} collective-permute-done((bf16[256,512]{1,0:T(8,128)(2,1)S(1)}, bf16[256,512]{1,0:T(8,128)(2,1)S(1)}, u32[]{:S(2)}, u32[]{:S(2)}) %collective-permute-start.32) | collective-permute-done | bytes 262176 | tf_op jit(solution)/shard_map/ppermute | solution.py:457
  151.8 4.0 %collective-permute-done.42.refs_8_ = bf16[256,512]{1,0:T(8,128)(2,1)S(1)} collective-permute-done((bf16[256,512]{1,0:T(8,128)(2,1)S(1)}, bf16[256,512]{1,0:T(8,128)(2,1)S(1)}, u32[]{:S(2)}, u32[]{:S(2)}) %collective-permute-start.42) | collective-permute-done | bytes 262176 | tf_op jit(solution)/shard_map/ppermute | solution.py:457
  156.4 4.2 %assemble.2 = bf16[2048,2048]{1,0:T(8,128)(2,1)} custom-call(bf16[512,2048]{1,0:T(8,128)(2,1)S(1)} %get-tuple-element.31.refs_3_.refs_1_.refs_0_, bf16[512,2048]{1,0:T(8,128)(2,1)S(1)} %collective-permute-done.2.refs_4_.refs_2_.refs_1_, bf16[256,512]{1,0:T(8,128)(2,1)S(1)} %collective-permute-done.7.refs_5_.refs_3_.refs_2_, ...), custom_call_target="tpu_custom_call" | custom-call | flops 1000000000 | bytes 16777216 | tf_op jit(solution)/shard_map/assemble/pallas_call | solution.py:46
  160.6 4.2 %assemble.3 = bf16[2048,2048]{1,0:T(8,128)(2,1)} custom-call(bf16[512,2048]{1,0:T(8,128)(2,1)S(1)} %get-tuple-element.39.refs_12_.refs_19_.refs_0_, bf16[512,2048]{1,0:T(8,128)(2,1)S(1)} %collective-permute-done.19.refs_13_.refs_20_.refs_1_, bf16[64,2048]{1,0:T(8,128)(2,1)S(1)} %collective-permute-done.24.refs_8_.refs_2_, ...), custom_call_target="tpu_custom_call" | custom-call | flops 1000000000 | bytes 16777216 | tf_op jit(solution)/shard_map/assemble/pallas_call | solution.py:46
  164.9 1.5 collective-permute-done.33.refs_6_
  166.3 2.0 %collective-permute-done.43.refs_9_ = bf16[128,512]{1,0:T(8,128)(2,1)S(1)} collective-permute-done((bf16[128,512]{1,0:T(8,128)(2,1)S(1)}, bf16[128,512]{1,0:T(8,128)(2,1)S(1)}, u32[]{:S(2)}, u32[]{:S(2)}) %collective-permute-start.43) | collective-permute-done | bytes 131104 | tf_op jit(solution)/shard_map/ppermute | solution.py:457
  169.1 2.6 %finish.1 = bf16[128,2048]{1,0:T(8,128)(2,1)} custom-call(f32[1,2048]{1,0:T(1,128)} %bitcast.2, bf16[128,1024]{1,0:T(8,128)(2,1)} %copy-done, bf16[128,1024]{1,0:T(8,128)(2,1)} %copy-done.5, bf16[128,1024]{1,0:T(8,128)(2,1)} %copy-done.6, bf16[128,512]{1,0:T(8,128)(2,1)} %copy-done.1, bf16[256,512]{1,0:T(8,128)(2,1)} %copy-done.3, ...), custom_call_target="tpu_custom_call" | custom-call | tf_op jit(solution)/shard_map/finish/pallas_call | solution.py:431
  (73 shorter events, 9.2 us)
Async XLA Ops:
  3.4 13.3 %collective-permute-start.3 = (bf16[256,512]{1,0:T(8,128)(2,1)S(1)}, bf16[256,512]{1,0:T(8,128)(2,1)S(1)}, u32[]{:S(2)}, u32[]{:S(2)}) collective-permute-start(bf16[256,512]{1,0:T(8,128)(2,1)S(1)} %get-tuple-element.32), channel_id=1, source_target_pairs={{0,8},{4,12},{8,0},{12,4},{1,9},{5,13},{9,1},{13,5},{2,10},{6,14},... | collective-permute-start | bytes 786440 | tf_op jit(solution)/shard_map/ppermute | solution.py:451
  9.8 9.4 %collective-permute-start.7 = (bf16[256,512]{1,0:T(8,128)(2,1)S(1)}, bf16[256,512]{1,0:T(8,128)(2,1)S(1)}, u32[]{:S(2)}, u32[]{:S(2)}) collective-permute-start(bf16[256,512]{1,0:T(8,128)(2,1)S(1)} %get-tuple-element.33), channel_id=1, source_target_pairs={{0,8},{4,12},{8,0},{12,4},{1,9},{5,13},{9,1},{13,5},{2,10},{6,14},... | collective-permute-start | bytes 786440 | tf_op jit(solution)/shard_map/ppermute | solution.py:451
  9.9 14.9 %collective-permute-start.11 = (bf16[256,512]{1,0:T(8,128)(2,1)S(1)}, bf16[256,512]{1,0:T(8,128)(2,1)S(1)}, u32[]{:S(2)}, u32[]{:S(2)}) collective-permute-start(bf16[256,512]{1,0:T(8,128)(2,1)S(1)} %get-tuple-element.34), channel_id=1, source_target_pairs={{0,8},{4,12},{8,0},{12,4},{1,9},{5,13},{9,1},{13,5},{2,10},{6,14},... | collective-permute-start | bytes 786440 | tf_op jit(solution)/shard_map/ppermute | solution.py:451
  11.9 18.5 %collective-permute-start.15 = (bf16[256,512]{1,0:T(8,128)(2,1)S(1)}, bf16[256,512]{1,0:T(8,128)(2,1)S(1)}, u32[]{:S(2)}, u32[]{:S(2)}) collective-permute-start(bf16[256,512]{1,0:T(8,128)(2,1)S(1)} %get-tuple-element.35), channel_id=1, source_target_pairs={{0,8},{4,12},{8,0},{12,4},{1,9},{5,13},{9,1},{13,5},{2,10},{6,14},... | collective-permute-start | bytes 786440 | tf_op jit(solution)/shard_map/ppermute | solution.py:451
  14.7 21.3 %collective-permute-start.24 = (bf16[64,2048]{1,0:T(8,128)(2,1)S(1)}, bf16[64,2048]{1,0:T(8,128)(2,1)S(1)}, u32[]{:S(2)}, u32[]{:S(2)}) collective-permute-start(bf16[64,2048]{1,0:T(8,128)(2,1)S(1)} %get-tuple-element.49), channel_id=1, source_target_pairs={{0,8},{4,12},{8,0},{12,4},{1,9},{5,13},{9,1},{13,5},{2,10},{6,14},... | collective-permute-start | bytes 786440 | tf_op jit(solution)/shard_map/ppermute | solution.py:451
  16.7 24.9 %collective-permute-start.28 = (bf16[64,2048]{1,0:T(8,128)(2,1)S(1)}, bf16[64,2048]{1,0:T(8,128)(2,1)S(1)}, u32[]{:S(2)}, u32[]{:S(2)}) collective-permute-start(bf16[64,2048]{1,0:T(8,128)(2,1)S(1)} %get-tuple-element.50), channel_id=1, source_target_pairs={{0,8},{4,12},{8,0},{12,4},{1,9},{5,13},{9,1},{13,5},{2,10},{6,14},... | collective-permute-start | bytes 786440 | tf_op jit(solution)/shard_map/ppermute | solution.py:451
  19.2 27.3 %collective-permute-start.34 = (bf16[64,2048]{1,0:T(8,128)(2,1)S(1)}, bf16[64,2048]{1,0:T(8,128)(2,1)S(1)}, u32[]{:S(2)}, u32[]{:S(2)}) collective-permute-start(bf16[64,2048]{1,0:T(8,128)(2,1)S(1)} %get-tuple-element.54), channel_id=1, source_target_pairs={{0,8},{4,12},{8,0},{12,4},{1,9},{5,13},{9,1},{13,5},{2,10},{6,14},... | collective-permute-start | bytes 786440 | tf_op jit(solution)/shard_map/ppermute | solution.py:451
  24.8 30.7 %collective-permute-start = (bf16[128,2048]{1,0:T(8,128)(2,1)S(1)}, bf16[128,2048]{1,0:T(8,128)(2,1)S(1)}, u32[]{:S(2)}, u32[]{:S(2)}) collective-permute-start(bf16[128,2048]{1,0:T(8,128)(2,1)S(1)} %cast.4.refs_1_), channel_id=1, source_target_pairs={{0,1},{1,0},{2,3},{3,2},{4,5},{5,4},{6,7},{7,6},{8,9},{9,8},{10,11... | collective-permute-start | bytes 1572872 | tf_op jit(solution)/shard_map/ppermute | solution.py:457
  30.4 80.3 %collective-permute-start.2 = (bf16[512,2048]{1,0:T(8,128)(2,1)S(1)}, bf16[512,2048]{1,0:T(8,128)(2,1)S(1)}, u32[]{:S(2)}, u32[]{:S(2)}) collective-permute-start(bf16[512,2048]{1,0:T(8,128)(2,1)S(1)} %get-tuple-element.31.refs_3_.refs_1_.refs_0_), channel_id=1, source_target_pairs={{0,4},{4,0},{8,12},{12,8},{1,5},{5,1},{9,13},{13,9},{2,6},{6,2},{1... | collective-permute-start | bytes 6291464 | tf_op jit(solution)/shard_map/ppermute | solution.py:454
  36.0 74.7 %collective-permute-start.19 = (bf16[512,2048]{1,0:T(8,128)(2,1)S(1)}, bf16[512,2048]{1,0:T(8,128)(2,1)S(1)}, u32[]{:S(2)}, u32[]{:S(2)}) collective-permute-start(bf16[512,2048]{1,0:T(8,128)(2,1)S(1)} %get-tuple-element.39.refs_12_.refs_19_.refs_0_), channel_id=1, source_target_pairs={{0,4},{4,0},{8,12},{12,8},{1,5},{5,1},{9,13},{13,9},{2,6},{6,2},{1... | collective-permute-start | bytes 6291464 | tf_op jit(solution)/shard_map/ppermute | solution.py:454
  41.6 24.5 %collective-permute-start.1 = (bf16[128,2048]{1,0:T(8,128)(2,1)S(1)}, bf16[128,2048]{1,0:T(8,128)(2,1)S(1)}, u32[]{:S(2)}, u32[]{:S(2)}) collective-permute-start(bf16[128,2048]{1,0:T(8,128)(2,1)S(1)} %cast.4.refs_1_), channel_id=1, source_target_pairs={{0,2},{1,3},{2,0},{3,1},{4,6},{5,7},{6,4},{7,5},{8,10},{9,11},{10,... | collective-permute-start | bytes 1572872 | tf_op jit(solution)/shard_map/ppermute | solution.py:457
  46.5 7.5 %collective-permute-start.38 = (bf16[64,2048]{1,0:T(8,128)(2,1)S(1)}, bf16[64,2048]{1,0:T(8,128)(2,1)S(1)}, u32[]{:S(2)}, u32[]{:S(2)}) collective-permute-start(bf16[64,2048]{1,0:T(8,128)(2,1)S(1)} %get-tuple-element.55), channel_id=1, source_target_pairs={{0,8},{4,12},{8,0},{12,4},{1,9},{5,13},{9,1},{13,5},{2,10},{6,14},... | collective-permute-start | bytes 786440 | tf_op jit(solution)/shard_map/ppermute | solution.py:451
  54.0 13.6 %collective-permute-start.4 = (bf16[256,512]{1,0:T(8,128)(2,1)S(1)}, bf16[256,512]{1,0:T(8,128)(2,1)S(1)}, u32[]{:S(2)}, u32[]{:S(2)}) collective-permute-start(bf16[256,512]{1,0:T(8,128)(2,1)S(1)} %collective-permute-done.3.refs_5_.refs_15_.refs_14_), channel_id=1, source_target_pairs={{0,16},{16,0},{1,17},{17,1},{2,18},{18,2},{3,19},{19,3},{4,20},{20... | collective-permute-start | bytes 786440 | tf_op jit(solution)/shard_map/ppermute | solution.py:448
  55.5 12.1 %collective-permute-start.5 = (bf16[256,512]{1,0:T(8,128)(2,1)S(1)}, bf16[256,512]{1,0:T(8,128)(2,1)S(1)}, u32[]{:S(2)}, u32[]{:S(2)}) collective-permute-start(bf16[256,512]{1,0:T(8,128)(2,1)S(1)} %collective-permute-done.3.refs_5_.refs_15_.refs_14_), channel_id=1, source_target_pairs={{0,4},{4,0},{8,12},{12,8},{1,5},{5,1},{9,13},{13,9},{2,6},{6,2},{1... | collective-permute-start | bytes 786440 | tf_op jit(solution)/shard_map/ppermute | solution.py:454
  66.1 9.2 %collective-permute-start.8 = (bf16[256,512]{1,0:T(8,128)(2,1)S(1)}, bf16[256,512]{1,0:T(8,128)(2,1)S(1)}, u32[]{:S(2)}, u32[]{:S(2)}) collective-permute-start(bf16[256,512]{1,0:T(8,128)(2,1)S(1)} %collective-permute-done.7.refs_5_.refs_3_.refs_2_), channel_id=1, source_target_pairs={{0,16},{16,0},{1,17},{17,1},{2,18},{18,2},{3,19},{19,3},{4,20},{20... | collective-permute-start | bytes 786440 | tf_op jit(solution)/shard_map/ppermute | solution.py:448
  67.6 7.7 %collective-permute-start.9 = (bf16[256,512]{1,0:T(8,128)(2,1)S(1)}, bf16[256,512]{1,0:T(8,128)(2,1)S(1)}, u32[]{:S(2)}, u32[]{:S(2)}) collective-permute-start(bf16[256,512]{1,0:T(8,128)(2,1)S(1)} %collective-permute-done.7.refs_5_.refs_3_.refs_2_), channel_id=1, source_target_pairs={{0,4},{4,0},{8,12},{12,8},{1,5},{5,1},{9,13},{13,9},{2,6},{6,2},{1... | collective-permute-start | bytes 786440 | tf_op jit(solution)/shard_map/ppermute | solution.py:454
  67.7 11.9 %collective-permute-start.12 = (bf16[256,512]{1,0:T(8,128)(2,1)S(1)}, bf16[256,512]{1,0:T(8,128)(2,1)S(1)}, u32[]{:S(2)}, u32[]{:S(2)}) collective-permute-start(bf16[256,512]{1,0:T(8,128)(2,1)S(1)} %collective-permute-done.11.refs_9_.refs_7_.refs_6_), channel_id=1, source_target_pairs={{0,16},{16,0},{1,17},{17,1},{2,18},{18,2},{3,19},{19,3},{4,20},{20... | collective-permute-start | bytes 786440 | tf_op jit(solution)/shard_map/ppermute | solution.py:448
  75.3 4.2 %collective-permute-start.13 = (bf16[256,512]{1,0:T(8,128)(2,1)S(1)}, bf16[256,512]{1,0:T(8,128)(2,1)S(1)}, u32[]{:S(2)}, u32[]{:S(2)}) collective-permute-start(bf16[256,512]{1,0:T(8,128)(2,1)S(1)} %collective-permute-done.11.refs_9_.refs_7_.refs_6_), channel_id=1, source_target_pairs={{0,4},{4,0},{8,12},{12,8},{1,5},{5,1},{9,13},{13,9},{2,6},{6,2},{1... | collective-permute-start | bytes 786440 | tf_op jit(solution)/shard_map/ppermute | solution.py:454
  75.3 9.8 %collective-permute-start.16 = (bf16[256,512]{1,0:T(8,128)(2,1)S(1)}, bf16[256,512]{1,0:T(8,128)(2,1)S(1)}, u32[]{:S(2)}, u32[]{:S(2)}) collective-permute-start(bf16[256,512]{1,0:T(8,128)(2,1)S(1)} %collective-permute-done.15.refs_13_.refs_11_.refs_10_), channel_id=1, source_target_pairs={{0,16},{16,0},{1,17},{17,1},{2,18},{18,2},{3,19},{19,3},{4,20},{20... | collective-permute-start | bytes 786440 | tf_op jit(solution)/shard_map/ppermute | solution.py:448
  79.5 5.6 %collective-permute-start.17 = (bf16[256,512]{1,0:T(8,128)(2,1)S(1)}, bf16[256,512]{1,0:T(8,128)(2,1)S(1)}, u32[]{:S(2)}, u32[]{:S(2)}) collective-permute-start(bf16[256,512]{1,0:T(8,128)(2,1)S(1)} %collective-permute-done.15.refs_13_.refs_11_.refs_10_), channel_id=1, source_target_pairs={{0,4},{4,0},{8,12},{12,8},{1,5},{5,1},{9,13},{13,9},{2,6},{6,2},{1... | collective-permute-start | bytes 786440 | tf_op jit(solution)/shard_map/ppermute | solution.py:454
  79.5 11.2 %collective-permute-start.25 = (bf16[64,2048]{1,0:T(8,128)(2,1)S(1)}, bf16[64,2048]{1,0:T(8,128)(2,1)S(1)}, u32[]{:S(2)}, u32[]{:S(2)}) collective-permute-start(bf16[64,2048]{1,0:T(8,128)(2,1)S(1)} %collective-permute-done.24.refs_8_.refs_2_), channel_id=1, source_target_pairs={{0,16},{16,0},{1,17},{17,1},{2,18},{18,2},{3,19},{19,3},{4,20},{20... | collective-permute-start | bytes 786440 | tf_op jit(solution)/shard_map/ppermute | solution.py:448
  85.1 5.6 %collective-permute-start.26 = (bf16[64,2048]{1,0:T(8,128)(2,1)S(1)}, bf16[64,2048]{1,0:T(8,128)(2,1)S(1)}, u32[]{:S(2)}, u32[]{:S(2)}) collective-permute-start(bf16[64,2048]{1,0:T(8,128)(2,1)S(1)} %collective-permute-done.24.refs_8_.refs_2_), channel_id=1, source_target_pairs={{0,4},{4,0},{8,12},{12,8},{1,5},{5,1},{9,13},{13,9},{2,6},{6,2},{1... | collective-permute-start | bytes 786440 | tf_op jit(solution)/shard_map/ppermute | solution.py:454
  85.1 10.7 %collective-permute-start.29 = (bf16[64,2048]{1,0:T(8,128)(2,1)S(1)}, bf16[64,2048]{1,0:T(8,128)(2,1)S(1)}, u32[]{:S(2)}, u32[]{:S(2)}) collective-permute-start(bf16[64,2048]{1,0:T(8,128)(2,1)S(1)} %collective-permute-done.28.refs_12_.refs_6_), channel_id=1, source_target_pairs={{0,16},{16,0},{1,17},{17,1},{2,18},{18,2},{3,19},{19,3},{4,20},{20... | collective-permute-start | bytes 786440 | tf_op jit(solution)/shard_map/ppermute | solution.py:448
  90.8 6.8 %collective-permute-start.6 = (bf16[256,512]{1,0:T(8,128)(2,1)S(1)}, bf16[256,512]{1,0:T(8,128)(2,1)S(1)}, u32[]{:S(2)}, u32[]{:S(2)}) collective-permute-start(bf16[256,512]{1,0:T(8,128)(2,1)S(1)} %collective-permute-done.4.refs_6_.refs_16_.refs_15_), channel_id=1, source_target_pairs={{0,4},{4,0},{8,12},{12,8},{1,5},{5,1},{9,13},{13,9},{2,6},{6,2},{1... | collective-permute-start | bytes 786440 | tf_op jit(solution)/shard_map/ppermute | solution.py:454
  90.8 6.8 %collective-permute-start.10 = (bf16[256,512]{1,0:T(8,128)(2,1)S(1)}, bf16[256,512]{1,0:T(8,128)(2,1)S(1)}, u32[]{:S(2)}, u32[]{:S(2)}) collective-permute-start(bf16[256,512]{1,0:T(8,128)(2,1)S(1)} %collective-permute-done.8.refs_6_.refs_4_.refs_3_), channel_id=1, source_target_pairs={{0,4},{4,0},{8,12},{12,8},{1,5},{5,1},{9,13},{13,9},{2,6},{6,2},{1... | collective-permute-start | bytes 786440 | tf_op jit(solution)/shard_map/ppermute | solution.py:454
  95.8 13.4 %collective-permute-start.21 = (bf16[128,2048]{1,0:T(8,128)(2,1)S(1)}, bf16[128,2048]{1,0:T(8,128)(2,1)S(1)}, u32[]{:S(2)}, u32[]{:S(2)}) collective-permute-start(bf16[128,2048]{1,0:T(8,128)(2,1)S(1)} %collective-permute-done.1.refs_2_), channel_id=1, source_target_pairs={{0,1},{1,0},{2,3},{3,2},{4,5},{5,4},{6,7},{7,6},{8,9},{9,8},{10,11... | collective-permute-start | bytes 1572872 | tf_op jit(solution)/shard_map/ppermute | solution.py:457
  97.5 1.5 collective-permute-start.14
  97.5 1.9 %collective-permute-start.18 = (bf16[256,512]{1,0:T(8,128)(2,1)S(1)}, bf16[256,512]{1,0:T(8,128)(2,1)S(1)}, u32[]{:S(2)}, u32[]{:S(2)}) collective-permute-start(bf16[256,512]{1,0:T(8,128)(2,1)S(1)} %collective-permute-done.16.refs_14_.refs_12_.refs_11_), channel_id=1, source_target_pairs={{0,4},{4,0},{8,12},{12,8},{1,5},{5,1},{9,13},{13,9},{2,6},{6,2},{1... | collective-permute-start | bytes 786440 | tf_op jit(solution)/shard_map/ppermute | solution.py:454
  99.1 21.7 %collective-permute-start.30 = (bf16[64,2048]{1,0:T(8,128)(2,1)S(1)}, bf16[64,2048]{1,0:T(8,128)(2,1)S(1)}, u32[]{:S(2)}, u32[]{:S(2)}) collective-permute-start(bf16[64,2048]{1,0:T(8,128)(2,1)S(1)} %collective-permute-done.28.refs_12_.refs_6_), channel_id=1, source_target_pairs={{0,4},{4,0},{8,12},{12,8},{1,5},{5,1},{9,13},{13,9},{2,6},{6,2},{1... | collective-permute-start | bytes 786440 | tf_op jit(solution)/shard_map/ppermute | solution.py:454
  99.4 21.5 %collective-permute-start.35 = (bf16[64,2048]{1,0:T(8,128)(2,1)S(1)}, bf16[64,2048]{1,0:T(8,128)(2,1)S(1)}, u32[]{:S(2)}, u32[]{:S(2)}) collective-permute-start(bf16[64,2048]{1,0:T(8,128)(2,1)S(1)} %collective-permute-done.34.refs_8_.refs_10_), channel_id=1, source_target_pairs={{0,16},{16,0},{1,17},{17,1},{2,18},{18,2},{3,19},{19,3},{4,20},{20... | collective-permute-start | bytes 786440 | tf_op jit(solution)/shard_map/ppermute | solution.py:448
  109.2 12.1 %collective-permute-start.39 = (bf16[64,2048]{1,0:T(8,128)(2,1)S(1)}, bf16[64,2048]{1,0:T(8,128)(2,1)S(1)}, u32[]{:S(2)}, u32[]{:S(2)}) collective-permute-start(bf16[64,2048]{1,0:T(8,128)(2,1)S(1)} %collective-permute-done.38.refs_12_.refs_14_), channel_id=1, source_target_pairs={{0,16},{16,0},{1,17},{17,1},{2,18},{18,2},{3,19},{19,3},{4,20},{20... | collective-permute-start | bytes 786440 | tf_op jit(solution)/shard_map/ppermute | solution.py:448
  110.7 10.7 %collective-permute-start.27 = (bf16[64,2048]{1,0:T(8,128)(2,1)S(1)}, bf16[64,2048]{1,0:T(8,128)(2,1)S(1)}, u32[]{:S(2)}, u32[]{:S(2)}) collective-permute-start(bf16[64,2048]{1,0:T(8,128)(2,1)S(1)} %collective-permute-done.25.refs_9_.refs_3_), channel_id=1, source_target_pairs={{0,4},{4,0},{8,12},{12,8},{1,5},{5,1},{9,13},{13,9},{2,6},{6,2},{1... | collective-permute-start | bytes 786440 | tf_op jit(solution)/shard_map/ppermute | solution.py:454
  110.7 11.1 %collective-permute-start.31 = (bf16[64,2048]{1,0:T(8,128)(2,1)S(1)}, bf16[64,2048]{1,0:T(8,128)(2,1)S(1)}, u32[]{:S(2)}, u32[]{:S(2)}) collective-permute-start(bf16[64,2048]{1,0:T(8,128)(2,1)S(1)} %collective-permute-done.29.refs_13_.refs_7_), channel_id=1, source_target_pairs={{0,4},{4,0},{8,12},{12,8},{1,5},{5,1},{9,13},{13,9},{2,6},{6,2},{1... | collective-permute-start | bytes 786440 | tf_op jit(solution)/shard_map/ppermute | solution.py:454
  120.8 9.3 %collective-permute-start.36 = (bf16[64,2048]{1,0:T(8,128)(2,1)S(1)}, bf16[64,2048]{1,0:T(8,128)(2,1)S(1)}, u32[]{:S(2)}, u32[]{:S(2)}) collective-permute-start(bf16[64,2048]{1,0:T(8,128)(2,1)S(1)} %collective-permute-done.34.refs_8_.refs_10_), channel_id=1, source_target_pairs={{0,4},{4,0},{8,12},{12,8},{1,5},{5,1},{9,13},{13,9},{2,6},{6,2},{1... | collective-permute-start | bytes 786440 | tf_op jit(solution)/shard_map/ppermute | solution.py:454
  120.9 9.9 %collective-permute-start.40 = (bf16[64,2048]{1,0:T(8,128)(2,1)S(1)}, bf16[64,2048]{1,0:T(8,128)(2,1)S(1)}, u32[]{:S(2)}, u32[]{:S(2)}) collective-permute-start(bf16[64,2048]{1,0:T(8,128)(2,1)S(1)} %collective-permute-done.38.refs_12_.refs_14_), channel_id=1, source_target_pairs={{0,4},{4,0},{8,12},{12,8},{1,5},{5,1},{9,13},{13,9},{2,6},{6,2},{1... | collective-permute-start | bytes 786440 | tf_op jit(solution)/shard_map/ppermute | solution.py:454
  121.3 10.8 %collective-permute-start.37 = (bf16[64,2048]{1,0:T(8,128)(2,1)S(1)}, bf16[64,2048]{1,0:T(8,128)(2,1)S(1)}, u32[]{:S(2)}, u32[]{:S(2)}) collective-permute-start(bf16[64,2048]{1,0:T(8,128)(2,1)S(1)} %collective-permute-done.35.refs_9_.refs_11_), channel_id=1, source_target_pairs={{0,4},{4,0},{8,12},{12,8},{1,5},{5,1},{9,13},{13,9},{2,6},{6,2},{1... | collective-permute-start | bytes 786440 | tf_op jit(solution)/shard_map/ppermute | solution.py:454
  121.4 10.7 %collective-permute-start.41 = (bf16[64,2048]{1,0:T(8,128)(2,1)S(1)}, bf16[64,2048]{1,0:T(8,128)(2,1)S(1)}, u32[]{:S(2)}, u32[]{:S(2)}) collective-permute-start(bf16[64,2048]{1,0:T(8,128)(2,1)S(1)} %collective-permute-done.39.refs_13_.refs_15_), channel_id=1, source_target_pairs={{0,4},{4,0},{8,12},{12,8},{1,5},{5,1},{9,13},{13,9},{2,6},{6,2},{1... | collective-permute-start | bytes 786440 | tf_op jit(solution)/shard_map/ppermute | solution.py:454
  121.9 13.6 %collective-permute-start.22 = (bf16[128,1024]{1,0:T(8,128)(2,1)S(1)}, bf16[128,1024]{1,0:T(8,128)(2,1)S(1)}, u32[]{:S(2)}, u32[]{:S(2)}) collective-permute-start(bf16[128,1024]{1,0:T(8,128)(2,1)S(1)} %get-tuple-element.43), channel_id=1, source_target_pairs={{0,1},{1,0},{2,3},{3,2},{4,5},{5,4},{6,7},{7,6},{8,9},{9,8},{10,11... | collective-permute-start | bytes 786440 | tf_op jit(solution)/shard_map/ppermute | solution.py:457
  127.5 7.2 %copy-start = (bf16[128,1024]{1,0:T(8,128)(2,1)}, bf16[128,1024]{1,0:T(8,128)(2,1)S(1)}, u32[]{:S(2)}) copy-start(bf16[128,1024]{1,0:T(8,128)(2,1)S(1)} %get-tuple-element.40.refs_1_) | copy-start | bytes 786436
  130.0 30.5 %copy-start.1 = (bf16[128,512]{1,0:T(8,128)(2,1)}, bf16[128,512]{1,0:T(8,128)(2,1)S(1)}, u32[]{:S(2)}) copy-start(bf16[128,512]{1,0:T(8,128)(2,1)S(1)} %get-tuple-element.51.refs_4_) | copy-start | bytes 393220
  130.0 34.8 %collective-permute-start.20 = (bf16[128,1024]{1,0:T(8,128)(2,1)S(1)}, bf16[128,1024]{1,0:T(8,128)(2,1)S(1)}, u32[]{:S(2)}, u32[]{:S(2)}) collective-permute-start(bf16[128,1024]{1,0:T(8,128)(2,1)S(1)} %get-tuple-element.41), channel_id=1, source_target_pairs={{0,1},{1,0},{2,3},{3,2},{4,5},{5,4},{6,7},{7,6},{8,9},{9,8},{10,11... | collective-permute-start | bytes 786440 | tf_op jit(solution)/shard_map/ppermute | solution.py:457
  130.8 19.7 %collective-permute-start.32 = (bf16[256,512]{1,0:T(8,128)(2,1)S(1)}, bf16[256,512]{1,0:T(8,128)(2,1)S(1)}, u32[]{:S(2)}, u32[]{:S(2)}) collective-permute-start(bf16[256,512]{1,0:T(8,128)(2,1)S(1)} %get-tuple-element.52), channel_id=1, source_target_pairs={{0,1},{1,0},{2,3},{3,2},{4,5},{5,4},{6,7},{7,6},{8,9},{9,8},{10,11... | collective-permute-start | bytes 786440 | tf_op jit(solution)/shard_map/ppermute | solution.py:457
  134.7 25.9 %copy-start.2 = (bf16[128,512]{1,0:T(8,128)(2,1)}, bf16[128,512]{1,0:T(8,128)(2,1)S(1)}, u32[]{:S(2)}) copy-start(bf16[128,512]{1,0:T(8,128)(2,1)S(1)} %get-tuple-element.56.refs_7_) | copy-start | bytes 393220
  134.7 21.1 %collective-permute-start.42 = (bf16[256,512]{1,0:T(8,128)(2,1)S(1)}, bf16[256,512]{1,0:T(8,128)(2,1)S(1)}, u32[]{:S(2)}, u32[]{:S(2)}) collective-permute-start(bf16[256,512]{1,0:T(8,128)(2,1)S(1)} %get-tuple-element.57), channel_id=1, source_target_pairs={{0,1},{1,0},{2,3},{3,2},{4,5},{5,4},{6,7},{7,6},{8,9},{9,8},{10,11... | collective-permute-start | bytes 786440 | tf_op jit(solution)/shard_map/ppermute | solution.py:457
  135.6 32.8 %collective-permute-start.23 = (bf16[128,1024]{1,0:T(8,128)(2,1)S(1)}, bf16[128,1024]{1,0:T(8,128)(2,1)S(1)}, u32[]{:S(2)}, u32[]{:S(2)}) collective-permute-start(bf16[128,1024]{1,0:T(8,128)(2,1)S(1)} %add_convert_fusion), channel_id=1, source_target_pairs={{0,2},{1,3},{2,0},{3,1},{4,6},{5,7},{6,4},{7,5},{8,10},{9,11},{10,... | collective-permute-start | bytes 786440 | tf_op jit(solution)/shard_map/ppermute | solution.py:457
  150.5 10.1 %copy-start.3 = (bf16[256,512]{1,0:T(8,128)(2,1)}, bf16[256,512]{1,0:T(8,128)(2,1)S(1)}, u32[]{:S(2)}) copy-start(bf16[256,512]{1,0:T(8,128)(2,1)S(1)} %collective-permute-done.32.refs_5_) | copy-start | bytes 786436
  150.6 15.7 %collective-permute-start.33 = (bf16[128,512]{1,0:T(8,128)(2,1)S(1)}, bf16[128,512]{1,0:T(8,128)(2,1)S(1)}, u32[]{:S(2)}, u32[]{:S(2)}) collective-permute-start(bf16[128,512]{1,0:T(8,128)(2,1)S(1)} %add_convert_fusion.2), channel_id=1, source_target_pairs={{0,2},{1,3},{2,0},{3,1},{4,6},{5,7},{6,4},{7,5},{8,10},{9,11},{10,... | collective-permute-start | bytes 393224 | tf_op jit(solution)/shard_map/ppermute | solution.py:457
  155.8 12.5 %collective-permute-start.43 = (bf16[128,512]{1,0:T(8,128)(2,1)S(1)}, bf16[128,512]{1,0:T(8,128)(2,1)S(1)}, u32[]{:S(2)}, u32[]{:S(2)}) collective-permute-start(bf16[128,512]{1,0:T(8,128)(2,1)S(1)} %add_convert_fusion.1), channel_id=1, source_target_pairs={{0,2},{1,3},{2,0},{3,1},{4,6},{5,7},{6,4},{7,5},{8,10},{9,11},{10,... | collective-permute-start | bytes 393224 | tf_op jit(solution)/shard_map/ppermute | solution.py:457
  (5 other events, 11.7 us)

commit v3 on v2

--- a/solution.py
+++ b/solution.py
@@ -39,6 +39,10 @@
 
 def in_hbm(x):
     return pltpu.with_memory_space_constraint(x, pltpu.HBM)
+
+
+def in_vmem(x):
+    return pltpu.with_memory_space_constraint(x, pltpu.VMEM)
 
 
 def hbm_call(body, out_shape, args, **options):
@@ -283,7 +287,12 @@
     ]
     flops = 2 * n_tok * width * tile * nc
     if down_near:
-        out_shape += [jax.ShapeDtypeStruct((count, 2 * rows), BF) for _, count in cuts]
+        out_shape += [
+            pltpu.HBM((count, 2 * rows), BF)
+            if i == 1
+            else jax.ShapeDtypeStruct((count, 2 * rows), BF)
+            for i, (_, count) in enumerate(cuts)
+        ]
         scratch += [pltpu.VMEM((2 * rows, hid), BF), pltpu.VMEM((n_tok, 2 * rows), BF)]
         flops += 2 * n_tok * hid * 2 * rows
     args = list(blocks) + list(near)
@@ -303,14 +312,15 @@
     )
 
 
-def down_far_step(hiddens, groups, cuts, sub):
+def down_far_step(hiddens, groups, cuts, sub, before):
     hid = groups[0][0].shape[1]
     n_groups, nf = len(groups), len(groups[0])
     counts = [h[0].shape[0] for h in hiddens]
     n_tok = sum(counts)
     n_h = sum(len(h) for h in hiddens)
     cols = n_groups * nf * sub
-    n_in = n_h + n_groups * nf
+    ahead = 0 if before is None else before.shape[1]
+    n_in = n_h + n_groups * nf + (ahead > 0)
 
     def body(*refs):
         ins, outs = refs[:n_in], refs[n_in : n_in + len(cuts)]
@@ -334,24 +344,34 @@
             for a in place:
                 loads.append(go.start(ins[k], d.at[pl.ds(pl.multiple_of(a, 64), sub), :]))
                 k += 1
+        stores = []
+        if ahead:
+            stores.append(go.start(ins[k], outs[-1].at[:, :ahead]))
         wait_all(loads)
         o[...] = lax.dot_general(
             h[...], d[...], (((1,), (1,)), ((), ())), preferred_element_type=F32
         ).astype(BF)
-        stores = []
-        for out, runs in zip(outs, cuts):
+        for q, (out, runs) in enumerate(zip(outs, cuts)):
             r0 = 0
             for first, count in runs:
+                to = pl.ds(ahead if q == len(cuts) - 1 else 0, cols)
                 stores.append(
-                    go.start(o.at[first : first + count, :], out.at[r0 : r0 + count, :])
+                    go.start(o.at[first : first + count, :], out.at[r0 : r0 + count, to])
                 )
                 r0 += count
         wait_all(stores)
 
     return hbm_call(
         body,
-        tuple(jax.ShapeDtypeStruct((sum(c for _, c in runs), cols), BF) for runs in cuts),
-        [t for h in hiddens for t in h] + [p for g in groups for p in g],
+        tuple(
+            (pltpu.HBM if i == 1 else jax.ShapeDtypeStruct)(
+                (sum(c for _, c in runs), cols + (ahead if i == len(cuts) - 1 else 0)), BF
+            )
+            for i, runs in enumerate(cuts)
+        ),
+        [t for h in hiddens for t in h]
+        + [p for g in groups for p in g]
+        + ([before] if ahead else []),
         scratch_shapes=[
             pltpu.VMEM((n_tok, hid), BF),
             pltpu.VMEM((cols, hid), BF),
@@ -366,31 +386,41 @@
     )
 
 
-def assemble(near, far, shape, places):
-    pieces = list(near) + [p for g in far for p in g]
+def assemble(pieces, shape, places, base=None):
+    n = len(pieces)
 
     def body(*refs):
-        ins, out, buf, sems = refs[: len(pieces)], refs[len(pieces)], refs[-2], refs[-1]
+        ins, out, buf, sems = refs[:n], refs[-3], refs[-2], refs[-1]
         go = Copies(sems)
         spots = [
             (pl.ds(row, p.shape[0]), pl.ds(col, p.shape[1]))
             for p, (row, col) in zip(pieces, places())
         ]
-        loads = [go.start(ref, buf.at[spot]) for ref, spot in zip(ins, spots)]
+        spaces, at = [], 0
+        for p in pieces:
+            spaces.append(buf.at[at : at + p.shape[0], : p.shape[1]])
+            at += p.shape[0]
+        loads = [go.start(ref, space) for ref, space in zip(ins, spaces)]
         stores = []
-        for load, spot in zip(loads, spots):
+        for load, space, spot in zip(loads, spaces, spots):
             load.wait()
-            stores.append(go.start(buf.at[spot], out.at[spot]))
+            stores.append(go.start(space, out.at[spot]))
         wait_all(stores)
 
+    args = list(pieces) + ([base] if base is not None else [])
+    total = sum(p.shape[0] for p in pieces)
     return hbm_call(
         body,
         jax.ShapeDtypeStruct(shape, BF),
-        pieces,
-        scratch_shapes=[pltpu.VMEM(shape, BF), pltpu.SemaphoreType.DMA((2 * len(pieces),))],
+        args,
+        input_output_aliases={n: 0} if base is not None else {},
+        scratch_shapes=[
+            pltpu.VMEM((total, max(p.shape[1] for p in pieces)), BF),
+            pltpu.SemaphoreType.DMA((2 * n,)),
+        ],
         compiler_params=LIMIT,
         cost_estimate=pl.CostEstimate(
-            flops=10**9, bytes_accessed=4 * shape[0] * shape[1], transcendentals=0
+            flops=10**9, bytes_accessed=2 * shape[0] * shape[1], transcendentals=0
         ),
         name="assemble",
     )
@@ -400,47 +430,121 @@
     return (keep.astype(F32) + got.astype(F32)).astype(BF)
 
 
-def finish(near, far, post_gain, tok, rows):
+def before_last(near, far, post_gain, rows):
     width = 4 * rows
     terms = [near] + far
     flat = [a for t in terms for a in t]
+    tok = near[0].shape[0]
+    counts = [t[0].shape[1] for t in terms]
+    n_far = sum(counts[1:])
 
     def body(*refs):
-        gain, ins, o = refs[0], list(refs[1:-1]), refs[-1]
+        n_in = 1 + len(flat)
+        o, part, part_gain, power = refs[n_in : n_in + 4]
+        local, sems = refs[n_in + 4 : -1], refs[-1]
+        go = Copies(sems)
+        wait_all([go.start(a.at[: b.shape[0]], b) for a, b in zip(refs[:n_in], local)])
+        gain, ins = local[0], list(local[1:])
         sums = []
         for t in terms:
             group, ins = ins[: len(t)], ins[len(t) :]
-            sums.append(sum(g[:tok].astype(F32) for g in group))
-        power = sum(jnp.sum(s * s, axis=1, keepdims=True) for s in sums)
-        scale = lax.rsqrt(power / width + 1e-06)
-        y = here()[0]
-
-        def put(value, start):
-            to = pl.ds(pl.multiple_of(start, 128), value.shape[1])
-            o[:, to] = (value * scale * gain[:, to]).astype(BF)
-
-        put(sums[0], y * 2 * rows)
-        c0 = 0
+            sums.append(sum(g[...].astype(F32) for g in group))
+        total = jnp.sum(sums[0] * sums[0], axis=1, keepdims=True)
+        power[...] = jnp.broadcast_to(total, (tok, 128))
+        at = 0
         for s in sums[1:]:
-            n = s.shape[1] // 2
-            for c in range(2):
-                put(s[:, c * n : (c + 1) * n], (1 - y) * 2 * rows + c * rows + c0)
-            c0 += n
+            part[:, at : at + s.shape[1]] = s
+            at += s.shape[1]
+        for y in range(2):
+
+            @pl.when(here()[0] == y)
+            def _(y=y):
+                place = near_place(y, rows)
+                o[:, place] = sums[0] * gain[:, place]
+                for place, at, n in far_places(y, rows, counts[1:]):
+                    part_gain[:, at : at + n] = gain[:, place]
+
+    vm = pl.BlockSpec(memory_space=pltpu.VMEM)
+    return pl.pallas_call(
+        body,
+        out_shape=(
+            pltpu.VMEM((tok, width), F32),
+            pltpu.VMEM((tok, n_far), F32),
+            pltpu.VMEM((1, n_far), F32),
+            pltpu.VMEM((tok, 128), F32),
+        ),
+        in_specs=[ANY] * (1 + len(flat)),
+        out_specs=(vm,) * 4,
+        scratch_shapes=[pltpu.VMEM((1, width), F32)]
+        + [pltpu.VMEM((tok, a.shape[1]), BF) for a in flat]
+        + [pltpu.SemaphoreType.DMA((1 + len(flat),))],
+        name="before_last",
+    )(post_gain.reshape(1, width), *flat)
+
+
+def near_place(y, rows):
+    return slice(y * 2 * rows, (y + 1) * 2 * rows)
+
+
+def far_places(y, rows, counts):
+    found, at, before = [], 0, 0
+    for count in counts:
+        n = count // 2
+        for c in range(2):
+            start = (1 - y) * 2 * rows + c * rows + before
+            found.append((slice(start, start + n), at, n))
+            at += n
+        before += n
+    return found
+
+
+def finish(ready, part, part_gain, power, one, two, counts, rows):
+    tok, width = ready.shape
+    n_two = two.shape[1]
+
+    def body(r, p, g, w, a, b, out, v, o, sems):
+        v[...] = p[...] + a[...].astype(F32)
+        v[:, -n_two:] += b[...].astype(F32)
+        total = w[:, :1] + jnp.sum(v[...] * v[...], axis=1, keepdims=True)
+        scale = lax.rsqrt(total / width + 1e-06)
+        go = Copies(sems)
+        step = tok // 4
+        stores = []
+        for r0 in range(0, tok, step):
+            own = slice(r0, r0 + step)
+            for y in range(2):
+
+                @pl.when(here()[0] == y)
+                def _(y=y):
+                    place = near_place(y, rows)
+                    o[own, place] = (r[own, place] * scale[own]).astype(BF)
+                    for place, at, n in far_places(y, rows, counts):
+                        cols = slice(at, at + n)
+                        o[own, place] = (v[own, cols] * g[:, cols] * scale[own]).astype(BF)
+
+            stores.append(go.start(o.at[own, :], out.at[own, :]))
+        wait_all(stores)
 
     vm = pl.BlockSpec(memory_space=pltpu.VMEM)
     return pl.pallas_call(
         body,
         out_shape=jax.ShapeDtypeStruct((tok, width), BF),
-        in_specs=[vm] * (1 + len(flat)),
-        out_specs=vm,
+        in_specs=[vm] * 6,
+        out_specs=ANY,
+        scratch_shapes=[
+            pltpu.VMEM(part.shape, F32),
+            pltpu.VMEM((tok, width), BF),
+            pltpu.SemaphoreType.DMA((4,)),
+        ],
         name="finish",
-    )(post_gain.reshape(1, width), *flat)
+    )(*[in_vmem(a) for a in (ready, part, part_gain, power, one, two)])
 
 
 U_CUTS = 4
-D_CUTS = 4
+D_CUTS = 2
 LEAD = 3
-ROUNDS = ((0, 1), (2, 3))
+FIRST = 3
+ROUNDS = ((0,), (1,))
 
 
 def routed():
@@ -470,15 +574,21 @@
             return [got, part, near, core_swap(part)]
 
         gain = pre_gain.reshape(1, rows)
-        spots = [lambda i=i: (here()[2] * half, i * tile) for i in range(U_CUTS)]
+        tops = [lambda i=i: (here()[2] * half, i * tile) for i in range(U_CUTS)]
         block = (half, tile)
-        lead = cast(up_weight, gain, [block] * LEAD, lambda: [f() for f in spots[:LEAD]])
-        *_, r0 = cast(up_weight, None, [], lambda: [], prompt_tokens)
+        (lead,) = cast(up_weight, gain, [block], lambda: [tops[0]()])
+        *second, r0 = cast(
+            up_weight,
+            gain,
+            [block] * (LEAD - 1),
+            lambda: [f() for f in tops[1:LEAD]],
+            prompt_tokens,
+        )
         up_own, *rest = cast(
             up_weight,
             gain,
             [(rows, hid)] + [block] * (U_CUTS - LEAD),
-            lambda: [(0, 0)] + [f() for f in spots[LEAD:]],
+            lambda: [(0, 0)] + [f() for f in tops[LEAD:]],
         )
         down_own, *mine = cast(
             down_weight,
@@ -486,7 +596,7 @@
             [(rows, hid)] + [(sub, hid)] * D_CUTS,
             lambda: [(0, 0)] + [((2 * i + here()[2]) * sub, 0) for i in range(D_CUTS)],
         )
-        up_far = [exchange(v) for v in [*lead, *rest]]
+        up_far = [exchange(v) for v in [lead, *second, *rest]]
         down_far = [exchange(v) for v in mine]
         up_near = [up_own, core_swap(up_own)]
         down_near = [down_own, core_swap(down_own)]
@@ -497,45 +607,51 @@
 
         tiles = list(enumerate(up_far))
         cut = [(0, tok), (tok, tok), (2 * tok, tok)]
-        hidden = list(feed([r1, r0, r2], up_near, tiles[:-1], [], None, []))
-        last, send1, keep0, keep2 = feed([r1, r0, r2], up_near, tiles[-1:], hidden, down_near, cut)
-        hidden = hidden + [last]
+        hidden = list(feed([r1, r0, r2], up_near, tiles[:FIRST], [], None, []))
+        *last, send1, keep0, keep2 = feed(
+            [r1, r0, r2], up_near, tiles[FIRST:], hidden, down_near, cut
+        )
+        hidden = hidden + last
         got1 = tp_swap(send1, 1)
         *hidden3, send3 = feed([r3], up_near, tiles, [], down_near, cut[:1])
-        got3 = tp_swap(send3, 1)
-        pair = add_rows(keep2, got3)
-        near_terms = [keep0, got1, tp_swap(pair, 2)]
-
-        far_terms = []
-        cuts = [[cut[0], (3 * tok, tok)], [cut[1]], [cut[2]]]
+        near_terms = [keep0, got1, tp_swap(keep2, 2), tp_swap(send3, 3)]
+
+        far_terms, sent = [], None
+        cuts = [[(3 * tok, tok)], [cut[1]], [cut[2]], [cut[0]]]
         for ids in ROUNDS:
-            send, keep0, keep2 = down_far_step(
-                [hidden, hidden3], [down_far[g] for g in ids], cuts, sub
+            send3, keep0, keep2, sent = down_far_step(
+                [hidden, hidden3], [down_far[g] for g in ids], cuts, sub, sent
             )
-            got = tp_swap(send, 1)
-            pair = add_rows(keep2, got[tok:])
-            far_terms.append([keep0, got, tp_swap(pair, 2)])
+            got3 = tp_swap(send3, 1)
+            pair = add_rows(keep2, got3)
+            far_terms.append([keep0, tp_swap(pair, 2)])
+        one = tp_swap(sent, 1)
+        two = far_terms[-1].pop()
+        counts = [t[0].shape[1] for t in far_terms]
+        state = before_last(near_terms, far_terms, post_gain, rows)
+
+        def own_spots():
+            y, core, _ = here()
+            return [(pl.multiple_of((2 * y + c) * rows, 64), 0) for c in (core, 1 - core)]
 
         def up_spots():
-            at = up_places(rows, half)
-            spots = [(a, 0) for a in at[:2]]
-            return spots + [(a, i * tile) for i in range(U_CUTS) for a in at[2:]]
+            return [(a, i * tile) for i in range(U_CUTS) for a in up_places(rows, half)[2:]]
 
         def down_spots():
             y, core, grp = here()
-            spots = [((2 * y + c) * rows, 0) for c in (core, 1 - core)]
-            for i in range(D_CUTS):
-                spots += [
-                    ((2 * (1 - y) + c) * rows + (2 * i + side) * sub, 0)
-                    for c in (core, 1 - core)
-                    for side in (grp, 1 - grp)
-                ]
-            return [(pl.multiple_of(a, 64), c) for a, c in spots]
+            return [
+                (pl.multiple_of((2 * (1 - y) + c) * rows + (2 * i + side) * sub, 64), 0)
+                for i in range(D_CUTS)
+                for c in (core, 1 - core)
+                for side in (grp, 1 - grp)
+            ]
 
         shape = (4 * rows, hid)
-        whole_up = assemble(up_near, up_far, shape, up_spots)
-        whole_down = assemble(down_near, down_far, shape, down_spots)
-        mixed = finish(near_terms, far_terms, post_gain, tok, rows)
+        whole_up = assemble(up_near, shape, own_spots)
+        whole_up = assemble([p for g in up_far for p in g], shape, up_spots, whole_up)
+        whole_down = assemble(down_near, shape, own_spots)
+        whole_down = assemble([p for g in down_far for p in g], shape, down_spots, whole_down)
+        mixed = finish(*state, one, two, counts, rows)
         return mixed, whole_up, whole_down
 
     return per_device

time: 172 us -> 151 us (0.88)
  waiting for transfers between devices: 89 us -> 70.1 us
  starting transfers between devices: 40.7 us -> 36.4 us
  Pallas kernels: 40.2 us -> 42.4 us
    ppermute x8 -> x6, waiting for transfers between devices: 26.8 us -> 12.5 us  [y_swap(): return lax.ppermute(v, 'fs', [(i, i ^ 2) for i in range(4)])]
    ppermute x10 -> x11, waiting for transfers between devices: 38.4 us -> 30.1 us  [tp_swap(): return lax.ppermute(v, 'tp', [(i, i ^ m) for i in range(4)])]
    ppermute x8 -> x6, starting transfers between devices: 11.2 us -> 8.38 us  [y_swap(): return lax.ppermute(v, 'fs', [(i, i ^ 2) for i in range(4)])]
    ppermute x18 -> x14, waiting for transfers between devices: 1.3 us -> 3.73 us  [core_swap(): return lax.ppermute(v, 'fs', [(i, i ^ 1) for i in range(4)])]
    ppermute x8 -> x6, starting transfers between devices: 11 us -> 8.97 us  [grp_swap(): return lax.ppermute(v, 'grp', [(0, 1), (1, 0)])]
    pallas_call x11 -> x13, Pallas kernels: 37.6 us -> 39.6 us  [hbm_call(): pl.pallas_call(body, out_shape=out_shape, in_specs=[ANY] * len(args), out...]
    ppermute x8 -> x6, waiting for transfers between devices: 22.6 us -> 23.7 us  [grp_swap(): return lax.ppermute(v, 'grp', [(0, 1), (1, 0)])]
    ppermute x10 -> x11, starting transfers between devices: 15.7 us -> 16.8 us  [tp_swap(): return lax.ppermute(v, 'tp', [(i, i ^ m) for i in range(4)])]
  transfers between devices with their start and end apart: 44 -> 37, of which waited for: 20 -> 14; matrix products, arithmetic and copies ran while one was open for 0% -> 0% of each run, Pallas kernels for 20% -> 26%
where the time goes in v3:
time: 151 us
  waiting for transfers between devices  70.1 us (46%)
  Pallas kernels  42.4 us (28%)
  starting transfers between devices  36.4 us (24%)
    pallas_call x13, Pallas kernels, hbm_call(): pl.pallas_call(body, out_shape=out_shape, in_specs=[ANY] * len(args), out...  39.6 us
    ppermute x11, waiting for transfers between devices, tp_swap(): return lax.ppermute(v, 'tp', [(i, i ^ m) for i in range(4)])  30.1 us
    ppermute x6, waiting for transfers between devices, grp_swap(): return lax.ppermute(v, 'grp', [(0, 1), (1, 0)])  23.7 us
    ppermute x11, starting transfers between devices, tp_swap(): return lax.ppermute(v, 'tp', [(i, i ^ m) for i in range(4)])  16.8 us
    ppermute x6, waiting for transfers between devices, y_swap(): return lax.ppermute(v, 'fs', [(i, i ^ 2) for i in range(4)])  12.5 us
    ppermute x6, starting transfers between devices, grp_swap(): return lax.ppermute(v, 'grp', [(0, 1), (1, 0)])  8.97 us
    ppermute x6, starting transfers between devices, y_swap(): return lax.ppermute(v, 'fs', [(i, i ^ 2) for i in range(4)])  8.38 us
    ppermute x14, waiting for transfers between devices, core_swap(): return lax.ppermute(v, 'fs', [(i, i ^ 1) for i in range(4)])  3.73 us
  transfers between devices with their start and end apart: 37, of which 14 were waited for; matrix products, arithmetic and copies ran while one was open for 0% of the time, Pallas kernels for 26%

profile of v3, /device:TPU:0, one launch (start us, length us, event | category | flops | bytes accessed | tf_op | source)
XLA Modules:
  0.0 150.7 jit_solution(6627337331071804198)
XLA Ops:
  0.6 1.9 %cast.6 = bf16[256,512]{1,0:T(8,128)(2,1)S(1)} custom-call(f32[512,2048]{1,0:T(8,128)} %refs_0_.6, f32[1,512]{1,0:T(1,128)} %bitcast.2), custom_call_target="tpu_custom_call" | custom-call | flops 100000000 | bytes 6291456 | tf_op jit(solution)/shard_map/cast/pallas_call | solution.py:50
  2.5 3.1 %collective-permute-start.7 = (bf16[256,512]{1,0:T(8,128)(2,1)S(1)}, bf16[256,512]{1,0:T(8,128)(2,1)S(1)}, u32[]{:S(2)}, u32[]{:S(2)}) collective-permute-start(bf16[256,512]{1,0:T(8,128)(2,1)S(1)} %cast.6), channel_id=1, source_target_pairs={{0,8},{4,12},{8,0},{12,4},{1,9},{5,13},{9,1},{13,5},{2,10},{6,14},... | collective-permute-start | bytes 786440 | tf_op jit(solution)/shard_map/ppermute | solution.py:555
  5.6 3.0 %cast.4 = (bf16[256,512]{1,0:T(8,128)(2,1)S(1)}, bf16[256,512]{1,0:T(8,128)(2,1)S(1)}, bf16[128,2048]{1,0:T(8,128)(2,1)S(1)}) custom-call(f32[512,2048]{1,0:T(8,128)} %refs_0_.6, f32[1,512]{1,0:T(1,128)} %bitcast.3, bf16[128,2048]{1,0:T(8,128)(2,1)} %refs_2_.1), custom_call_target="tpu_custom_call" | custom-call | flops 100000000 | bytes 6291456 | tf_op jit(solution)/shard_map/cast/pallas_call | solution.py:50
  8.6 2.0 %collective-permute-start.15 = (bf16[256,512]{1,0:T(8,128)(2,1)S(1)}, bf16[256,512]{1,0:T(8,128)(2,1)S(1)}, u32[]{:S(2)}, u32[]{:S(2)}) collective-permute-start(bf16[256,512]{1,0:T(8,128)(2,1)S(1)} %get-tuple-element.39), channel_id=1, source_target_pairs={{0,8},{4,12},{8,0},{12,4},{1,9},{5,13},{9,1},{13,5},{2,10},{6,14},... | collective-permute-start | bytes 786440 | tf_op jit(solution)/shard_map/ppermute | solution.py:555
  10.6 2.8 %cast.5 = (bf16[512,2048]{1,0:T(8,128)(2,1)S(1)}, bf16[256,512]{1,0:T(8,128)(2,1)S(1)}) custom-call(f32[512,2048]{1,0:T(8,128)} %refs_0_.6, f32[1,512]{1,0:T(1,128)} %bitcast.4), custom_call_target="tpu_custom_call" | custom-call | flops 100000000 | bytes 6291456 | tf_op jit(solution)/shard_map/cast/pallas_call | solution.py:50
  13.6 1.9 %collective-permute-start.8 = (bf16[256,512]{1,0:T(8,128)(2,1)S(1)}, bf16[256,512]{1,0:T(8,128)(2,1)S(1)}, u32[]{:S(2)}, u32[]{:S(2)}) collective-permute-start(bf16[256,512]{1,0:T(8,128)(2,1)S(1)} %collective-permute-done.7.refs_5_.refs_3_.refs_0_), channel_id=1, source_target_pairs={{0,16},{16,0},{1,17},{17,1},{2,18},{18,2},{3,19},{19,3},{4,20},{20... | collective-permute-start | bytes 786440 | tf_op jit(solution)/shard_map/ppermute | solution.py:552
  15.5 2.9 %collective-permute-done.11.refs_9_.refs_7_.refs_4_ = bf16[256,512]{1,0:T(8,128)(2,1)S(1)} collective-permute-done((bf16[256,512]{1,0:T(8,128)(2,1)S(1)}, bf16[256,512]{1,0:T(8,128)(2,1)S(1)}, u32[]{:S(2)}, u32[]{:S(2)}) %collective-permute-start.11) | collective-permute-done | bytes 262176 | tf_op jit(solution)/shard_map/ppermute | solution.py:555
  18.3 5.6 %collective-permute-done.15.refs_13_.refs_11_.refs_8_ = bf16[256,512]{1,0:T(8,128)(2,1)S(1)} collective-permute-done((bf16[256,512]{1,0:T(8,128)(2,1)S(1)}, bf16[256,512]{1,0:T(8,128)(2,1)S(1)}, u32[]{:S(2)}, u32[]{:S(2)}) %collective-permute-start.15) | collective-permute-done | bytes 262176 | tf_op jit(solution)/shard_map/ppermute | solution.py:555
  23.9 2.0 %collective-permute-start.12 = (bf16[256,512]{1,0:T(8,128)(2,1)S(1)}, bf16[256,512]{1,0:T(8,128)(2,1)S(1)}, u32[]{:S(2)}, u32[]{:S(2)}) collective-permute-start(bf16[256,512]{1,0:T(8,128)(2,1)S(1)} %collective-permute-done.11.refs_9_.refs_7_.refs_4_), channel_id=1, source_target_pairs={{0,16},{16,0},{1,17},{17,1},{2,18},{18,2},{3,19},{19,3},{4,20},{20... | collective-permute-start | bytes 786440 | tf_op jit(solution)/shard_map/ppermute | solution.py:552
  25.9 2.7 %cast.7 = (bf16[512,2048]{1,0:T(8,128)(2,1)S(1)}, bf16[128,2048]{1,0:T(8,128)(2,1)S(1)}, bf16[128,2048]{1,0:T(8,128)(2,1)S(1)}) custom-call(f32[512,2048]{1,0:T(8,128)} %refs_0_.7), custom_call_target="tpu_custom_call" | custom-call | flops 100000000 | bytes 6291456 | tf_op jit(solution)/shard_map/cast/pallas_call | solution.py:50
  29.3 2.8 %collective-permute-start.1 = (bf16[128,2048]{1,0:T(8,128)(2,1)S(1)}, bf16[128,2048]{1,0:T(8,128)(2,1)S(1)}, u32[]{:S(2)}, u32[]{:S(2)}) collective-permute-start(bf16[128,2048]{1,0:T(8,128)(2,1)S(1)} %get-tuple-element.35.refs_1_), channel_id=1, source_target_pairs={{0,2},{1,3},{2,0},{3,1},{4,6},{5,7},{6,4},{7,5},{8,10},{9,11},{10,... | collective-permute-start | bytes 1572872 | tf_op jit(solution)/shard_map/ppermute | solution.py:561
  32.1 1.6 %collective-permute-start.16 = (bf16[256,512]{1,0:T(8,128)(2,1)S(1)}, bf16[256,512]{1,0:T(8,128)(2,1)S(1)}, u32[]{:S(2)}, u32[]{:S(2)}) collective-permute-start(bf16[256,512]{1,0:T(8,128)(2,1)S(1)} %collective-permute-done.15.refs_13_.refs_11_.refs_8_), channel_id=1, source_target_pairs={{0,16},{16,0},{1,17},{17,1},{2,18},{18,2},{3,19},{19,3},{4,20},{20... | collective-permute-start | bytes 786440 | tf_op jit(solution)/shard_map/ppermute | solution.py:552
  33.6 2.7 %collective-permute-done.17.refs_15_.refs_13_.refs_10_ = bf16[256,512]{1,0:T(8,128)(2,1)S(1)} collective-permute-done((bf16[256,512]{1,0:T(8,128)(2,1)S(1)}, bf16[256,512]{1,0:T(8,128)(2,1)S(1)}, u32[]{:S(2)}, u32[]{:S(2)}) %collective-permute-start.17) | collective-permute-done | bytes 262176 | tf_op jit(solution)/shard_map/ppermute | solution.py:558
  36.4 4.3 %collective-permute-done.16.refs_14_.refs_12_.refs_9_ = bf16[256,512]{1,0:T(8,128)(2,1)S(1)} collective-permute-done((bf16[256,512]{1,0:T(8,128)(2,1)S(1)}, bf16[256,512]{1,0:T(8,128)(2,1)S(1)}, u32[]{:S(2)}, u32[]{:S(2)}) %collective-permute-start.16) | collective-permute-done | bytes 262176 | tf_op jit(solution)/shard_map/ppermute | solution.py:552
  40.8 1.5 %collective-permute-start.24 = (bf16[128,2048]{1,0:T(8,128)(2,1)S(1)}, bf16[128,2048]{1,0:T(8,128)(2,1)S(1)}, u32[]{:S(2)}, u32[]{:S(2)}) collective-permute-start(bf16[128,2048]{1,0:T(8,128)(2,1)S(1)} %get-tuple-element.53), channel_id=1, source_target_pairs={{0,8},{4,12},{8,0},{12,4},{1,9},{5,13},{9,1},{13,5},{2,10},{6,14},... | collective-permute-start | bytes 1572872 | tf_op jit(solution)/shard_map/ppermute | solution.py:555
  42.3 13.1 %collective-permute-done.1.refs_2_ = bf16[128,2048]{1,0:T(8,128)(2,1)S(1)} collective-permute-done((bf16[128,2048]{1,0:T(8,128)(2,1)S(1)}, bf16[128,2048]{1,0:T(8,128)(2,1)S(1)}, u32[]{:S(2)}, u32[]{:S(2)}) %collective-permute-start.1) | collective-permute-done | bytes 524320 | tf_op jit(solution)/shard_map/ppermute | solution.py:561
  55.4 1.6 %collective-permute-start.30 = (bf16[128,2048]{1,0:T(8,128)(2,1)S(1)}, bf16[128,2048]{1,0:T(8,128)(2,1)S(1)}, u32[]{:S(2)}, u32[]{:S(2)}) collective-permute-start(bf16[128,2048]{1,0:T(8,128)(2,1)S(1)} %get-tuple-element.57), channel_id=1, source_target_pairs={{0,8},{4,12},{8,0},{12,4},{1,9},{5,13},{9,1},{13,5},{2,10},{6,14},... | collective-permute-start | bytes 1572872 | tf_op jit(solution)/shard_map/ppermute | solution.py:555
  57.0 1.5 collective-permute-start.4
  58.5 5.6 %collective-permute-done.4.refs_6_.refs_16_.refs_13_ = bf16[256,512]{1,0:T(8,128)(2,1)S(1)} collective-permute-done((bf16[256,512]{1,0:T(8,128)(2,1)S(1)}, bf16[256,512]{1,0:T(8,128)(2,1)S(1)}, u32[]{:S(2)}, u32[]{:S(2)}) %collective-permute-start.4) | collective-permute-done | bytes 262176 | tf_op jit(solution)/shard_map/ppermute | solution.py:552
  64.7 3.9 %collective-permute-done.30.refs_8_.refs_4_ = bf16[128,2048]{1,0:T(8,128)(2,1)S(1)} collective-permute-done((bf16[128,2048]{1,0:T(8,128)(2,1)S(1)}, bf16[128,2048]{1,0:T(8,128)(2,1)S(1)}, u32[]{:S(2)}, u32[]{:S(2)}) %collective-permute-start.30) | collective-permute-done | bytes 524320 | tf_op jit(solution)/shard_map/ppermute | solution.py:555
  68.6 1.4 collective-permute-start.22
  70.5 1.0 collective-permute-done.18.refs_16_.refs_14_.refs_11_
  71.6 1.5 collective-permute-start.25
  73.6 7.7 %collective-permute-done.22.refs_0_ = bf16[128,2048]{1,0:T(8,128)(2,1)S(1)} collective-permute-done((bf16[128,2048]{1,0:T(8,128)(2,1)S(1)}, bf16[128,2048]{1,0:T(8,128)(2,1)S(1)}, u32[]{:S(2)}, u32[]{:S(2)}) %collective-permute-start.22) | collective-permute-done | bytes 524320 | tf_op jit(solution)/shard_map/ppermute | solution.py:561
  81.3 1.7 %collective-permute-start = (bf16[128,2048]{1,0:T(8,128)(2,1)S(1)}, bf16[128,2048]{1,0:T(8,128)(2,1)S(1)}, u32[]{:S(2)}, u32[]{:S(2)}) collective-permute-start(bf16[128,2048]{1,0:T(8,128)(2,1)S(1)} %get-tuple-element.35.refs_1_), channel_id=1, source_target_pairs={{0,1},{1,0},{2,3},{3,2},{4,5},{5,4},{6,7},{7,6},{8,9},{9,8},{10,11... | collective-permute-start | bytes 1572872 | tf_op jit(solution)/shard_map/ppermute | solution.py:561
  83.0 3.3 %collective-permute-done.25.refs_9_.refs_1_ = bf16[128,2048]{1,0:T(8,128)(2,1)S(1)} collective-permute-done((bf16[128,2048]{1,0:T(8,128)(2,1)S(1)}, bf16[128,2048]{1,0:T(8,128)(2,1)S(1)}, u32[]{:S(2)}, u32[]{:S(2)}) %collective-permute-start.25) | collective-permute-done | bytes 524320 | tf_op jit(solution)/shard_map/ppermute | solution.py:552
  86.4 10.4 %collective-permute-done.31.refs_9_.refs_5_ = bf16[128,2048]{1,0:T(8,128)(2,1)S(1)} collective-permute-done((bf16[128,2048]{1,0:T(8,128)(2,1)S(1)}, bf16[128,2048]{1,0:T(8,128)(2,1)S(1)}, u32[]{:S(2)}, u32[]{:S(2)}) %collective-permute-start.31) | collective-permute-done | bytes 524320 | tf_op jit(solution)/shard_map/ppermute | solution.py:552
  97.3 5.3 %feed.5 = (bf16[128,512]{1,0:T(8,128)(2,1)S(1)}, bf16[128,512]{1,0:T(8,128)(2,1)S(1)}, bf16[128,512]{1,0:T(8,128)(2,1)S(1)}, bf16[128,512]{1,0:T(8,128)(2,1)S(1)}, bf16[128,1024]{1,0:T(8,128)(2,1)S(1)}) custom-call(bf16[128,2048]{1,0:T(8,128)(2,1)S(1)} %collective-permute-done.22.refs_0_, bf16[512,2048]{1,0:T(8,128)(2,1)S(1)} %get-tuple-element.36.refs_3_.refs_1_.refs_0_, ...), custom_call_target="tpu_custom_call" | custom-call | flops 1610612736 | bytes 8388608 | tf_op jit(solution)/shard_map/feed/pallas_call | solution.py:50
  102.7 2.9 %collective-permute-start.23 = (bf16[128,1024]{1,0:T(8,128)(2,1)S(1)}, bf16[128,1024]{1,0:T(8,128)(2,1)S(1)}, u32[]{:S(2)}, u32[]{:S(2)}) collective-permute-start(bf16[128,1024]{1,0:T(8,128)(2,1)S(1)} %get-tuple-element.47), channel_id=1, source_target_pairs={{0,3},{1,2},{2,1},{3,0},{4,7},{5,6},{6,5},{7,4},{8,11},{9,10},{10,... | collective-permute-start | bytes 786440 | tf_op jit(solution)/shard_map/ppermute | solution.py:561
  105.5 4.2 %feed.3 = (bf16[384,512]{1,0:T(8,128)(2,1)S(1)}, bf16[384,512]{1,0:T(8,128)(2,1)S(1)}, bf16[384,512]{1,0:T(8,128)(2,1)S(1)}) custom-call(bf16[128,2048]{1,0:T(8,128)(2,1)S(1)} %collective-permute-done.refs_0_, bf16[128,2048]{1,0:T(8,128)(2,1)S(1)} %get-tuple-element.35.refs_1_, bf16[128,2048]{1,0:T(8,128)(2,1)S(1)} %collective-permute-done.1.refs_2_, ...), custom_call_target="tpu_custom_call" | custom-call | flops 2415919104 | bytes 6291456 | tf_op jit(solution)/shard_map/feed/pallas_call | solution.py:50
  109.7 4.9 %feed.4 = (bf16[384,512]{1,0:T(8,128)(2,1)S(1)}, bf16[128,1024]{1,0:T(8,128)(2,1)S(1)}, bf16[128,1024]{1,0:T(8,128)(2,1)}, bf16[128,1024]{1,0:T(8,128)(2,1)S(1)}) custom-call(bf16[128,2048]{1,0:T(8,128)(2,1)S(1)} %collective-permute-done.refs_0_, bf16[128,2048]{1,0:T(8,128)(2,1)S(1)} %get-tuple-element.35.refs_1_, ...), custom_call_target="tpu_custom_call" | custom-call | flops 2415919104 | bytes 2097152 | tf_op jit(solution)/shard_map/feed/pallas_call | solution.py:50
  114.7 1.2 collective-permute-start.20
  116.3 2.6 %down_far.2 = (bf16[128,512]{1,0:T(8,128)(2,1)S(1)}, bf16[128,512]{1,0:T(8,128)(2,1)}, bf16[128,512]{1,0:T(8,128)(2,1)S(1)}, bf16[128,512]{1,0:T(8,128)(2,1)S(1)}) custom-call(bf16[384,512]{1,0:T(8,128)(2,1)S(1)} %get-tuple-element.40.refs_9_.refs_0_, bf16[384,512]{1,0:T(8,128)(2,1)S(1)} %get-tuple-element.41.refs_10_.refs_1_, ...), custom_call_target="tpu_custom_call" | custom-call | flops 1073741824 | bytes 2097152 | tf_op jit(solution)/shard_map/down_far/pallas_call | solution.py:50
  118.9 1.1 collective-permute-start.28
  120.1 2.6 %down_far.3 = (bf16[128,512]{1,0:T(8,128)(2,1)S(1)}, bf16[128,512]{1,0:T(8,128)(2,1)}, bf16[128,512]{1,0:T(8,128)(2,1)S(1)}, bf16[128,1024]{1,0:T(8,128)(2,1)S(1)}) custom-call(bf16[384,512]{1,0:T(8,128)(2,1)S(1)} %get-tuple-element.40.refs_9_.refs_0_, bf16[384,512]{1,0:T(8,128)(2,1)S(1)} %get-tuple-element.41.refs_10_.refs_1_, ...), custom_call_target="tpu_custom_call" | custom-call | flops 1073741824 | bytes 2097152 | tf_op jit(solution)/shard_map/down_far/pallas_call | solution.py:50
  122.7 1.0 collective-permute-start.35
  123.7 2.3 %assemble.6.refs_8_ = bf16[2048,2048]{1,0:T(8,128)(2,1)} custom-call(bf16[512,2048]{1,0:T(8,128)(2,1)S(1)} %get-tuple-element.43.refs_12_.refs_19_.refs_0_, bf16[512,2048]{1,0:T(8,128)(2,1)S(1)} %collective-permute-done.19.refs_13_.refs_20_.refs_1_), custom_call_target="tpu_custom_call" | custom-call | flops 1000000000 | bytes 8388608 | tf_op jit(solution)/shard_map/assemble/pallas_call | solution.py:50
  126.1 2.3 %assemble.4.refs_16_ = bf16[2048,2048]{1,0:T(8,128)(2,1)} custom-call(bf16[512,2048]{1,0:T(8,128)(2,1)S(1)} %get-tuple-element.36.refs_3_.refs_1_.refs_0_, bf16[512,2048]{1,0:T(8,128)(2,1)S(1)} %collective-permute-done.2.refs_4_.refs_2_.refs_1_), custom_call_target="tpu_custom_call" | custom-call | flops 1000000000 | bytes 8388608 | tf_op jit(solution)/shard_map/assemble/pallas_call | solution.py:50
  128.4 3.9 %collective-permute-done.28 = bf16[128,512]{1,0:T(8,128)(2,1)S(1)} collective-permute-done((bf16[128,512]{1,0:T(8,128)(2,1)S(1)}, bf16[128,512]{1,0:T(8,128)(2,1)S(1)}, u32[]{:S(2)}, u32[]{:S(2)}) %collective-permute-start.28) | collective-permute-done | bytes 131104 | tf_op jit(solution)/shard_map/ppermute | solution.py:561
  132.4 1.2 collective-permute-start.34
  133.6 1.6 %collective-permute-done.35 = bf16[128,512]{1,0:T(8,128)(2,1)S(1)} collective-permute-done((bf16[128,512]{1,0:T(8,128)(2,1)S(1)}, bf16[128,512]{1,0:T(8,128)(2,1)S(1)}, u32[]{:S(2)}, u32[]{:S(2)}) %collective-permute-start.35) | collective-permute-done | bytes 131104 | tf_op jit(solution)/shard_map/ppermute | solution.py:561
  135.9 2.4 %collective-permute-start.36 = (bf16[128,512]{1,0:T(8,128)(2,1)S(1)}, bf16[128,512]{1,0:T(8,128)(2,1)S(1)}, u32[]{:S(2)}, u32[]{:S(2)}) collective-permute-start(bf16[128,512]{1,0:T(8,128)(2,1)S(1)} %add_convert_fusion), channel_id=1, source_target_pairs={{0,2},{1,3},{2,0},{3,1},{4,6},{5,7},{6,4},{7,5},{8,10},{9,11},{10,... | collective-permute-start | bytes 393224 | tf_op jit(solution)/shard_map/ppermute | solution.py:561
  138.2 2.4 %assemble.7 = bf16[2048,2048]{1,0:T(8,128)(2,1)} custom-call(bf16[128,2048]{1,0:T(8,128)(2,1)S(1)} %collective-permute-done.24.refs_8_.refs_0_, bf16[128,2048]{1,0:T(8,128)(2,1)S(1)} %collective-permute-done.25.refs_9_.refs_1_, bf16[128,2048]{1,0:T(8,128)(2,1)S(1)} %collective-permute-done.26.refs_10_.refs_2_, ...), custom_call_target="tpu_custom_call", output_to_operand_aliasing={{}: (8, {})} | custom-call | flops 1000000000 | bytes 8388608 | tf_op jit(solution)/shard_map/assemble/pallas_call | solution.py:50
  140.7 2.6 %assemble.5 = bf16[2048,2048]{1,0:T(8,128)(2,1)} custom-call(bf16[256,512]{1,0:T(8,128)(2,1)S(1)} %collective-permute-done.7.refs_5_.refs_3_.refs_0_, bf16[256,512]{1,0:T(8,128)(2,1)S(1)} %collective-permute-done.8.refs_6_.refs_4_.refs_1_, bf16[256,512]{1,0:T(8,128)(2,1)S(1)} %collective-permute-done.9.refs_7_.refs_5_.refs_2_, ...), custom_call_target="tpu_custom_call", output_to_operand_aliasing={{}: (16, {})} | custom-call | flops 1000000000 | bytes 8388608 | tf_op jit(solution)/shard_map/assemble/pallas_call | solution.py:50
  143.3 3.7 %collective-permute-done.29.refs_6_ = bf16[128,512]{1,0:T(8,128)(2,1)S(1)} collective-permute-done((bf16[128,512]{1,0:T(8,128)(2,1)S(1)}, bf16[128,512]{1,0:T(8,128)(2,1)S(1)}, u32[]{:S(2)}, u32[]{:S(2)}) %collective-permute-start.29) | collective-permute-done | bytes 131104 | tf_op jit(solution)/shard_map/ppermute | solution.py:561
  147.0 0.7 copy-done.3
  147.7 1.7 %before_last.1 = (f32[128,2048]{1,0:T(8,128)S(1)}, f32[128,1024]{1,0:T(8,128)S(1)}, f32[1,1024]{1,0:T(1,128)S(1)}, f32[128,128]{1,0:T(8,128)S(1)}) custom-call(f32[1,2048]{1,0:T(1,128)} %bitcast.5, bf16[128,1024]{1,0:T(8,128)(2,1)} %get-tuple-element.44.refs_1_, bf16[128,1024]{1,0:T(8,128)(2,1)} %copy-done.1, bf16[128,1024]{1,0:T(8,128)(2,1)} %copy-done.2, ...), custom_call_target="tpu_custom_call" | custom-call | tf_op jit(solution)/shard_map/before_last/pallas_call | solution.py:468
  149.4 1.1 finish.1
  (51 shorter events, 4.3 us)
Async XLA Ops:
  2.5 11.0 %collective-permute-start.7 = (bf16[256,512]{1,0:T(8,128)(2,1)S(1)}, bf16[256,512]{1,0:T(8,128)(2,1)S(1)}, u32[]{:S(2)}, u32[]{:S(2)}) collective-permute-start(bf16[256,512]{1,0:T(8,128)(2,1)S(1)} %cast.6), channel_id=1, source_target_pairs={{0,8},{4,12},{8,0},{12,4},{1,9},{5,13},{9,1},{13,5},{2,10},{6,14},... | collective-permute-start | bytes 786440 | tf_op jit(solution)/shard_map/ppermute | solution.py:555
  8.5 9.8 %collective-permute-start.11 = (bf16[256,512]{1,0:T(8,128)(2,1)S(1)}, bf16[256,512]{1,0:T(8,128)(2,1)S(1)}, u32[]{:S(2)}, u32[]{:S(2)}) collective-permute-start(bf16[256,512]{1,0:T(8,128)(2,1)S(1)} %get-tuple-element.38), channel_id=1, source_target_pairs={{0,8},{4,12},{8,0},{12,4},{1,9},{5,13},{9,1},{13,5},{2,10},{6,14},... | collective-permute-start | bytes 786440 | tf_op jit(solution)/shard_map/ppermute | solution.py:555
  8.6 15.3 %collective-permute-start.15 = (bf16[256,512]{1,0:T(8,128)(2,1)S(1)}, bf16[256,512]{1,0:T(8,128)(2,1)S(1)}, u32[]{:S(2)}, u32[]{:S(2)}) collective-permute-start(bf16[256,512]{1,0:T(8,128)(2,1)S(1)} %get-tuple-element.39), channel_id=1, source_target_pairs={{0,8},{4,12},{8,0},{12,4},{1,9},{5,13},{9,1},{13,5},{2,10},{6,14},... | collective-permute-start | bytes 786440 | tf_op jit(solution)/shard_map/ppermute | solution.py:555
  13.4 15.3 %collective-permute-start.3 = (bf16[256,512]{1,0:T(8,128)(2,1)S(1)}, bf16[256,512]{1,0:T(8,128)(2,1)S(1)}, u32[]{:S(2)}, u32[]{:S(2)}) collective-permute-start(bf16[256,512]{1,0:T(8,128)(2,1)S(1)} %get-tuple-element.37), channel_id=1, source_target_pairs={{0,8},{4,12},{8,0},{12,4},{1,9},{5,13},{9,1},{13,5},{2,10},{6,14},... | collective-permute-start | bytes 786440 | tf_op jit(solution)/shard_map/ppermute | solution.py:555
  13.5 15.2 %collective-permute-start.9 = (bf16[256,512]{1,0:T(8,128)(2,1)S(1)}, bf16[256,512]{1,0:T(8,128)(2,1)S(1)}, u32[]{:S(2)}, u32[]{:S(2)}) collective-permute-start(bf16[256,512]{1,0:T(8,128)(2,1)S(1)} %collective-permute-done.7.refs_5_.refs_3_.refs_0_), channel_id=1, source_target_pairs={{0,4},{4,0},{8,12},{12,8},{1,5},{5,1},{9,13},{13,9},{2,6},{6,2},{1... | collective-permute-start | bytes 786440 | tf_op jit(solution)/shard_map/ppermute | solution.py:558
  13.6 15.7 %collective-permute-start.8 = (bf16[256,512]{1,0:T(8,128)(2,1)S(1)}, bf16[256,512]{1,0:T(8,128)(2,1)S(1)}, u32[]{:S(2)}, u32[]{:S(2)}) collective-permute-start(bf16[256,512]{1,0:T(8,128)(2,1)S(1)} %collective-permute-done.7.refs_5_.refs_3_.refs_0_), channel_id=1, source_target_pairs={{0,16},{16,0},{1,17},{17,1},{2,18},{18,2},{3,19},{19,3},{4,20},{20... | collective-permute-start | bytes 786440 | tf_op jit(solution)/shard_map/ppermute | solution.py:552
  18.3 13.7 %collective-permute-start.13 = (bf16[256,512]{1,0:T(8,128)(2,1)S(1)}, bf16[256,512]{1,0:T(8,128)(2,1)S(1)}, u32[]{:S(2)}, u32[]{:S(2)}) collective-permute-start(bf16[256,512]{1,0:T(8,128)(2,1)S(1)} %collective-permute-done.11.refs_9_.refs_7_.refs_4_), channel_id=1, source_target_pairs={{0,4},{4,0},{8,12},{12,8},{1,5},{5,1},{9,13},{13,9},{2,6},{6,2},{1... | collective-permute-start | bytes 786440 | tf_op jit(solution)/shard_map/ppermute | solution.py:558
  23.9 8.1 %collective-permute-start.12 = (bf16[256,512]{1,0:T(8,128)(2,1)S(1)}, bf16[256,512]{1,0:T(8,128)(2,1)S(1)}, u32[]{:S(2)}, u32[]{:S(2)}) collective-permute-start(bf16[256,512]{1,0:T(8,128)(2,1)S(1)} %collective-permute-done.11.refs_9_.refs_7_.refs_4_), channel_id=1, source_target_pairs={{0,16},{16,0},{1,17},{17,1},{2,18},{18,2},{3,19},{19,3},{4,20},{20... | collective-permute-start | bytes 786440 | tf_op jit(solution)/shard_map/ppermute | solution.py:552
  28.7 68.0 %collective-permute-start.2 = (bf16[512,2048]{1,0:T(8,128)(2,1)S(1)}, bf16[512,2048]{1,0:T(8,128)(2,1)S(1)}, u32[]{:S(2)}, u32[]{:S(2)}) collective-permute-start(bf16[512,2048]{1,0:T(8,128)(2,1)S(1)} %get-tuple-element.36.refs_3_.refs_1_.refs_0_), channel_id=1, source_target_pairs={{0,4},{4,0},{8,12},{12,8},{1,5},{5,1},{9,13},{13,9},{2,6},{6,2},{1... | collective-permute-start | bytes 6291464 | tf_op jit(solution)/shard_map/ppermute | solution.py:558
  28.8 68.5 %collective-permute-start.19 = (bf16[512,2048]{1,0:T(8,128)(2,1)S(1)}, bf16[512,2048]{1,0:T(8,128)(2,1)S(1)}, u32[]{:S(2)}, u32[]{:S(2)}) collective-permute-start(bf16[512,2048]{1,0:T(8,128)(2,1)S(1)} %get-tuple-element.43.refs_12_.refs_19_.refs_0_), channel_id=1, source_target_pairs={{0,4},{4,0},{8,12},{12,8},{1,5},{5,1},{9,13},{13,9},{2,6},{6,2},{1... | collective-permute-start | bytes 6291464 | tf_op jit(solution)/shard_map/ppermute | solution.py:558
  29.3 26.2 %collective-permute-start.1 = (bf16[128,2048]{1,0:T(8,128)(2,1)S(1)}, bf16[128,2048]{1,0:T(8,128)(2,1)S(1)}, u32[]{:S(2)}, u32[]{:S(2)}) collective-permute-start(bf16[128,2048]{1,0:T(8,128)(2,1)S(1)} %get-tuple-element.35.refs_1_), channel_id=1, source_target_pairs={{0,2},{1,3},{2,0},{3,1},{4,6},{5,7},{6,4},{7,5},{8,10},{9,11},{10,... | collective-permute-start | bytes 1572872 | tf_op jit(solution)/shard_map/ppermute | solution.py:561
  32.0 4.2 %collective-permute-start.17 = (bf16[256,512]{1,0:T(8,128)(2,1)S(1)}, bf16[256,512]{1,0:T(8,128)(2,1)S(1)}, u32[]{:S(2)}, u32[]{:S(2)}) collective-permute-start(bf16[256,512]{1,0:T(8,128)(2,1)S(1)} %collective-permute-done.15.refs_13_.refs_11_.refs_8_), channel_id=1, source_target_pairs={{0,4},{4,0},{8,12},{12,8},{1,5},{5,1},{9,13},{13,9},{2,6},{6,2},{1... | collective-permute-start | bytes 786440 | tf_op jit(solution)/shard_map/ppermute | solution.py:558
  32.1 8.7 %collective-permute-start.16 = (bf16[256,512]{1,0:T(8,128)(2,1)S(1)}, bf16[256,512]{1,0:T(8,128)(2,1)S(1)}, u32[]{:S(2)}, u32[]{:S(2)}) collective-permute-start(bf16[256,512]{1,0:T(8,128)(2,1)S(1)} %collective-permute-done.15.refs_13_.refs_11_.refs_8_), channel_id=1, source_target_pairs={{0,16},{16,0},{1,17},{17,1},{2,18},{18,2},{3,19},{19,3},{4,20},{20... | collective-permute-start | bytes 786440 | tf_op jit(solution)/shard_map/ppermute | solution.py:552
  36.3 20.7 %collective-permute-start.5 = (bf16[256,512]{1,0:T(8,128)(2,1)S(1)}, bf16[256,512]{1,0:T(8,128)(2,1)S(1)}, u32[]{:S(2)}, u32[]{:S(2)}) collective-permute-start(bf16[256,512]{1,0:T(8,128)(2,1)S(1)} %collective-permute-done.3.refs_5_.refs_15_.refs_12_), channel_id=1, source_target_pairs={{0,4},{4,0},{8,12},{12,8},{1,5},{5,1},{9,13},{13,9},{2,6},{6,2},{1... | collective-permute-start | bytes 786440 | tf_op jit(solution)/shard_map/ppermute | solution.py:558
  40.8 23.4 %collective-permute-start.24 = (bf16[128,2048]{1,0:T(8,128)(2,1)S(1)}, bf16[128,2048]{1,0:T(8,128)(2,1)S(1)}, u32[]{:S(2)}, u32[]{:S(2)}) collective-permute-start(bf16[128,2048]{1,0:T(8,128)(2,1)S(1)} %get-tuple-element.53), channel_id=1, source_target_pairs={{0,8},{4,12},{8,0},{12,4},{1,9},{5,13},{9,1},{13,5},{2,10},{6,14},... | collective-permute-start | bytes 1572872 | tf_op jit(solution)/shard_map/ppermute | solution.py:555
  55.4 13.2 %collective-permute-start.30 = (bf16[128,2048]{1,0:T(8,128)(2,1)S(1)}, bf16[128,2048]{1,0:T(8,128)(2,1)S(1)}, u32[]{:S(2)}, u32[]{:S(2)}) collective-permute-start(bf16[128,2048]{1,0:T(8,128)(2,1)S(1)} %get-tuple-element.57), channel_id=1, source_target_pairs={{0,8},{4,12},{8,0},{12,4},{1,9},{5,13},{9,1},{13,5},{2,10},{6,14},... | collective-permute-start | bytes 1572872 | tf_op jit(solution)/shard_map/ppermute | solution.py:555
  57.0 7.1 %collective-permute-start.4 = (bf16[256,512]{1,0:T(8,128)(2,1)S(1)}, bf16[256,512]{1,0:T(8,128)(2,1)S(1)}, u32[]{:S(2)}, u32[]{:S(2)}) collective-permute-start(bf16[256,512]{1,0:T(8,128)(2,1)S(1)} %collective-permute-done.3.refs_5_.refs_15_.refs_12_), channel_id=1, source_target_pairs={{0,16},{16,0},{1,17},{17,1},{2,18},{18,2},{3,19},{19,3},{4,20},{20... | collective-permute-start | bytes 786440 | tf_op jit(solution)/shard_map/ppermute | solution.py:552
  64.2 5.9 %collective-permute-start.10 = (bf16[256,512]{1,0:T(8,128)(2,1)S(1)}, bf16[256,512]{1,0:T(8,128)(2,1)S(1)}, u32[]{:S(2)}, u32[]{:S(2)}) collective-permute-start(bf16[256,512]{1,0:T(8,128)(2,1)S(1)} %collective-permute-done.8.refs_6_.refs_4_.refs_1_), channel_id=1, source_target_pairs={{0,4},{4,0},{8,12},{12,8},{1,5},{5,1},{9,13},{13,9},{2,6},{6,2},{1... | collective-permute-start | bytes 786440 | tf_op jit(solution)/shard_map/ppermute | solution.py:558
  64.2 5.9 %collective-permute-start.14 = (bf16[256,512]{1,0:T(8,128)(2,1)S(1)}, bf16[256,512]{1,0:T(8,128)(2,1)S(1)}, u32[]{:S(2)}, u32[]{:S(2)}) collective-permute-start(bf16[256,512]{1,0:T(8,128)(2,1)S(1)} %collective-permute-done.12.refs_10_.refs_8_.refs_5_), channel_id=1, source_target_pairs={{0,4},{4,0},{8,12},{12,8},{1,5},{5,1},{9,13},{13,9},{2,6},{6,2},{1... | collective-permute-start | bytes 786440 | tf_op jit(solution)/shard_map/ppermute | solution.py:558
  68.6 12.7 %collective-permute-start.22 = (bf16[128,2048]{1,0:T(8,128)(2,1)S(1)}, bf16[128,2048]{1,0:T(8,128)(2,1)S(1)}, u32[]{:S(2)}, u32[]{:S(2)}) collective-permute-start(bf16[128,2048]{1,0:T(8,128)(2,1)S(1)} %collective-permute-done.1.refs_2_), channel_id=1, source_target_pairs={{0,1},{1,0},{2,3},{3,2},{4,5},{5,4},{6,7},{7,6},{8,9},{9,8},{10,11... | collective-permute-start | bytes 1572872 | tf_op jit(solution)/shard_map/ppermute | solution.py:561
  70.0 1.5 %collective-permute-start.18 = (bf16[256,512]{1,0:T(8,128)(2,1)S(1)}, bf16[256,512]{1,0:T(8,128)(2,1)S(1)}, u32[]{:S(2)}, u32[]{:S(2)}) collective-permute-start(bf16[256,512]{1,0:T(8,128)(2,1)S(1)} %collective-permute-done.16.refs_14_.refs_12_.refs_9_), channel_id=1, source_target_pairs={{0,4},{4,0},{8,12},{12,8},{1,5},{5,1},{9,13},{13,9},{2,6},{6,2},{1... | collective-permute-start | bytes 786440 | tf_op jit(solution)/shard_map/ppermute | solution.py:558
  70.0 3.0 %collective-permute-start.6 = (bf16[256,512]{1,0:T(8,128)(2,1)S(1)}, bf16[256,512]{1,0:T(8,128)(2,1)S(1)}, u32[]{:S(2)}, u32[]{:S(2)}) collective-permute-start(bf16[256,512]{1,0:T(8,128)(2,1)S(1)} %collective-permute-done.4.refs_6_.refs_16_.refs_13_), channel_id=1, source_target_pairs={{0,4},{4,0},{8,12},{12,8},{1,5},{5,1},{9,13},{13,9},{2,6},{6,2},{1... | collective-permute-start | bytes 786440 | tf_op jit(solution)/shard_map/ppermute | solution.py:558
  71.6 14.8 %collective-permute-start.25 = (bf16[128,2048]{1,0:T(8,128)(2,1)S(1)}, bf16[128,2048]{1,0:T(8,128)(2,1)S(1)}, u32[]{:S(2)}, u32[]{:S(2)}) collective-permute-start(bf16[128,2048]{1,0:T(8,128)(2,1)S(1)} %collective-permute-done.24.refs_8_.refs_0_), channel_id=1, source_target_pairs={{0,16},{16,0},{1,17},{17,1},{2,18},{18,2},{3,19},{19,3},{4,20},{20... | collective-permute-start | bytes 1572872 | tf_op jit(solution)/shard_map/ppermute | solution.py:552
  73.1 23.7 %collective-permute-start.31 = (bf16[128,2048]{1,0:T(8,128)(2,1)S(1)}, bf16[128,2048]{1,0:T(8,128)(2,1)S(1)}, u32[]{:S(2)}, u32[]{:S(2)}) collective-permute-start(bf16[128,2048]{1,0:T(8,128)(2,1)S(1)} %collective-permute-done.30.refs_8_.refs_4_), channel_id=1, source_target_pairs={{0,16},{16,0},{1,17},{17,1},{2,18},{18,2},{3,19},{19,3},{4,20},{20... | collective-permute-start | bytes 1572872 | tf_op jit(solution)/shard_map/ppermute | solution.py:552
  81.3 21.4 %collective-permute-start = (bf16[128,2048]{1,0:T(8,128)(2,1)S(1)}, bf16[128,2048]{1,0:T(8,128)(2,1)S(1)}, u32[]{:S(2)}, u32[]{:S(2)}) collective-permute-start(bf16[128,2048]{1,0:T(8,128)(2,1)S(1)} %get-tuple-element.35.refs_1_), channel_id=1, source_target_pairs={{0,1},{1,0},{2,3},{3,2},{4,5},{5,4},{6,7},{7,6},{8,9},{9,8},{10,11... | collective-permute-start | bytes 1572872 | tf_op jit(solution)/shard_map/ppermute | solution.py:561
  86.4 28.3 %collective-permute-start.26 = (bf16[128,2048]{1,0:T(8,128)(2,1)S(1)}, bf16[128,2048]{1,0:T(8,128)(2,1)S(1)}, u32[]{:S(2)}, u32[]{:S(2)}) collective-permute-start(bf16[128,2048]{1,0:T(8,128)(2,1)S(1)} %collective-permute-done.24.refs_8_.refs_0_), channel_id=1, source_target_pairs={{0,4},{4,0},{8,12},{12,8},{1,5},{5,1},{9,13},{13,9},{2,6},{6,2},{1... | collective-permute-start | bytes 1572872 | tf_op jit(solution)/shard_map/ppermute | solution.py:558
  96.8 22.2 %collective-permute-start.32 = (bf16[128,2048]{1,0:T(8,128)(2,1)S(1)}, bf16[128,2048]{1,0:T(8,128)(2,1)S(1)}, u32[]{:S(2)}, u32[]{:S(2)}) collective-permute-start(bf16[128,2048]{1,0:T(8,128)(2,1)S(1)} %collective-permute-done.30.refs_8_.refs_4_), channel_id=1, source_target_pairs={{0,4},{4,0},{8,12},{12,8},{1,5},{5,1},{9,13},{13,9},{2,6},{6,2},{1... | collective-permute-start | bytes 1572872 | tf_op jit(solution)/shard_map/ppermute | solution.py:558
  96.8 19.1 %collective-permute-start.27 = (bf16[128,2048]{1,0:T(8,128)(2,1)S(1)}, bf16[128,2048]{1,0:T(8,128)(2,1)S(1)}, u32[]{:S(2)}, u32[]{:S(2)}) collective-permute-start(bf16[128,2048]{1,0:T(8,128)(2,1)S(1)} %collective-permute-done.25.refs_9_.refs_1_), channel_id=1, source_target_pairs={{0,4},{4,0},{8,12},{12,8},{1,5},{5,1},{9,13},{13,9},{2,6},{6,2},{1... | collective-permute-start | bytes 1572872 | tf_op jit(solution)/shard_map/ppermute | solution.py:558
  97.3 22.8 %collective-permute-start.33 = (bf16[128,2048]{1,0:T(8,128)(2,1)S(1)}, bf16[128,2048]{1,0:T(8,128)(2,1)S(1)}, u32[]{:S(2)}, u32[]{:S(2)}) collective-permute-start(bf16[128,2048]{1,0:T(8,128)(2,1)S(1)} %collective-permute-done.31.refs_9_.refs_5_), channel_id=1, source_target_pairs={{0,4},{4,0},{8,12},{12,8},{1,5},{5,1},{9,13},{13,9},{2,6},{6,2},{1... | collective-permute-start | bytes 1572872 | tf_op jit(solution)/shard_map/ppermute | solution.py:558
  102.7 33.2 %collective-permute-start.23 = (bf16[128,1024]{1,0:T(8,128)(2,1)S(1)}, bf16[128,1024]{1,0:T(8,128)(2,1)S(1)}, u32[]{:S(2)}, u32[]{:S(2)}) collective-permute-start(bf16[128,1024]{1,0:T(8,128)(2,1)S(1)} %get-tuple-element.47), channel_id=1, source_target_pairs={{0,3},{1,2},{2,1},{3,0},{4,7},{5,6},{6,5},{7,4},{8,11},{9,10},{10,... | collective-permute-start | bytes 786440 | tf_op jit(solution)/shard_map/ppermute | solution.py:561
  114.7 28.6 %collective-permute-start.20 = (bf16[128,1024]{1,0:T(8,128)(2,1)S(1)}, bf16[128,1024]{1,0:T(8,128)(2,1)S(1)}, u32[]{:S(2)}, u32[]{:S(2)}) collective-permute-start(bf16[128,1024]{1,0:T(8,128)(2,1)S(1)} %get-tuple-element.45), channel_id=1, source_target_pairs={{0,1},{1,0},{2,3},{3,2},{4,5},{5,4},{6,7},{7,6},{8,9},{9,8},{10,11... | collective-permute-start | bytes 786440 | tf_op jit(solution)/shard_map/ppermute | solution.py:561
  115.9 27.4 %collective-permute-start.21 = (bf16[128,1024]{1,0:T(8,128)(2,1)S(1)}, bf16[128,1024]{1,0:T(8,128)(2,1)S(1)}, u32[]{:S(2)}, u32[]{:S(2)}) collective-permute-start(bf16[128,1024]{1,0:T(8,128)(2,1)S(1)} %get-tuple-element.46), channel_id=1, source_target_pairs={{0,2},{1,3},{2,0},{3,1},{4,6},{5,7},{6,4},{7,5},{8,10},{9,11},{10,... | collective-permute-start | bytes 786440 | tf_op jit(solution)/shard_map/ppermute | solution.py:561
  118.9 13.4 %collective-permute-start.28 = (bf16[128,512]{1,0:T(8,128)(2,1)S(1)}, bf16[128,512]{1,0:T(8,128)(2,1)S(1)}, u32[]{:S(2)}, u32[]{:S(2)}) collective-permute-start(bf16[128,512]{1,0:T(8,128)(2,1)S(1)} %get-tuple-element.56), channel_id=1, source_target_pairs={{0,1},{1,0},{2,3},{3,2},{4,5},{5,4},{6,7},{7,6},{8,9},{9,8},{10,11... | collective-permute-start | bytes 393224 | tf_op jit(solution)/shard_map/ppermute | solution.py:561
  122.7 12.5 %collective-permute-start.35 = (bf16[128,512]{1,0:T(8,128)(2,1)S(1)}, bf16[128,512]{1,0:T(8,128)(2,1)S(1)}, u32[]{:S(2)}, u32[]{:S(2)}) collective-permute-start(bf16[128,512]{1,0:T(8,128)(2,1)S(1)} %get-tuple-element.66), channel_id=1, source_target_pairs={{0,1},{1,0},{2,3},{3,2},{4,5},{5,4},{6,7},{7,6},{8,9},{9,8},{10,11... | collective-permute-start | bytes 393224 | tf_op jit(solution)/shard_map/ppermute | solution.py:561
  132.4 17.0 %collective-permute-start.34 = (bf16[128,1024]{1,0:T(8,128)(2,1)S(1)}, bf16[128,1024]{1,0:T(8,128)(2,1)S(1)}, u32[]{:S(2)}, u32[]{:S(2)}) collective-permute-start(bf16[128,1024]{1,0:T(8,128)(2,1)S(1)} %get-tuple-element.64), channel_id=1, source_target_pairs={{0,1},{1,0},{2,3},{3,2},{4,5},{5,4},{6,7},{7,6},{8,9},{9,8},{10,11... | collective-permute-start | bytes 786440 | tf_op jit(solution)/shard_map/ppermute | solution.py:561
  135.2 11.9 %collective-permute-start.29 = (bf16[128,512]{1,0:T(8,128)(2,1)S(1)}, bf16[128,512]{1,0:T(8,128)(2,1)S(1)}, u32[]{:S(2)}, u32[]{:S(2)}) collective-permute-start(bf16[128,512]{1,0:T(8,128)(2,1)S(1)} %add_convert_fusion.1), channel_id=1, source_target_pairs={{0,2},{1,3},{2,0},{3,1},{4,6},{5,7},{6,4},{7,5},{8,10},{9,11},{10,... | collective-permute-start | bytes 393224 | tf_op jit(solution)/shard_map/ppermute | solution.py:561
  135.9 4.8 %copy-start = (bf16[128,1024]{1,0:T(8,128)(2,1)}, bf16[128,1024]{1,0:T(8,128)(2,1)S(1)}, u32[]{:S(2)}) copy-start(bf16[128,1024]{1,0:T(8,128)(2,1)S(1)} %collective-permute-done.23.refs_4_) | copy-start | bytes 786436
  135.9 13.5 %collective-permute-start.36 = (bf16[128,512]{1,0:T(8,128)(2,1)S(1)}, bf16[128,512]{1,0:T(8,128)(2,1)S(1)}, u32[]{:S(2)}, u32[]{:S(2)}) collective-permute-start(bf16[128,512]{1,0:T(8,128)(2,1)S(1)} %add_convert_fusion), channel_id=1, source_target_pairs={{0,2},{1,3},{2,0},{3,1},{4,6},{5,7},{6,4},{7,5},{8,10},{9,11},{10,... | collective-permute-start | bytes 393224 | tf_op jit(solution)/shard_map/ppermute | solution.py:561
  143.3 4.4 %copy-start.1 = (bf16[128,1024]{1,0:T(8,128)(2,1)}, bf16[128,1024]{1,0:T(8,128)(2,1)S(1)}, u32[]{:S(2)}) copy-start(bf16[128,1024]{1,0:T(8,128)(2,1)S(1)} %collective-permute-done.20.refs_2_) | copy-start | bytes 786436
  143.3 4.4 %copy-start.2 = (bf16[128,1024]{1,0:T(8,128)(2,1)}, bf16[128,1024]{1,0:T(8,128)(2,1)S(1)}, u32[]{:S(2)}) copy-start(bf16[128,1024]{1,0:T(8,128)(2,1)S(1)} %collective-permute-done.21.refs_3_) | copy-start | bytes 786436
  147.0 0.7 copy-start.3

commit v4 on v3

--- a/solution.py
+++ b/solution.py
@@ -209,7 +209,7 @@
     )
 
 
-def feed(blocks, near, chunks, prev, down_near, cuts, n_chunk=512):
+def feed(blocks, near, chunks, prev, down_near, cuts, whole=False, n_chunk=512):
     tok, width = blocks[0].shape
     rows, hid = near[0].shape
     half = rows // 2
@@ -218,8 +218,8 @@
     n_tok = nb * tok
     nf = len(chunks[0][1])
     n_in = nb + 2 + nc * nf + npv + (2 if down_near else 0)
-    n_out = nc + (len(cuts) if down_near else 0)
-    n_sem = n_in + nc * 2 + n_out * (2 * rows // n_chunk + 1)
+    n_out = nc + (len(cuts) if down_near else 0) + 2 * whole
+    n_sem = n_in + nc * 3 + n_out * (2 * rows // n_chunk + 1)
 
     def body(*refs):
         ins, outs, scratch = refs[:n_in], refs[n_in : n_in + n_out], refs[n_in + n_out :]
@@ -254,6 +254,8 @@
         stores = []
         for k, (t, _) in enumerate(chunks):
             wait_all(per_tile[k])
+            if whole:
+                stores.append(go.start(w.at[k], outs[-2].at[:, pl.ds(t * tile, tile)]))
             for c in range(0, tile, n_chunk):
                 n = min(n_chunk, tile)
                 lifted = jnp.dot(x[...], w[k, :, c : c + n], preferred_element_type=F32)
@@ -262,6 +264,9 @@
                 ).astype(BF)
             stores.append(go.start(h.at[:, t * tile : (t + 1) * tile], outs[k]))
         wait_all(late)
+        if whole:
+            first = pl.multiple_of(here()[0] * 2 * rows, 128)
+            stores.append(go.start(d, outs[-1].at[pl.ds(first, 2 * rows), :]))
         if down_near:
             for c in range(0, 2 * rows, n_chunk):
                 o[:, c : c + n_chunk] = lax.dot_general(
@@ -295,6 +300,8 @@
         ]
         scratch += [pltpu.VMEM((2 * rows, hid), BF), pltpu.VMEM((n_tok, 2 * rows), BF)]
         flops += 2 * n_tok * hid * 2 * rows
+    if whole:
+        out_shape += [jax.ShapeDtypeStruct((4 * rows, hid), BF)] * 2
     args = list(blocks) + list(near)
     for _, far in chunks:
         args += far
@@ -312,7 +319,7 @@
     )
 
 
-def down_far_step(hiddens, groups, cuts, sub, before):
+def down_far_step(hiddens, groups, cuts, sub, before, whole, first_group):
     hid = groups[0][0].shape[1]
     n_groups, nf = len(groups), len(groups[0])
     counts = [h[0].shape[0] for h in hiddens]
@@ -320,11 +327,13 @@
     n_h = sum(len(h) for h in hiddens)
     cols = n_groups * nf * sub
     ahead = 0 if before is None else before.shape[1]
-    n_in = n_h + n_groups * nf + (ahead > 0)
+    n_in = n_h + n_groups * nf + (ahead > 0) + 1
+    n_out = len(cuts) + 1
+    rows = whole.shape[0] // 4
 
     def body(*refs):
         ins, outs = refs[:n_in], refs[n_in : n_in + len(cuts)]
-        h, d, o, sems = refs[n_in + len(cuts) :]
+        whole_out, h, d, o, sems = refs[n_in + len(cuts) :]
         go = Copies(sems)
         loads, k, r0 = [], 0, 0
         for tiles, count in zip(hiddens, counts):
@@ -348,6 +357,14 @@
         if ahead:
             stores.append(go.start(ins[k], outs[-1].at[:, :ahead]))
         wait_all(loads)
+        for c in range(2):
+            to = (2 * (1 - here()[0]) + c) * rows + first_group * 2 * sub
+            stores.append(
+                go.start(
+                    d.at[c * (cols // 2) : (c + 1) * (cols // 2), :],
+                    whole_out.at[pl.ds(pl.multiple_of(to, 128), cols // 2), :],
+                )
+            )
         o[...] = lax.dot_general(
             h[...], d[...], (((1,), (1,)), ((), ())), preferred_element_type=F32
         ).astype(BF)
@@ -368,61 +385,24 @@
                 (sum(c for _, c in runs), cols + (ahead if i == len(cuts) - 1 else 0)), BF
             )
             for i, runs in enumerate(cuts)
-        ),
+        )
+        + (jax.ShapeDtypeStruct(whole.shape, BF),),
         [t for h in hiddens for t in h]
         + [p for g in groups for p in g]
-        + ([before] if ahead else []),
+        + ([before] if ahead else [])
+        + [whole],
+        input_output_aliases={n_in - 1: n_out - 1},
         scratch_shapes=[
             pltpu.VMEM((n_tok, hid), BF),
             pltpu.VMEM((cols, hid), BF),
             pltpu.VMEM((n_tok, cols), BF),
-            pltpu.SemaphoreType.DMA((n_in + sum(len(r) for r in cuts),)),
+            pltpu.SemaphoreType.DMA((n_in + 2 + sum(len(r) for r in cuts),)),
         ],
         compiler_params=LIMIT,
         cost_estimate=pl.CostEstimate(
             flops=2 * n_tok * cols * hid, bytes_accessed=2 * cols * hid, transcendentals=0
         ),
         name="down_far",
-    )
-
-
-def assemble(pieces, shape, places, base=None):
-    n = len(pieces)
-
-    def body(*refs):
-        ins, out, buf, sems = refs[:n], refs[-3], refs[-2], refs[-1]
-        go = Copies(sems)
-        spots = [
-            (pl.ds(row, p.shape[0]), pl.ds(col, p.shape[1]))
-            for p, (row, col) in zip(pieces, places())
-        ]
-        spaces, at = [], 0
-        for p in pieces:
-            spaces.append(buf.at[at : at + p.shape[0], : p.shape[1]])
-            at += p.shape[0]
-        loads = [go.start(ref, space) for ref, space in zip(ins, spaces)]
-        stores = []
-        for load, space, spot in zip(loads, spaces, spots):
-            load.wait()
-            stores.append(go.start(space, out.at[spot]))
-        wait_all(stores)
-
-    args = list(pieces) + ([base] if base is not None else [])
-    total = sum(p.shape[0] for p in pieces)
-    return hbm_call(
-        body,
-        jax.ShapeDtypeStruct(shape, BF),
-        args,
-        input_output_aliases={n: 0} if base is not None else {},
-        scratch_shapes=[
-            pltpu.VMEM((total, max(p.shape[1] for p in pieces)), BF),
-            pltpu.SemaphoreType.DMA((2 * n,)),
-        ],
-        compiler_params=LIMIT,
-        cost_estimate=pl.CostEstimate(
-            flops=10**9, bytes_accessed=2 * shape[0] * shape[1], transcendentals=0
-        ),
-        name="assemble",
     )
 
 
@@ -541,10 +521,10 @@
 
 
 U_CUTS = 4
-D_CUTS = 2
+D_CUTS = 4
 LEAD = 3
 FIRST = 3
-ROUNDS = ((0,), (1,))
+ROUNDS = ((0, 1), (2, 3))
 
 
 def routed():
@@ -613,14 +593,16 @@
         )
         hidden = hidden + last
         got1 = tp_swap(send1, 1)
-        *hidden3, send3 = feed([r3], up_near, tiles, [], down_near, cut[:1])
+        *hidden3, send3, whole_up, whole_down = feed(
+            [r3], up_near, tiles, [], down_near, cut[:1], True
+        )
         near_terms = [keep0, got1, tp_swap(keep2, 2), tp_swap(send3, 3)]
 
         far_terms, sent = [], None
         cuts = [[(3 * tok, tok)], [cut[1]], [cut[2]], [cut[0]]]
         for ids in ROUNDS:
-            send3, keep0, keep2, sent = down_far_step(
-                [hidden, hidden3], [down_far[g] for g in ids], cuts, sub, sent
+            send3, keep0, keep2, sent, whole_down = down_far_step(
+                [hidden, hidden3], [down_far[g] for g in ids], cuts, sub, sent, whole_down, ids[0]
             )
             got3 = tp_swap(send3, 1)
             pair = add_rows(keep2, got3)
@@ -630,27 +612,6 @@
         counts = [t[0].shape[1] for t in far_terms]
         state = before_last(near_terms, far_terms, post_gain, rows)
 
-        def own_spots():
-            y, core, _ = here()
-            return [(pl.multiple_of((2 * y + c) * rows, 64), 0) for c in (core, 1 - core)]
-
-        def up_spots():
-            return [(a, i * tile) for i in range(U_CUTS) for a in up_places(rows, half)[2:]]
-
-        def down_spots():
-            y, core, grp = here()
-            return [
-                (pl.multiple_of((2 * (1 - y) + c) * rows + (2 * i + side) * sub, 64), 0)
-                for i in range(D_CUTS)
-                for c in (core, 1 - core)
-                for side in (grp, 1 - grp)
-            ]
-
-        shape = (4 * rows, hid)
-        whole_up = assemble(up_near, shape, own_spots)
-        whole_up = assemble([p for g in up_far for p in g], shape, up_spots, whole_up)
-        whole_down = assemble(down_near, shape, own_spots)
-        whole_down = assemble([p for g in down_far for p in g], shape, down_spots, whole_down)
         mixed = finish(*state, one, two, counts, rows)
         return mixed, whole_up, whole_down
 

time: 151 us -> 165 us (1.093)
  starting transfers between devices: 36.4 us -> 49.6 us
  waiting for transfers between devices: 70.1 us -> 79.7 us
  Pallas kernels: 42.4 us -> 34 us
    ppermute x6 -> x8, waiting for transfers between devices: 12.5 us -> 24.8 us  [y_swap(): return lax.ppermute(v, 'fs', [(i, i ^ 2) for i in range(4)])]
    ppermute x11, starting transfers between devices: 16.8 us -> 25.9 us  [tp_swap(): return lax.ppermute(v, 'tp', [(i, i ^ m) for i in range(4)])]
    pallas_call x13 -> x9, Pallas kernels: 39.6 us -> 31.2 us  [hbm_call(): pl.pallas_call(body, out_shape=out_shape, in_specs=[ANY] * len(args), out...]
    ppermute x6 -> x8, starting transfers between devices: 8.38 us -> 11.4 us  [y_swap(): return lax.ppermute(v, 'fs', [(i, i ^ 2) for i in range(4)])]
    ppermute x11, waiting for transfers between devices: 30.1 us -> 27.7 us  [tp_swap(): return lax.ppermute(v, 'tp', [(i, i ^ m) for i in range(4)])]
    ppermute x14 -> x18, waiting for transfers between devices: 3.73 us -> 1.38 us  [core_swap(): return lax.ppermute(v, 'fs', [(i, i ^ 1) for i in range(4)])]
    ppermute x6 -> x8, waiting for transfers between devices: 23.7 us -> 25.8 us  [grp_swap(): return lax.ppermute(v, 'grp', [(0, 1), (1, 0)])]
    ppermute x6 -> x8, starting transfers between devices: 8.97 us -> 10.2 us  [grp_swap(): return lax.ppermute(v, 'grp', [(0, 1), (1, 0)])]
  transfers between devices with their start and end apart: 37 -> 45, of which waited for: 14 -> 22; matrix products, arithmetic and copies ran while one was open for 0% -> 0% of each run, Pallas kernels for 26% -> 18%
where the time goes in v4:
time: 165 us
  waiting for transfers between devices  79.7 us (48%)
  starting transfers between devices  49.6 us (30%)
  Pallas kernels  34 us (21%)
    pallas_call x9, Pallas kernels, hbm_call(): pl.pallas_call(body, out_shape=out_shape, in_specs=[ANY] * len(args), out...  31.2 us
    ppermute x11, waiting for transfers between devices, tp_swap(): return lax.ppermute(v, 'tp', [(i, i ^ m) for i in range(4)])  27.7 us
    ppermute x11, starting transfers between devices, tp_swap(): return lax.ppermute(v, 'tp', [(i, i ^ m) for i in range(4)])  25.9 us
    ppermute x8, waiting for transfers between devices, grp_swap(): return lax.ppermute(v, 'grp', [(0, 1), (1, 0)])  25.8 us
    ppermute x8, waiting for transfers between devices, y_swap(): return lax.ppermute(v, 'fs', [(i, i ^ 2) for i in range(4)])  24.8 us
    ppermute x8, starting transfers between devices, y_swap(): return lax.ppermute(v, 'fs', [(i, i ^ 2) for i in range(4)])  11.4 us
    ppermute x8, starting transfers between devices, grp_swap(): return lax.ppermute(v, 'grp', [(0, 1), (1, 0)])  10.2 us
  transfers between devices with their start and end apart: 45, of which 22 were waited for; matrix products, arithmetic and copies ran while one was open for 0% of the time, Pallas kernels for 18%

profile of v4, /device:TPU:0, one launch (start us, length us, event | category | flops | bytes accessed | tf_op | source)
XLA Modules:
  0.0 164.9 jit_solution(3537709706546990615)
XLA Ops:
  0.6 3.0 %cast.4 = (bf16[256,512]{1,0:T(8,128)(2,1)S(1)}, bf16[256,512]{1,0:T(8,128)(2,1)S(1)}, bf16[128,2048]{1,0:T(8,128)(2,1)S(1)}) custom-call(f32[512,2048]{1,0:T(8,128)} %refs_0_.6, f32[1,512]{1,0:T(1,128)} %bitcast.2, bf16[128,2048]{1,0:T(8,128)(2,1)} %refs_2_.1), custom_call_target="tpu_custom_call" | custom-call | flops 100000000 | bytes 6291456 | tf_op jit(solution)/shard_map/cast/pallas_call | solution.py:50
  3.6 3.1 %collective-permute-start.11 = (bf16[256,512]{1,0:T(8,128)(2,1)S(1)}, bf16[256,512]{1,0:T(8,128)(2,1)S(1)}, u32[]{:S(2)}, u32[]{:S(2)}) collective-permute-start(bf16[256,512]{1,0:T(8,128)(2,1)S(1)} %get-tuple-element.44), channel_id=1, source_target_pairs={{0,8},{4,12},{8,0},{12,4},{1,9},{5,13},{9,1},{13,5},{2,10},{6,14},... | collective-permute-start | bytes 786440 | tf_op jit(solution)/shard_map/ppermute | solution.py:535
  6.7 2.8 %cast.5 = (bf16[512,2048]{1,0:T(8,128)(2,1)S(1)}, bf16[256,512]{1,0:T(8,128)(2,1)S(1)}) custom-call(f32[512,2048]{1,0:T(8,128)} %refs_0_.6, f32[1,512]{1,0:T(1,128)} %bitcast.3), custom_call_target="tpu_custom_call" | custom-call | flops 100000000 | bytes 6291456 | tf_op jit(solution)/shard_map/cast/pallas_call | solution.py:50
  9.5 2.0 %collective-permute-start.3 = (bf16[256,512]{1,0:T(8,128)(2,1)S(1)}, bf16[256,512]{1,0:T(8,128)(2,1)S(1)}, u32[]{:S(2)}, u32[]{:S(2)}) collective-permute-start(bf16[256,512]{1,0:T(8,128)(2,1)S(1)} %get-tuple-element.43), channel_id=1, source_target_pairs={{0,8},{4,12},{8,0},{12,4},{1,9},{5,13},{9,1},{13,5},{2,10},{6,14},... | collective-permute-start | bytes 786440 | tf_op jit(solution)/shard_map/ppermute | solution.py:535
  11.5 1.9 %cast.6 = bf16[256,512]{1,0:T(8,128)(2,1)S(1)} custom-call(f32[512,2048]{1,0:T(8,128)} %refs_0_.6, f32[1,512]{1,0:T(1,128)} %bitcast.4), custom_call_target="tpu_custom_call" | custom-call | flops 100000000 | bytes 6291456 | tf_op jit(solution)/shard_map/cast/pallas_call | solution.py:50
  13.5 2.8 %cast.7 = (bf16[512,2048]{1,0:T(8,128)(2,1)S(1)}, bf16[64,2048]{1,0:T(8,128)(2,1)S(1)}, bf16[64,2048]{1,0:T(8,128)(2,1)S(1)}, bf16[64,2048]{1,0:T(8,128)(2,1)S(1)}, bf16[64,2048]{1,0:T(8,128)(2,1)S(1)}) custom-call(f32[512,2048]{1,0:T(8,128)} %refs_0_.7), custom_call_target="tpu_custom_call" | custom-call | flops 100000000 | bytes 6291456 | tf_op jit(solution)/shard_map/cast/pallas_call | solution.py:50
  16.3 2.0 %collective-permute-start.24 = (bf16[64,2048]{1,0:T(8,128)(2,1)S(1)}, bf16[64,2048]{1,0:T(8,128)(2,1)S(1)}, u32[]{:S(2)}, u32[]{:S(2)}) collective-permute-start(bf16[64,2048]{1,0:T(8,128)(2,1)S(1)} %get-tuple-element.59), channel_id=1, source_target_pairs={{0,8},{4,12},{8,0},{12,4},{1,9},{5,13},{9,1},{13,5},{2,10},{6,14},... | collective-permute-start | bytes 786440 | tf_op jit(solution)/shard_map/ppermute | solution.py:535
  18.4 1.0 collective-permute-done.15.refs_13_.refs_11_
  19.4 2.0 %collective-permute-start.34 = (bf16[64,2048]{1,0:T(8,128)(2,1)S(1)}, bf16[64,2048]{1,0:T(8,128)(2,1)S(1)}, u32[]{:S(2)}, u32[]{:S(2)}) collective-permute-start(bf16[64,2048]{1,0:T(8,128)(2,1)S(1)} %get-tuple-element.65), channel_id=1, source_target_pairs={{0,8},{4,12},{8,0},{12,4},{1,9},{5,13},{9,1},{13,5},{2,10},{6,14},... | collective-permute-start | bytes 786440 | tf_op jit(solution)/shard_map/ppermute | solution.py:535
  21.5 3.6 %collective-permute-done.3.refs_5_.refs_15_ = bf16[256,512]{1,0:T(8,128)(2,1)S(1)} collective-permute-done((bf16[256,512]{1,0:T(8,128)(2,1)S(1)}, bf16[256,512]{1,0:T(8,128)(2,1)S(1)}, u32[]{:S(2)}, u32[]{:S(2)}) %collective-permute-start.3) | collective-permute-done | bytes 262176 | tf_op jit(solution)/shard_map/ppermute | solution.py:535
  25.1 5.6 %collective-permute-done.7.refs_5_.refs_3_ = bf16[256,512]{1,0:T(8,128)(2,1)S(1)} collective-permute-done((bf16[256,512]{1,0:T(8,128)(2,1)S(1)}, bf16[256,512]{1,0:T(8,128)(2,1)S(1)}, u32[]{:S(2)}, u32[]{:S(2)}) %collective-permute-start.7) | collective-permute-done | bytes 262176 | tf_op jit(solution)/shard_map/ppermute | solution.py:535
  30.7 2.0 %collective-permute-start.38 = (bf16[64,2048]{1,0:T(8,128)(2,1)S(1)}, bf16[64,2048]{1,0:T(8,128)(2,1)S(1)}, u32[]{:S(2)}, u32[]{:S(2)}) collective-permute-start(bf16[64,2048]{1,0:T(8,128)(2,1)S(1)} %get-tuple-element.66), channel_id=1, source_target_pairs={{0,8},{4,12},{8,0},{12,4},{1,9},{5,13},{9,1},{13,5},{2,10},{6,14},... | collective-permute-start | bytes 786440 | tf_op jit(solution)/shard_map/ppermute | solution.py:535
  32.7 3.6 %collective-permute-done.24.refs_8_ = bf16[64,2048]{1,0:T(8,128)(2,1)S(1)} collective-permute-done((bf16[64,2048]{1,0:T(8,128)(2,1)S(1)}, bf16[64,2048]{1,0:T(8,128)(2,1)S(1)}, u32[]{:S(2)}, u32[]{:S(2)}) %collective-permute-start.24) | collective-permute-done | bytes 262176 | tf_op jit(solution)/shard_map/ppermute | solution.py:535
  36.3 5.6 %collective-permute-done.28.refs_12_ = bf16[64,2048]{1,0:T(8,128)(2,1)S(1)} collective-permute-done((bf16[64,2048]{1,0:T(8,128)(2,1)S(1)}, bf16[64,2048]{1,0:T(8,128)(2,1)S(1)}, u32[]{:S(2)}, u32[]{:S(2)}) %collective-permute-start.28) | collective-permute-done | bytes 262176 | tf_op jit(solution)/shard_map/ppermute | solution.py:535
  41.9 2.0 %collective-permute-start.12 = (bf16[256,512]{1,0:T(8,128)(2,1)S(1)}, bf16[256,512]{1,0:T(8,128)(2,1)S(1)}, u32[]{:S(2)}, u32[]{:S(2)}) collective-permute-start(bf16[256,512]{1,0:T(8,128)(2,1)S(1)} %collective-permute-done.11.refs_9_.refs_7_), channel_id=1, source_target_pairs={{0,16},{16,0},{1,17},{17,1},{2,18},{18,2},{3,19},{19,3},{4,20},{20... | collective-permute-start | bytes 786440 | tf_op jit(solution)/shard_map/ppermute | solution.py:532
  43.9 3.6 %collective-permute-done.34.refs_8_ = bf16[64,2048]{1,0:T(8,128)(2,1)S(1)} collective-permute-done((bf16[64,2048]{1,0:T(8,128)(2,1)S(1)}, bf16[64,2048]{1,0:T(8,128)(2,1)S(1)}, u32[]{:S(2)}, u32[]{:S(2)}) %collective-permute-start.34) | collective-permute-done | bytes 262176 | tf_op jit(solution)/shard_map/ppermute | solution.py:535
  47.5 3.1 %collective-permute-start.1 = (bf16[128,2048]{1,0:T(8,128)(2,1)S(1)}, bf16[128,2048]{1,0:T(8,128)(2,1)S(1)}, u32[]{:S(2)}, u32[]{:S(2)}) collective-permute-start(bf16[128,2048]{1,0:T(8,128)(2,1)S(1)} %get-tuple-element.41.refs_1_), channel_id=1, source_target_pairs={{0,2},{1,3},{2,0},{3,1},{4,6},{5,7},{6,4},{7,5},{8,10},{9,11},{10,... | collective-permute-start | bytes 1572872 | tf_op jit(solution)/shard_map/ppermute | solution.py:541
  50.6 1.7 %collective-permute-done.38.refs_12_ = bf16[64,2048]{1,0:T(8,128)(2,1)S(1)} collective-permute-done((bf16[64,2048]{1,0:T(8,128)(2,1)S(1)}, bf16[64,2048]{1,0:T(8,128)(2,1)S(1)}, u32[]{:S(2)}, u32[]{:S(2)}) %collective-permute-start.38) | collective-permute-done | bytes 262176 | tf_op jit(solution)/shard_map/ppermute | solution.py:535
  52.3 1.7 %collective-permute-start.16 = (bf16[256,512]{1,0:T(8,128)(2,1)S(1)}, bf16[256,512]{1,0:T(8,128)(2,1)S(1)}, u32[]{:S(2)}, u32[]{:S(2)}) collective-permute-start(bf16[256,512]{1,0:T(8,128)(2,1)S(1)} %collective-permute-done.15.refs_13_.refs_11_), channel_id=1, source_target_pairs={{0,16},{16,0},{1,17},{17,1},{2,18},{18,2},{3,19},{19,3},{4,20},{20... | collective-permute-start | bytes 786440 | tf_op jit(solution)/shard_map/ppermute | solution.py:532
  54.3 7.1 %collective-permute-done.16.refs_14_.refs_12_ = bf16[256,512]{1,0:T(8,128)(2,1)S(1)} collective-permute-done((bf16[256,512]{1,0:T(8,128)(2,1)S(1)}, bf16[256,512]{1,0:T(8,128)(2,1)S(1)}, u32[]{:S(2)}, u32[]{:S(2)}) %collective-permute-start.16) | collective-permute-done | bytes 262176 | tf_op jit(solution)/shard_map/ppermute | solution.py:532
  61.5 3.9 %collective-permute-done.4.refs_6_.refs_16_ = bf16[256,512]{1,0:T(8,128)(2,1)S(1)} collective-permute-done((bf16[256,512]{1,0:T(8,128)(2,1)S(1)}, bf16[256,512]{1,0:T(8,128)(2,1)S(1)}, u32[]{:S(2)}, u32[]{:S(2)}) %collective-permute-start.4) | collective-permute-done | bytes 262176 | tf_op jit(solution)/shard_map/ppermute | solution.py:532
  65.4 6.5 %collective-permute-done.1.refs_2_ = bf16[128,2048]{1,0:T(8,128)(2,1)S(1)} collective-permute-done((bf16[128,2048]{1,0:T(8,128)(2,1)S(1)}, bf16[128,2048]{1,0:T(8,128)(2,1)S(1)}, u32[]{:S(2)}, u32[]{:S(2)}) %collective-permute-start.1) | collective-permute-done | bytes 524320 | tf_op jit(solution)/shard_map/ppermute | solution.py:541
  71.9 1.4 collective-permute-start.8
  74.0 5.2 %collective-permute-done.8.refs_6_.refs_4_ = bf16[256,512]{1,0:T(8,128)(2,1)S(1)} collective-permute-done((bf16[256,512]{1,0:T(8,128)(2,1)S(1)}, bf16[256,512]{1,0:T(8,128)(2,1)S(1)}, u32[]{:S(2)}, u32[]{:S(2)}) %collective-permute-start.8) | collective-permute-done | bytes 262176 | tf_op jit(solution)/shard_map/ppermute | solution.py:532
  79.2 1.4 collective-permute-start.25
  80.7 1.4 collective-permute-start.29
  82.1 3.8 %collective-permute-done.refs_0_ = bf16[128,2048]{1,0:T(8,128)(2,1)S(1)} collective-permute-done((bf16[128,2048]{1,0:T(8,128)(2,1)S(1)}, bf16[128,2048]{1,0:T(8,128)(2,1)S(1)}, u32[]{:S(2)}, u32[]{:S(2)}) %collective-permute-start) | collective-permute-done | bytes 524320 | tf_op jit(solution)/shard_map/ppermute | solution.py:541
  85.9 2.5 %collective-permute-done.25.refs_9_ = bf16[64,2048]{1,0:T(8,128)(2,1)S(1)} collective-permute-done((bf16[64,2048]{1,0:T(8,128)(2,1)S(1)}, bf16[64,2048]{1,0:T(8,128)(2,1)S(1)}, u32[]{:S(2)}, u32[]{:S(2)}) %collective-permute-start.25) | collective-permute-done | bytes 262176 | tf_op jit(solution)/shard_map/ppermute | solution.py:532
  88.4 5.2 %collective-permute-done.29.refs_13_ = bf16[64,2048]{1,0:T(8,128)(2,1)S(1)} collective-permute-done((bf16[64,2048]{1,0:T(8,128)(2,1)S(1)}, bf16[64,2048]{1,0:T(8,128)(2,1)S(1)}, u32[]{:S(2)}, u32[]{:S(2)}) %collective-permute-start.29) | collective-permute-done | bytes 262176 | tf_op jit(solution)/shard_map/ppermute | solution.py:532
  94.1 0.9 collective-permute-done.14.refs_12_.refs_10_
  95.4 1.6 collective-permute-start.22
  97.0 1.5 collective-permute-start.35
  99.0 4.2 %feed.3 = (bf16[384,512]{1,0:T(8,128)(2,1)S(1)}, bf16[384,512]{1,0:T(8,128)(2,1)S(1)}, bf16[384,512]{1,0:T(8,128)(2,1)S(1)}) custom-call(bf16[128,2048]{1,0:T(8,128)(2,1)S(1)} %collective-permute-done.refs_0_, bf16[128,2048]{1,0:T(8,128)(2,1)S(1)} %get-tuple-element.41.refs_1_, bf16[128,2048]{1,0:T(8,128)(2,1)S(1)} %collective-permute-done.1.refs_2_, ...), custom_call_target="tpu_custom_call" | custom-call | flops 2415919104 | bytes 6291456 | tf_op jit(solution)/shard_map/feed/pallas_call | solution.py:50
  103.8 4.8 %feed.4 = (bf16[384,512]{1,0:T(8,128)(2,1)S(1)}, bf16[128,1024]{1,0:T(8,128)(2,1)S(1)}, bf16[128,1024]{1,0:T(8,128)(2,1)}, bf16[128,1024]{1,0:T(8,128)(2,1)S(1)}) custom-call(bf16[128,2048]{1,0:T(8,128)(2,1)S(1)} %collective-permute-done.refs_0_, bf16[128,2048]{1,0:T(8,128)(2,1)S(1)} %get-tuple-element.41.refs_1_, ...), custom_call_target="tpu_custom_call" | custom-call | flops 2415919104 | bytes 2097152 | tf_op jit(solution)/shard_map/feed/pallas_call | solution.py:50
  108.7 2.0 %collective-permute-done.39.refs_13_ = bf16[64,2048]{1,0:T(8,128)(2,1)S(1)} collective-permute-done((bf16[64,2048]{1,0:T(8,128)(2,1)S(1)}, bf16[64,2048]{1,0:T(8,128)(2,1)S(1)}, u32[]{:S(2)}, u32[]{:S(2)}) %collective-permute-start.39) | collective-permute-done | bytes 262176 | tf_op jit(solution)/shard_map/ppermute | solution.py:532
  111.3 6.4 %feed.5 = (bf16[128,512]{1,0:T(8,128)(2,1)S(1)}, bf16[128,512]{1,0:T(8,128)(2,1)S(1)}, bf16[128,512]{1,0:T(8,128)(2,1)S(1)}, bf16[128,512]{1,0:T(8,128)(2,1)S(1)...) custom-call(bf16[128,2048]{1,0:T(8,128)(2,1)S(1)} %collective-permute-done.22.refs_0_, ...), custom_call_target="tpu_custom_call" | custom-call | flops 1610612736 | bytes 8388608 | tf_op jit(solution)/shard_map/feed/pallas_call | solution.py:50
  117.7 2.7 %down_far.2 = (bf16[128,512]{1,0:T(8,128)(2,1)S(1)}, bf16[128,512]{1,0:T(8,128)(2,1)}, bf16[128,512]{1,0:T(8,128)(2,1)S(1)}, bf16[128,512]{1,0:T(8,128)(2,1)S(1)}, bf16[2048,2048]{1,0:T(8,128)(2,1)}) custom-call(bf16[384,512]{1,0:T(8,128)(2,1)S(1)} %get-tuple-element.46.refs_9_.refs_0_, ...), custom_call_target="tpu_custom_call", output_to_operand_aliasing={{4}: (16, {})} | custom-call | flops 1073741824 | bytes 2097152 | tf_op jit(solution)/shard_map/down_far/pallas_call | solution.py:50
  121.2 2.7 %down_far.3 = (bf16[128,512]{1,0:T(8,128)(2,1)S(1)}, bf16[128,512]{1,0:T(8,128)(2,1)}, bf16[128,512]{1,0:T(8,128)(2,1)S(1)}, bf16[128,1024]{1,0:T(8,128)(2,1)S(1)}, bf16[2048,2048]{1,0:T(8,128)(2,1)}) custom-call(bf16[384,512]{1,0:T(8,128)(2,1)S(1)} %get-tuple-element.46.refs_9_.refs_0_, ...), custom_call_target="tpu_custom_call", output_to_operand_aliasing={{4}: (17, {})} | custom-call | flops 1073741824 | bytes 2097152 | tf_op jit(solution)/shard_map/down_far/pallas_call | solution.py:50
  123.9 1.4 collective-permute-start.43
  125.4 3.5 %collective-permute-start.23 = (bf16[128,1024]{1,0:T(8,128)(2,1)S(1)}, bf16[128,1024]{1,0:T(8,128)(2,1)S(1)}, u32[]{:S(2)}, u32[]{:S(2)}) collective-permute-start(bf16[128,1024]{1,0:T(8,128)(2,1)S(1)} %get-tuple-element.53), channel_id=1, source_target_pairs={{0,3},{1,2},{2,1},{3,0},{4,7},{5,6},{6,5},{7,4},{8,11},{9,10},{10,... | collective-permute-start | bytes 786440 | tf_op jit(solution)/shard_map/ppermute | solution.py:541
  129.8 1.1 collective-permute-start.42
  130.9 7.2 %collective-permute-start.33 = (bf16[128,512]{1,0:T(8,128)(2,1)S(1)}, bf16[128,512]{1,0:T(8,128)(2,1)S(1)}, u32[]{:S(2)}, u32[]{:S(2)}) collective-permute-start(bf16[128,512]{1,0:T(8,128)(2,1)S(1)} %add_convert_fusion.1), channel_id=1, source_target_pairs={{0,2},{1,3},{2,0},{3,1},{4,6},{5,7},{6,4},{7,5},{8,10},{9,11},{10,... | collective-permute-start | bytes 393224 | tf_op jit(solution)/shard_map/ppermute | solution.py:541
  138.8 5.7 %collective-permute-start.44 = (bf16[128,512]{1,0:T(8,128)(2,1)S(1)}, bf16[128,512]{1,0:T(8,128)(2,1)S(1)}, u32[]{:S(2)}, u32[]{:S(2)}) collective-permute-start(bf16[128,512]{1,0:T(8,128)(2,1)S(1)} %add_convert_fusion), channel_id=1, source_target_pairs={{0,2},{1,3},{2,0},{3,1},{4,6},{5,7},{6,4},{7,5},{8,10},{9,11},{10,... | collective-permute-start | bytes 393224 | tf_op jit(solution)/shard_map/ppermute | solution.py:541
  144.6 1.6 collective-permute-done.20.refs_2_
  146.2 6.7 %collective-permute-done.21.refs_3_ = bf16[128,1024]{1,0:T(8,128)(2,1)S(1)} collective-permute-done((bf16[128,1024]{1,0:T(8,128)(2,1)S(1)}, bf16[128,1024]{1,0:T(8,128)(2,1)S(1)}, u32[]{:S(2)}, u32[]{:S(2)}) %collective-permute-start.21) | collective-permute-done | bytes 262176 | tf_op jit(solution)/shard_map/ppermute | solution.py:541
  152.9 8.4 %collective-permute-done.33.refs_6_ = bf16[128,512]{1,0:T(8,128)(2,1)S(1)} collective-permute-done((bf16[128,512]{1,0:T(8,128)(2,1)S(1)}, bf16[128,512]{1,0:T(8,128)(2,1)S(1)}, u32[]{:S(2)}, u32[]{:S(2)}) %collective-permute-start.33) | collective-permute-done | bytes 131104 | tf_op jit(solution)/shard_map/ppermute | solution.py:541
  161.9 1.7 %before_last.1 = (f32[128,2048]{1,0:T(8,128)S(1)}, f32[128,1024]{1,0:T(8,128)S(1)}, f32[1,1024]{1,0:T(1,128)S(1)}, f32[128,128]{1,0:T(8,128)S(1)}) custom-call(f32[1,2048]{1,0:T(1,128)} %bitcast.5, bf16[128,1024]{1,0:T(8,128)(2,1)} %get-tuple-element.50.refs_1_, bf16[128,1024]{1,0:T(8,128)(2,1)} %copy-done.1, bf16[128,1024]{1,0:T(8,128)(2,1)} %copy-done.2, ...), custom_call_target="tpu_custom_call" | custom-call | tf_op jit(solution)/shard_map/before_last/pallas_call | solution.py:448
  163.6 1.1 finish.1
  (63 shorter events, 7.3 us)
Async XLA Ops:
  3.6 14.7 %collective-permute-start.11 = (bf16[256,512]{1,0:T(8,128)(2,1)S(1)}, bf16[256,512]{1,0:T(8,128)(2,1)S(1)}, u32[]{:S(2)}, u32[]{:S(2)}) collective-permute-start(bf16[256,512]{1,0:T(8,128)(2,1)S(1)} %get-tuple-element.44), channel_id=1, source_target_pairs={{0,8},{4,12},{8,0},{12,4},{1,9},{5,13},{9,1},{13,5},{2,10},{6,14},... | collective-permute-start | bytes 786440 | tf_op jit(solution)/shard_map/ppermute | solution.py:535
  6.7 12.8 %collective-permute-start.15 = (bf16[256,512]{1,0:T(8,128)(2,1)S(1)}, bf16[256,512]{1,0:T(8,128)(2,1)S(1)}, u32[]{:S(2)}, u32[]{:S(2)}) collective-permute-start(bf16[256,512]{1,0:T(8,128)(2,1)S(1)} %get-tuple-element.45), channel_id=1, source_target_pairs={{0,8},{4,12},{8,0},{12,4},{1,9},{5,13},{9,1},{13,5},{2,10},{6,14},... | collective-permute-start | bytes 786440 | tf_op jit(solution)/shard_map/ppermute | solution.py:535
  9.5 15.5 %collective-permute-start.3 = (bf16[256,512]{1,0:T(8,128)(2,1)S(1)}, bf16[256,512]{1,0:T(8,128)(2,1)S(1)}, u32[]{:S(2)}, u32[]{:S(2)}) collective-permute-start(bf16[256,512]{1,0:T(8,128)(2,1)S(1)} %get-tuple-element.43), channel_id=1, source_target_pairs={{0,8},{4,12},{8,0},{12,4},{1,9},{5,13},{9,1},{13,5},{2,10},{6,14},... | collective-permute-start | bytes 786440 | tf_op jit(solution)/shard_map/ppermute | solution.py:535
  13.4 17.3 %collective-permute-start.7 = (bf16[256,512]{1,0:T(8,128)(2,1)S(1)}, bf16[256,512]{1,0:T(8,128)(2,1)S(1)}, u32[]{:S(2)}, u32[]{:S(2)}) collective-permute-start(bf16[256,512]{1,0:T(8,128)(2,1)S(1)} %cast.6), channel_id=1, source_target_pairs={{0,8},{4,12},{8,0},{12,4},{1,9},{5,13},{9,1},{13,5},{2,10},{6,14},... | collective-permute-start | bytes 786440 | tf_op jit(solution)/shard_map/ppermute | solution.py:535
  16.3 20.0 %collective-permute-start.24 = (bf16[64,2048]{1,0:T(8,128)(2,1)S(1)}, bf16[64,2048]{1,0:T(8,128)(2,1)S(1)}, u32[]{:S(2)}, u32[]{:S(2)}) collective-permute-start(bf16[64,2048]{1,0:T(8,128)(2,1)S(1)} %get-tuple-element.59), channel_id=1, source_target_pairs={{0,8},{4,12},{8,0},{12,4},{1,9},{5,13},{9,1},{13,5},{2,10},{6,14},... | collective-permute-start | bytes 786440 | tf_op jit(solution)/shard_map/ppermute | solution.py:535
  18.3 23.6 %collective-permute-start.28 = (bf16[64,2048]{1,0:T(8,128)(2,1)S(1)}, bf16[64,2048]{1,0:T(8,128)(2,1)S(1)}, u32[]{:S(2)}, u32[]{:S(2)}) collective-permute-start(bf16[64,2048]{1,0:T(8,128)(2,1)S(1)} %get-tuple-element.60), channel_id=1, source_target_pairs={{0,8},{4,12},{8,0},{12,4},{1,9},{5,13},{9,1},{13,5},{2,10},{6,14},... | collective-permute-start | bytes 786440 | tf_op jit(solution)/shard_map/ppermute | solution.py:535
  19.4 28.1 %collective-permute-start.34 = (bf16[64,2048]{1,0:T(8,128)(2,1)S(1)}, bf16[64,2048]{1,0:T(8,128)(2,1)S(1)}, u32[]{:S(2)}, u32[]{:S(2)}) collective-permute-start(bf16[64,2048]{1,0:T(8,128)(2,1)S(1)} %get-tuple-element.65), channel_id=1, source_target_pairs={{0,8},{4,12},{8,0},{12,4},{1,9},{5,13},{9,1},{13,5},{2,10},{6,14},... | collective-permute-start | bytes 786440 | tf_op jit(solution)/shard_map/ppermute | solution.py:535
  25.1 74.0 %collective-permute-start.2 = (bf16[512,2048]{1,0:T(8,128)(2,1)S(1)}, bf16[512,2048]{1,0:T(8,128)(2,1)S(1)}, u32[]{:S(2)}, u32[]{:S(2)}) collective-permute-start(bf16[512,2048]{1,0:T(8,128)(2,1)S(1)} %get-tuple-element.42.refs_3_.refs_1_), channel_id=1, source_target_pairs={{0,4},{4,0},{8,12},{12,8},{1,5},{5,1},{9,13},{13,9},{2,6},{6,2},{1... | collective-permute-start | bytes 6291464 | tf_op jit(solution)/shard_map/ppermute | solution.py:538
  30.7 21.6 %collective-permute-start.38 = (bf16[64,2048]{1,0:T(8,128)(2,1)S(1)}, bf16[64,2048]{1,0:T(8,128)(2,1)S(1)}, u32[]{:S(2)}, u32[]{:S(2)}) collective-permute-start(bf16[64,2048]{1,0:T(8,128)(2,1)S(1)} %get-tuple-element.66), channel_id=1, source_target_pairs={{0,8},{4,12},{8,0},{12,4},{1,9},{5,13},{9,1},{13,5},{2,10},{6,14},... | collective-permute-start | bytes 786440 | tf_op jit(solution)/shard_map/ppermute | solution.py:535
  36.3 67.0 %collective-permute-start.19 = (bf16[512,2048]{1,0:T(8,128)(2,1)S(1)}, bf16[512,2048]{1,0:T(8,128)(2,1)S(1)}, u32[]{:S(2)}, u32[]{:S(2)}) collective-permute-start(bf16[512,2048]{1,0:T(8,128)(2,1)S(1)} %get-tuple-element.49.refs_12_.refs_19_), channel_id=1, source_target_pairs={{0,4},{4,0},{8,12},{12,8},{1,5},{5,1},{9,13},{13,9},{2,6},{6,2},{1... | collective-permute-start | bytes 6291464 | tf_op jit(solution)/shard_map/ppermute | solution.py:538
  41.9 12.1 %collective-permute-start.12 = (bf16[256,512]{1,0:T(8,128)(2,1)S(1)}, bf16[256,512]{1,0:T(8,128)(2,1)S(1)}, u32[]{:S(2)}, u32[]{:S(2)}) collective-permute-start(bf16[256,512]{1,0:T(8,128)(2,1)S(1)} %collective-permute-done.11.refs_9_.refs_7_), channel_id=1, source_target_pairs={{0,16},{16,0},{1,17},{17,1},{2,18},{18,2},{3,19},{19,3},{4,20},{20... | collective-permute-start | bytes 786440 | tf_op jit(solution)/shard_map/ppermute | solution.py:532
  47.5 24.4 %collective-permute-start.1 = (bf16[128,2048]{1,0:T(8,128)(2,1)S(1)}, bf16[128,2048]{1,0:T(8,128)(2,1)S(1)}, u32[]{:S(2)}, u32[]{:S(2)}) collective-permute-start(bf16[128,2048]{1,0:T(8,128)(2,1)S(1)} %get-tuple-element.41.refs_1_), channel_id=1, source_target_pairs={{0,2},{1,3},{2,0},{3,1},{4,6},{5,7},{6,4},{7,5},{8,10},{9,11},{10,... | collective-permute-start | bytes 1572872 | tf_op jit(solution)/shard_map/ppermute | solution.py:541
  52.3 9.2 %collective-permute-start.16 = (bf16[256,512]{1,0:T(8,128)(2,1)S(1)}, bf16[256,512]{1,0:T(8,128)(2,1)S(1)}, u32[]{:S(2)}, u32[]{:S(2)}) collective-permute-start(bf16[256,512]{1,0:T(8,128)(2,1)S(1)} %collective-permute-done.15.refs_13_.refs_11_), channel_id=1, source_target_pairs={{0,16},{16,0},{1,17},{17,1},{2,18},{18,2},{3,19},{19,3},{4,20},{20... | collective-permute-start | bytes 786440 | tf_op jit(solution)/shard_map/ppermute | solution.py:532
  54.0 11.4 %collective-permute-start.4 = (bf16[256,512]{1,0:T(8,128)(2,1)S(1)}, bf16[256,512]{1,0:T(8,128)(2,1)S(1)}, u32[]{:S(2)}, u32[]{:S(2)}) collective-permute-start(bf16[256,512]{1,0:T(8,128)(2,1)S(1)} %collective-permute-done.3.refs_5_.refs_15_), channel_id=1, source_target_pairs={{0,16},{16,0},{1,17},{17,1},{2,18},{18,2},{3,19},{19,3},{4,20},{20... | collective-permute-start | bytes 786440 | tf_op jit(solution)/shard_map/ppermute | solution.py:532
  61.5 11.9 %collective-permute-start.13 = (bf16[256,512]{1,0:T(8,128)(2,1)S(1)}, bf16[256,512]{1,0:T(8,128)(2,1)S(1)}, u32[]{:S(2)}, u32[]{:S(2)}) collective-permute-start(bf16[256,512]{1,0:T(8,128)(2,1)S(1)} %collective-permute-done.11.refs_9_.refs_7_), channel_id=1, source_target_pairs={{0,4},{4,0},{8,12},{12,8},{1,5},{5,1},{9,13},{13,9},{2,6},{6,2},{1... | collective-permute-start | bytes 786440 | tf_op jit(solution)/shard_map/ppermute | solution.py:538
  65.4 8.6 %collective-permute-start.17 = (bf16[256,512]{1,0:T(8,128)(2,1)S(1)}, bf16[256,512]{1,0:T(8,128)(2,1)S(1)}, u32[]{:S(2)}, u32[]{:S(2)}) collective-permute-start(bf16[256,512]{1,0:T(8,128)(2,1)S(1)} %collective-permute-done.15.refs_13_.refs_11_), channel_id=1, source_target_pairs={{0,4},{4,0},{8,12},{12,8},{1,5},{5,1},{9,13},{13,9},{2,6},{6,2},{1... | collective-permute-start | bytes 786440 | tf_op jit(solution)/shard_map/ppermute | solution.py:538
  71.9 7.3 %collective-permute-start.8 = (bf16[256,512]{1,0:T(8,128)(2,1)S(1)}, bf16[256,512]{1,0:T(8,128)(2,1)S(1)}, u32[]{:S(2)}, u32[]{:S(2)}) collective-permute-start(bf16[256,512]{1,0:T(8,128)(2,1)S(1)} %collective-permute-done.7.refs_5_.refs_3_), channel_id=1, source_target_pairs={{0,16},{16,0},{1,17},{17,1},{2,18},{18,2},{3,19},{19,3},{4,20},{20... | collective-permute-start | bytes 786440 | tf_op jit(solution)/shard_map/ppermute | solution.py:532
  73.3 12.6 %collective-permute-start = (bf16[128,2048]{1,0:T(8,128)(2,1)S(1)}, bf16[128,2048]{1,0:T(8,128)(2,1)S(1)}, u32[]{:S(2)}, u32[]{:S(2)}) collective-permute-start(bf16[128,2048]{1,0:T(8,128)(2,1)S(1)} %get-tuple-element.41.refs_1_), channel_id=1, source_target_pairs={{0,1},{1,0},{2,3},{3,2},{4,5},{5,4},{6,7},{7,6},{8,9},{9,8},{10,11... | collective-permute-start | bytes 1572872 | tf_op jit(solution)/shard_map/ppermute | solution.py:541
  74.0 5.2 %collective-permute-start.5 = (bf16[256,512]{1,0:T(8,128)(2,1)S(1)}, bf16[256,512]{1,0:T(8,128)(2,1)S(1)}, u32[]{:S(2)}, u32[]{:S(2)}) collective-permute-start(bf16[256,512]{1,0:T(8,128)(2,1)S(1)} %collective-permute-done.3.refs_5_.refs_15_), channel_id=1, source_target_pairs={{0,4},{4,0},{8,12},{12,8},{1,5},{5,1},{9,13},{13,9},{2,6},{6,2},{1... | collective-permute-start | bytes 786440 | tf_op jit(solution)/shard_map/ppermute | solution.py:538
  79.2 1.5 collective-permute-start.9
  79.2 9.2 %collective-permute-start.25 = (bf16[64,2048]{1,0:T(8,128)(2,1)S(1)}, bf16[64,2048]{1,0:T(8,128)(2,1)S(1)}, u32[]{:S(2)}, u32[]{:S(2)}) collective-permute-start(bf16[64,2048]{1,0:T(8,128)(2,1)S(1)} %collective-permute-done.24.refs_8_), channel_id=1, source_target_pairs={{0,16},{16,0},{1,17},{17,1},{2,18},{18,2},{3,19},{19,3},{4,20},{20... | collective-permute-start | bytes 786440 | tf_op jit(solution)/shard_map/ppermute | solution.py:532
  80.7 12.8 %collective-permute-start.29 = (bf16[64,2048]{1,0:T(8,128)(2,1)S(1)}, bf16[64,2048]{1,0:T(8,128)(2,1)S(1)}, u32[]{:S(2)}, u32[]{:S(2)}) collective-permute-start(bf16[64,2048]{1,0:T(8,128)(2,1)S(1)} %collective-permute-done.28.refs_12_), channel_id=1, source_target_pairs={{0,16},{16,0},{1,17},{17,1},{2,18},{18,2},{3,19},{19,3},{4,20},{20... | collective-permute-start | bytes 786440 | tf_op jit(solution)/shard_map/ppermute | solution.py:532
  85.9 7.6 %collective-permute-start.26 = (bf16[64,2048]{1,0:T(8,128)(2,1)S(1)}, bf16[64,2048]{1,0:T(8,128)(2,1)S(1)}, u32[]{:S(2)}, u32[]{:S(2)}) collective-permute-start(bf16[64,2048]{1,0:T(8,128)(2,1)S(1)} %collective-permute-done.24.refs_8_), channel_id=1, source_target_pairs={{0,4},{4,0},{8,12},{12,8},{1,5},{5,1},{9,13},{13,9},{2,6},{6,2},{1... | collective-permute-start | bytes 786440 | tf_op jit(solution)/shard_map/ppermute | solution.py:538
  88.4 5.7 %collective-permute-start.30 = (bf16[64,2048]{1,0:T(8,128)(2,1)S(1)}, bf16[64,2048]{1,0:T(8,128)(2,1)S(1)}, u32[]{:S(2)}, u32[]{:S(2)}) collective-permute-start(bf16[64,2048]{1,0:T(8,128)(2,1)S(1)} %collective-permute-done.28.refs_12_), channel_id=1, source_target_pairs={{0,4},{4,0},{8,12},{12,8},{1,5},{5,1},{9,13},{13,9},{2,6},{6,2},{1... | collective-permute-start | bytes 786440 | tf_op jit(solution)/shard_map/ppermute | solution.py:538
  93.5 1.5 collective-permute-start.14
  93.5 1.9 %collective-permute-start.18 = (bf16[256,512]{1,0:T(8,128)(2,1)S(1)}, bf16[256,512]{1,0:T(8,128)(2,1)S(1)}, u32[]{:S(2)}, u32[]{:S(2)}) collective-permute-start(bf16[256,512]{1,0:T(8,128)(2,1)S(1)} %collective-permute-done.16.refs_14_.refs_12_), channel_id=1, source_target_pairs={{0,4},{4,0},{8,12},{12,8},{1,5},{5,1},{9,13},{13,9},{2,6},{6,2},{1... | collective-permute-start | bytes 786440 | tf_op jit(solution)/shard_map/ppermute | solution.py:538
  94.0 3.0 %collective-permute-start.6 = (bf16[256,512]{1,0:T(8,128)(2,1)S(1)}, bf16[256,512]{1,0:T(8,128)(2,1)S(1)}, u32[]{:S(2)}, u32[]{:S(2)}) collective-permute-start(bf16[256,512]{1,0:T(8,128)(2,1)S(1)} %collective-permute-done.4.refs_6_.refs_16_), channel_id=1, source_target_pairs={{0,4},{4,0},{8,12},{12,8},{1,5},{5,1},{9,13},{13,9},{2,6},{6,2},{1... | collective-permute-start | bytes 786440 | tf_op jit(solution)/shard_map/ppermute | solution.py:538
  95.1 3.4 %collective-permute-start.10 = (bf16[256,512]{1,0:T(8,128)(2,1)S(1)}, bf16[256,512]{1,0:T(8,128)(2,1)S(1)}, u32[]{:S(2)}, u32[]{:S(2)}) collective-permute-start(bf16[256,512]{1,0:T(8,128)(2,1)S(1)} %collective-permute-done.8.refs_6_.refs_4_), channel_id=1, source_target_pairs={{0,4},{4,0},{8,12},{12,8},{1,5},{5,1},{9,13},{13,9},{2,6},{6,2},{1... | collective-permute-start | bytes 786440 | tf_op jit(solution)/shard_map/ppermute | solution.py:538
  95.4 15.8 %collective-permute-start.22 = (bf16[128,2048]{1,0:T(8,128)(2,1)S(1)}, bf16[128,2048]{1,0:T(8,128)(2,1)S(1)}, u32[]{:S(2)}, u32[]{:S(2)}) collective-permute-start(bf16[128,2048]{1,0:T(8,128)(2,1)S(1)} %collective-permute-done.1.refs_2_), channel_id=1, source_target_pairs={{0,1},{1,0},{2,3},{3,2},{4,5},{5,4},{6,7},{7,6},{8,9},{9,8},{10,11... | collective-permute-start | bytes 1572872 | tf_op jit(solution)/shard_map/ppermute | solution.py:541
  97.0 11.6 %collective-permute-start.35 = (bf16[64,2048]{1,0:T(8,128)(2,1)S(1)}, bf16[64,2048]{1,0:T(8,128)(2,1)S(1)}, u32[]{:S(2)}, u32[]{:S(2)}) collective-permute-start(bf16[64,2048]{1,0:T(8,128)(2,1)S(1)} %collective-permute-done.34.refs_8_), channel_id=1, source_target_pairs={{0,16},{16,0},{1,17},{17,1},{2,18},{18,2},{3,19},{19,3},{4,20},{20... | collective-permute-start | bytes 786440 | tf_op jit(solution)/shard_map/ppermute | solution.py:532
  98.5 12.2 %collective-permute-start.39 = (bf16[64,2048]{1,0:T(8,128)(2,1)S(1)}, bf16[64,2048]{1,0:T(8,128)(2,1)S(1)}, u32[]{:S(2)}, u32[]{:S(2)}) collective-permute-start(bf16[64,2048]{1,0:T(8,128)(2,1)S(1)} %collective-permute-done.38.refs_12_), channel_id=1, source_target_pairs={{0,16},{16,0},{1,17},{17,1},{2,18},{18,2},{3,19},{19,3},{4,20},{20... | collective-permute-start | bytes 786440 | tf_op jit(solution)/shard_map/ppermute | solution.py:532
  99.0 11.7 %collective-permute-start.27 = (bf16[64,2048]{1,0:T(8,128)(2,1)S(1)}, bf16[64,2048]{1,0:T(8,128)(2,1)S(1)}, u32[]{:S(2)}, u32[]{:S(2)}) collective-permute-start(bf16[64,2048]{1,0:T(8,128)(2,1)S(1)} %collective-permute-done.25.refs_9_), channel_id=1, source_target_pairs={{0,4},{4,0},{8,12},{12,8},{1,5},{5,1},{9,13},{13,9},{2,6},{6,2},{1... | collective-permute-start | bytes 786440 | tf_op jit(solution)/shard_map/ppermute | solution.py:538
  103.3 14.5 %collective-permute-start.31 = (bf16[64,2048]{1,0:T(8,128)(2,1)S(1)}, bf16[64,2048]{1,0:T(8,128)(2,1)S(1)}, u32[]{:S(2)}, u32[]{:S(2)}) collective-permute-start(bf16[64,2048]{1,0:T(8,128)(2,1)S(1)} %collective-permute-done.29.refs_13_), channel_id=1, source_target_pairs={{0,4},{4,0},{8,12},{12,8},{1,5},{5,1},{9,13},{13,9},{2,6},{6,2},{1... | collective-permute-start | bytes 786440 | tf_op jit(solution)/shard_map/ppermute | solution.py:538
  108.6 12.5 %collective-permute-start.36 = (bf16[64,2048]{1,0:T(8,128)(2,1)S(1)}, bf16[64,2048]{1,0:T(8,128)(2,1)S(1)}, u32[]{:S(2)}, u32[]{:S(2)}) collective-permute-start(bf16[64,2048]{1,0:T(8,128)(2,1)S(1)} %collective-permute-done.34.refs_8_), channel_id=1, source_target_pairs={{0,4},{4,0},{8,12},{12,8},{1,5},{5,1},{9,13},{13,9},{2,6},{6,2},{1... | collective-permute-start | bytes 786440 | tf_op jit(solution)/shard_map/ppermute | solution.py:538
  110.7 10.5 %collective-permute-start.40 = (bf16[64,2048]{1,0:T(8,128)(2,1)S(1)}, bf16[64,2048]{1,0:T(8,128)(2,1)S(1)}, u32[]{:S(2)}, u32[]{:S(2)}) collective-permute-start(bf16[64,2048]{1,0:T(8,128)(2,1)S(1)} %collective-permute-done.38.refs_12_), channel_id=1, source_target_pairs={{0,4},{4,0},{8,12},{12,8},{1,5},{5,1},{9,13},{13,9},{2,6},{6,2},{1... | collective-permute-start | bytes 786440 | tf_op jit(solution)/shard_map/ppermute | solution.py:538
  110.7 10.5 %collective-permute-start.37 = (bf16[64,2048]{1,0:T(8,128)(2,1)S(1)}, bf16[64,2048]{1,0:T(8,128)(2,1)S(1)}, u32[]{:S(2)}, u32[]{:S(2)}) collective-permute-start(bf16[64,2048]{1,0:T(8,128)(2,1)S(1)} %collective-permute-done.35.refs_9_), channel_id=1, source_target_pairs={{0,4},{4,0},{8,12},{12,8},{1,5},{5,1},{9,13},{13,9},{2,6},{6,2},{1... | collective-permute-start | bytes 786440 | tf_op jit(solution)/shard_map/ppermute | solution.py:538
  111.2 10.0 %collective-permute-start.41 = (bf16[64,2048]{1,0:T(8,128)(2,1)S(1)}, bf16[64,2048]{1,0:T(8,128)(2,1)S(1)}, u32[]{:S(2)}, u32[]{:S(2)}) collective-permute-start(bf16[64,2048]{1,0:T(8,128)(2,1)S(1)} %collective-permute-done.39.refs_13_), channel_id=1, source_target_pairs={{0,4},{4,0},{8,12},{12,8},{1,5},{5,1},{9,13},{13,9},{2,6},{6,2},{1... | collective-permute-start | bytes 786440 | tf_op jit(solution)/shard_map/ppermute | solution.py:538
  120.4 9.3 %collective-permute-start.32 = (bf16[128,512]{1,0:T(8,128)(2,1)S(1)}, bf16[128,512]{1,0:T(8,128)(2,1)S(1)}, u32[]{:S(2)}, u32[]{:S(2)}) collective-permute-start(bf16[128,512]{1,0:T(8,128)(2,1)S(1)} %get-tuple-element.64), channel_id=1, source_target_pairs={{0,1},{1,0},{2,3},{3,2},{4,5},{5,4},{6,7},{7,6},{8,9},{9,8},{10,11... | collective-permute-start | bytes 393224 | tf_op jit(solution)/shard_map/ppermute | solution.py:541
  123.9 7.0 %collective-permute-start.43 = (bf16[128,512]{1,0:T(8,128)(2,1)S(1)}, bf16[128,512]{1,0:T(8,128)(2,1)S(1)}, u32[]{:S(2)}, u32[]{:S(2)}) collective-permute-start(bf16[128,512]{1,0:T(8,128)(2,1)S(1)} %get-tuple-element.76), channel_id=1, source_target_pairs={{0,1},{1,0},{2,3},{3,2},{4,5},{5,4},{6,7},{7,6},{8,9},{9,8},{10,11... | collective-permute-start | bytes 393224 | tf_op jit(solution)/shard_map/ppermute | solution.py:541
  125.4 13.5 %collective-permute-start.23 = (bf16[128,1024]{1,0:T(8,128)(2,1)S(1)}, bf16[128,1024]{1,0:T(8,128)(2,1)S(1)}, u32[]{:S(2)}, u32[]{:S(2)}) collective-permute-start(bf16[128,1024]{1,0:T(8,128)(2,1)S(1)} %get-tuple-element.53), channel_id=1, source_target_pairs={{0,3},{1,2},{2,1},{3,0},{4,7},{5,6},{6,5},{7,4},{8,11},{9,10},{10,... | collective-permute-start | bytes 786440 | tf_op jit(solution)/shard_map/ppermute | solution.py:541
  128.8 17.4 %collective-permute-start.20 = (bf16[128,1024]{1,0:T(8,128)(2,1)S(1)}, bf16[128,1024]{1,0:T(8,128)(2,1)S(1)}, u32[]{:S(2)}, u32[]{:S(2)}) collective-permute-start(bf16[128,1024]{1,0:T(8,128)(2,1)S(1)} %get-tuple-element.51), channel_id=1, source_target_pairs={{0,1},{1,0},{2,3},{3,2},{4,5},{5,4},{6,7},{7,6},{8,9},{9,8},{10,11... | collective-permute-start | bytes 786440 | tf_op jit(solution)/shard_map/ppermute | solution.py:541
  129.3 23.6 %collective-permute-start.21 = (bf16[128,1024]{1,0:T(8,128)(2,1)S(1)}, bf16[128,1024]{1,0:T(8,128)(2,1)S(1)}, u32[]{:S(2)}, u32[]{:S(2)}) collective-permute-start(bf16[128,1024]{1,0:T(8,128)(2,1)S(1)} %get-tuple-element.52), channel_id=1, source_target_pairs={{0,2},{1,3},{2,0},{3,1},{4,6},{5,7},{6,4},{7,5},{8,10},{9,11},{10,... | collective-permute-start | bytes 786440 | tf_op jit(solution)/shard_map/ppermute | solution.py:541
  129.8 33.8 %collective-permute-start.42 = (bf16[128,1024]{1,0:T(8,128)(2,1)S(1)}, bf16[128,1024]{1,0:T(8,128)(2,1)S(1)}, u32[]{:S(2)}, u32[]{:S(2)}) collective-permute-start(bf16[128,1024]{1,0:T(8,128)(2,1)S(1)} %get-tuple-element.74), channel_id=1, source_target_pairs={{0,1},{1,0},{2,3},{3,2},{4,5},{5,4},{6,7},{7,6},{8,9},{9,8},{10,11... | collective-permute-start | bytes 786440 | tf_op jit(solution)/shard_map/ppermute | solution.py:541
  130.9 30.4 %collective-permute-start.33 = (bf16[128,512]{1,0:T(8,128)(2,1)S(1)}, bf16[128,512]{1,0:T(8,128)(2,1)S(1)}, u32[]{:S(2)}, u32[]{:S(2)}) collective-permute-start(bf16[128,512]{1,0:T(8,128)(2,1)S(1)} %add_convert_fusion.1), channel_id=1, source_target_pairs={{0,2},{1,3},{2,0},{3,1},{4,6},{5,7},{6,4},{7,5},{8,10},{9,11},{10,... | collective-permute-start | bytes 393224 | tf_op jit(solution)/shard_map/ppermute | solution.py:541
  138.8 22.4 %copy-start = (bf16[128,1024]{1,0:T(8,128)(2,1)}, bf16[128,1024]{1,0:T(8,128)(2,1)S(1)}, u32[]{:S(2)}) copy-start(bf16[128,1024]{1,0:T(8,128)(2,1)S(1)} %collective-permute-done.23.refs_4_) | copy-start | bytes 786436
  138.8 24.8 %collective-permute-start.44 = (bf16[128,512]{1,0:T(8,128)(2,1)S(1)}, bf16[128,512]{1,0:T(8,128)(2,1)S(1)}, u32[]{:S(2)}, u32[]{:S(2)}) collective-permute-start(bf16[128,512]{1,0:T(8,128)(2,1)S(1)} %add_convert_fusion), channel_id=1, source_target_pairs={{0,2},{1,3},{2,0},{3,1},{4,6},{5,7},{6,4},{7,5},{8,10},{9,11},{10,... | collective-permute-start | bytes 393224 | tf_op jit(solution)/shard_map/ppermute | solution.py:541
  146.2 15.1 %copy-start.1 = (bf16[128,1024]{1,0:T(8,128)(2,1)}, bf16[128,1024]{1,0:T(8,128)(2,1)S(1)}, u32[]{:S(2)}) copy-start(bf16[128,1024]{1,0:T(8,128)(2,1)S(1)} %collective-permute-done.20.refs_2_) | copy-start | bytes 786436
  152.9 8.4 %copy-start.2 = (bf16[128,1024]{1,0:T(8,128)(2,1)}, bf16[128,1024]{1,0:T(8,128)(2,1)S(1)}, u32[]{:S(2)}) copy-start(bf16[128,1024]{1,0:T(8,128)(2,1)S(1)} %collective-permute-done.21.refs_3_) | copy-start | bytes 786436
  (1 other events, 0.6 us)
